TPU v7x, 256 devices: a whole 4x4x8 slice. The times are simulated.
256 devices in a mesh: row: 32 (over z, x), col: 8 (over y, core).
Axes of the slice: x: 4, y: 4, z: 8, core: 2. Of those that a mesh axis runs over, the one named last changes fastest.
Arguments:
- tokens: bfloat16 [8192, 2048], P('row'), may hold values from -6 to 6
- norm_gain: float32 [2048], replicated, may hold values from 0.5 to 1.5
- first_gate: bfloat16 [2048, 1024], P(None, 'col'), may hold values from -0.125 to 0.125
- second_gate: bfloat16 [2048, 1024], P(None, 'col'), may hold values from -0.125 to 0.125
- value_weight: bfloat16 [2048, 1024], P(None, 'col'), may hold values from -0.125 to 0.125
- short_weight: bfloat16 [3, 3, 1024], P(None, None, 'col'), may hold values from -3.5 to 3.5
- short_bias: float32 [3, 1024], P(None, 'col'), may hold values from -2 to 2
- embed_weight: float32 [33, 64], replicated, may hold values from -1 to 1
- embed_bias: float32 [64], replicated, may hold values from -3 to 3
- inner_weight: float32 [64, 64], replicated, may hold values from -0.75 to 0.75
- inner_bias: float32 [64], replicated, may hold values from -3 to 3
- filter_freq: float32 [64], replicated, may hold values from 0.5 to 1.5
- filter_weight: float32 [2, 2, 64, 1024], P(None, None, None, ('col', 'row')), may hold values from -0.0234375 to 0.0234375
- filter_skip: float32 [2, 1024], P(None, ('col', 'row')), may hold values from -3 to 3
- output_gain: float32 [1024], P('col'), may hold values from 0.5 to 1.5
- output_weight: bfloat16 [1024, 2048], replicated, may hold values from -0.1875 to 0.1875
Outputs:
- mixed_output: bfloat16 [8192, 2048], P(('row', 'col'))
All inputs are finite; a program needn't handle non-finite values.
Results may differ from a plain program's by a relative error of at most 0.01.
Values may be sent and summed in bfloat16 or wider, within the bound.
No kernel may reach another device: no remote copies, remote signals or barrier semaphores. Data moves between devices by JAX's collectives and lax.ppermute only.
A program may use at most 64 MiB of HBM per device.

v0:
```python
import math

import jax
import jax.numpy as jnp
from jax import lax
from jax.sharding import PartitionSpec as P

CHANNELS = 1024
GROUPS = 8
FREQ_BANDS = 16


HIGHEST = lax.Precision.HIGHEST
NORM_EPS = 1e-06
DECAY_TARGET = 0.01
FAST_SPAN = 0.3
SLOW_SPAN = 1.5


def for_sending(value):
    return jax.tree.map(lambda a: a.astype(jnp.bfloat16) if a.dtype == jnp.float32 else a, value)


def position_features(length):
    position_ramp = jnp.linspace(0.0, 1.0, length, dtype=jnp.float32)[:, None]
    angles = 2.0 * math.pi * jnp.arange(length, dtype=jnp.float32)[:, None] / length
    band_freqs = jnp.linspace(0.0001, FREQ_BANDS - 1, FREQ_BANDS, dtype=jnp.float32)[None, :]
    features = jnp.concatenate(
        [position_ramp, jnp.cos(band_freqs * angles), -jnp.sin(band_freqs * angles)], axis=1
    )
    return (position_ramp, features)


def filter_hidden(length, embed_weight, embed_bias, inner_weight, inner_bias, filter_freq):
    position_ramp, features = position_features(length)
    hidden = jnp.sin(
        filter_freq * (jnp.dot(features, embed_weight, precision=HIGHEST) + embed_bias)
    )
    hidden = jnp.sin(filter_freq * (jnp.dot(hidden, inner_weight, precision=HIGHEST) + inner_bias))
    return (position_ramp, hidden)


def decay_rates():
    fastest = math.log(DECAY_TARGET) / FAST_SPAN
    slowest = math.log(DECAY_TARGET) / SLOW_SPAN
    return jnp.abs(jnp.linspace(slowest, fastest, CHANNELS, dtype=jnp.float32))


def short_filter(padded, weights, bias_row, length):
    result = bias_row.astype(jnp.float32)
    for tap_index in range(weights.shape[0]):
        result = result + padded[tap_index : tap_index + length].astype(jnp.float32) * weights[
            tap_index
        ].astype(jnp.float32)
    return result


def phase_table(rows, cols, period):
    phase_index = (
        lax.broadcasted_iota(jnp.int32, (rows, cols), 0)
        * lax.broadcasted_iota(jnp.int32, (rows, cols), 1)
        % period
    )
    phase_angle = phase_index.astype(jnp.float32) * (2.0 * math.pi / period)
    return (jnp.cos(phase_angle), jnp.sin(phase_angle))


def split_length(total_size):
    chosen = 2
    for candidate in range(2, math.isqrt(total_size) + 1, 2):
        if total_size % candidate == 0:
            chosen = candidate
    return chosen


def make_tables(total_size):
    major_size = split_length(total_size)
    minor_size = total_size // major_size
    inner_table = phase_table(major_size, major_size, major_size)
    twiddle = phase_table(major_size, minor_size, total_size)
    outer_table = phase_table(minor_size, minor_size, minor_size)
    return (major_size, minor_size, inner_table, twiddle, outer_table)


def finish_forward(part_real, part_imag, twiddle, outer_table):
    turn_cos = twiddle[0][:, :, None]
    turn_sin = twiddle[1][:, :, None]
    turned_real = part_real * turn_cos + part_imag * turn_sin
    turned_imag = part_imag * turn_cos - part_real * turn_sin
    outer_cos, outer_sin = outer_table
    spec_real = jnp.einsum("anc,nk->akc", turned_real, outer_cos, precision=HIGHEST) + jnp.einsum(
        "anc,nk->akc", turned_imag, outer_sin, precision=HIGHEST
    )
    spec_imag = jnp.einsum("anc,nk->akc", turned_imag, outer_cos, precision=HIGHEST) - jnp.einsum(
        "anc,nk->akc", turned_real, outer_sin, precision=HIGHEST
    )
    return (spec_real, spec_imag)


def forward_signal(signal, tables):
    major_size, minor_size, inner_table, twiddle, outer_table = tables
    channels = signal.shape[1]
    flattened = signal.reshape(major_size // 2, minor_size * channels)
    inner_cos = inner_table[0][:, : major_size // 2]
    inner_sin = inner_table[1][:, : major_size // 2]
    part_real = jnp.dot(inner_cos, flattened, precision=HIGHEST).reshape(
        major_size, minor_size, channels
    )
    part_imag = -jnp.dot(inner_sin, flattened, precision=HIGHEST).reshape(
        major_size, minor_size, channels
    )
    return finish_forward(part_real, part_imag, twiddle, outer_table)


def forward_taps(circular_taps, tables):
    major_size, minor_size, inner_table, twiddle, outer_table = tables
    channels = circular_taps.shape[1]
    flattened = circular_taps.reshape(major_size, minor_size * channels)
    part_real = jnp.dot(inner_table[0], flattened, precision=HIGHEST).reshape(
        major_size, minor_size, channels
    )
    part_imag = -jnp.dot(inner_table[1], flattened, precision=HIGHEST).reshape(
        major_size, minor_size, channels
    )
    return finish_forward(part_real, part_imag, twiddle, outer_table)


def inverse(spec_real, spec_imag, tables):
    major_size, minor_size, inner_table, twiddle, outer_table = tables
    channels = spec_real.shape[2]
    outer_cos, outer_sin = outer_table
    back_real = jnp.einsum("akc,kn->anc", spec_real, outer_cos, precision=HIGHEST) - jnp.einsum(
        "akc,kn->anc", spec_imag, outer_sin, precision=HIGHEST
    )
    back_imag = jnp.einsum("akc,kn->anc", spec_imag, outer_cos, precision=HIGHEST) + jnp.einsum(
        "akc,kn->anc", spec_real, outer_sin, precision=HIGHEST
    )
    turn_cos = twiddle[0][:, :, None]
    turn_sin = twiddle[1][:, :, None]
    turned_real = (back_real * turn_cos - back_imag * turn_sin).reshape(
        major_size, minor_size * channels
    )
    turned_imag = (back_imag * turn_cos + back_real * turn_sin).reshape(
        major_size, minor_size * channels
    )
    half_rows = major_size // 2
    values = jnp.dot(inner_table[0][:half_rows], turned_real, precision=HIGHEST) - jnp.dot(
        inner_table[1][:half_rows], turned_imag, precision=HIGHEST
    )
    return values.reshape(half_rows * minor_size, channels) / (major_size * minor_size)


def two_sided(signal, forward, backward, skip_gain, tables):
    circular_taps = jnp.concatenate([forward, jnp.zeros_like(forward[:1]), backward[:0:-1]], axis=0)
    signal_real, signal_imag = forward_signal(signal, tables)
    taps_real, taps_imag = forward_taps(circular_taps, tables)
    prod_real = signal_real * taps_real - signal_imag * taps_imag
    prod_imag = signal_real * taps_imag + signal_imag * taps_real
    return inverse(prod_real, prod_imag, tables) + signal * skip_gain


def channel_taps(hidden, position_ramp, filter_weight, deltas):
    window = jnp.exp(-position_ramp * deltas[None, :])
    pairs = []
    for order_index in range(filter_weight.shape[0]):
        forward = jnp.dot(hidden, filter_weight[order_index, 0], precision=HIGHEST) * window
        backward = jnp.dot(hidden, filter_weight[order_index, 1], precision=HIGHEST) * window
        pairs.append((forward, backward))
    return pairs


def local(
    tokens,
    norm_gain,
    first_gate,
    second_gate,
    value_weight,
    short_weight,
    short_bias,
    embed_weight,
    embed_bias,
    inner_weight,
    inner_bias,
    filter_freq,
    filter_weight,
    filter_skip,
    output_gain,
    output_weight,
):
    row_count = lax.axis_size("row")
    row_index = lax.axis_index("row")
    col_index = lax.axis_index("col")
    local_tokens = tokens.shape[0]
    length = local_tokens * row_count
    col_width = first_gate.shape[1]
    own_width = col_width // row_count
    widened = tokens.astype(jnp.float32)
    normed = (
        widened
        * lax.rsqrt(jnp.mean(widened * widened, axis=1, keepdims=True) + NORM_EPS)
        * norm_gain
    ).astype(jnp.bfloat16)
    gate_first = jnp.dot(normed, first_gate, preferred_element_type=jnp.float32).astype(
        jnp.bfloat16
    )
    gate_second = jnp.dot(normed, second_gate, preferred_element_type=jnp.float32).astype(
        jnp.bfloat16
    )
    gate_value = jnp.dot(normed, value_weight, preferred_element_type=jnp.float32).astype(
        jnp.bfloat16
    )
    position_ramp, hidden = filter_hidden(
        length, embed_weight, embed_bias, inner_weight, inner_bias, filter_freq
    )
    channel_start = (col_index * row_count + row_index) * own_width
    deltas = lax.dynamic_slice_in_dim(decay_rates(), channel_start, own_width)
    tap_pairs = channel_taps(hidden, position_ramp, filter_weight, deltas)
    tables = make_tables(2 * length)
    half_width = short_weight.shape[1] // 2
    moved = (
        lax.all_to_all(gate_first, "row", split_axis=1, concat_axis=0, tiled=True),
        lax.all_to_all(gate_second, "row", split_axis=1, concat_axis=0, tiled=True),
        lax.all_to_all(gate_value, "row", split_axis=1, concat_axis=0, tiled=True),
    )
    weights_own = lax.dynamic_slice_in_dim(short_weight, row_index * own_width, own_width, 2)
    bias_own = lax.dynamic_slice_in_dim(short_bias, row_index * own_width, own_width, 1)
    smoothed = [
        short_filter(
            jnp.pad(moved[branch], ((half_width, half_width), (0, 0))),
            weights_own[branch],
            bias_own[branch],
            length,
        )
        for branch in range(3)
    ]
    signal = smoothed[2]
    for order_index in range(2):
        signal = smoothed[order_index] * two_sided(
            signal,
            tap_pairs[order_index][0],
            tap_pairs[order_index][1],
            filter_skip[order_index],
            tables,
        )
    result = jax.tree.map(
        lambda part, own: part.astype(own.dtype),
        lax.all_to_all(for_sending(signal), "row", split_axis=0, concat_axis=1, tiled=True),
        signal,
    )
    group_width = CHANNELS // GROUPS
    grouped = result.reshape(local_tokens, col_width // group_width, group_width)
    scaled = grouped * lax.rsqrt(jnp.mean(grouped * grouped, axis=2, keepdims=True) + NORM_EPS)
    mix_local = (scaled.reshape(local_tokens, col_width) * output_gain).astype(jnp.bfloat16)
    gathered = lax.all_to_all(mix_local, "col", split_axis=0, concat_axis=1, tiled=True)
    return jnp.dot(gathered, output_weight, preferred_element_type=jnp.float32).astype(jnp.bfloat16)


def solution(mesh):
    in_specs = (
        P("row", None),
        P(),
        P(None, "col"),
        P(None, "col"),
        P(None, "col"),
        P(None, None, "col"),
        P(None, "col"),
        P(),
        P(),
        P(),
        P(),
        P(),
        P(None, None, None, ("col", "row")),
        P(None, ("col", "row")),
        P("col"),
        P(),
    )
    out_specs = P(("row", "col"), None)
    return jax.shard_map(local, mesh=mesh, in_specs=in_specs, out_specs=out_specs, check_vma=False)
```

profile of v0, /device:TPU:1, one launch (start us, length us, event | category | flops | bytes accessed | tf_op | source)
XLA Modules:
  0.0 213.7 jit_solution(14069972327601891070)
XLA Ops:
  0.0 1.6 fusion.4
  1.6 1.8 convolution_convert_fusion.1
  4.1 12.0 %all-to-all-start.2 = ((bf16[256,32,4]{0,2,1:T(4,128)(2,1)}), bf16[256,32,4]{0,2,1:T(4,128)(2,1)}, u32[]{:S(2)}, u32[]{:S(2)}) async-start(bf16[256,32,4]{0,2,1:T(4,128)(2,1)} %all_to_all.72), calls=%async_computation.2 | async-start | bytes 131072 | tf_op jit(solution)/shard_map/all_to_all | solution.py:223
  16.2 0.9 fusion.96
  18.0 1.9 multiply_cosine_fusion
  20.0 8.7 %fusion.3 = f32[8192,64]{0,1:T(8,128)S(1)} fusion(f32[33,64]{1,0:T(8,128)S(1)} %copy-done.8, f32[8192,16]{0,1:T(8,128)S(1)} %get-tuple-element.16, f32[8192,16]{0,1:T(8,128)S(1)} %get-tuple-element.15, f32[8192,1]{0,1:T(1,128)S(1)} %bitcast.258, f32[64]{0:T(128)S(1)} %copy-done.14, f32[64]{0:T(128)S(1)} %copy-done.11), kind=kOutput, calls=%fused_computation.5 | convolution fusion | flops 209207296 | bytes 3187456 | tf_op jit(solution)/shard_map/dot_general | solution.py:37
  28.7 8.9 %fusion.1 = f32[8192,64]{0,1:T(8,128)S(1)} fusion(f32[8192,64]{0,1:T(8,128)S(1)} %fusion.3, f32[64,64]{1,0:T(8,128)S(1)} %copy-done.7, f32[64]{0:T(128)S(1)} %copy-done.15, f32[64]{0:T(128)S(1)} %copy-done.11), kind=kOutput, calls=%fused_computation.2 | convolution fusion | flops 403701760 | bytes 4211200 | tf_op jit(solution)/shard_map/dot_general | solution.py:39
  37.7 1.2 fusion.130
  38.9 1.2 convolution_multiply_fusion
  40.1 12.5 %convolution_multiply_fusion.1 = f32[8192,4]{0,1:T(4,128)S(1)} fusion(f32[8192,64]{0,1:T(8,128)S(1)} %fusion.1, f32[4]{0:T(128)S(1)} %dynamic_slice.11, f32[8192]{0:T(1024)S(1)} %get-tuple-element.17, f32[2,2,64,4]{2,3,1,0:T(4,128)S(1)} %copy-done.9), kind=kOutput, calls=%fused_computation.7 | convolution fusion | flops 25231360 | bytes 2263552 | tf_op jit(solution)/shard_map/dot_general | solution.py:166
  52.6 1.2 fusion.133
  54.1 5.6 %reverse = f32[8192,4]{0,1:T(4,128)S(1)} reverse(f32[8192,4]{0,1:T(4,128)S(1)} %bitcast.254), dimensions={0} | reverse | bytes 262144
  60.1 5.1 %copy.95 = f32[16384,4]{1,0:T(8,128)} copy(f32[16384,4]{0,1:T(4,128)S(1)} %concatenate.29) | data formatting | bytes 524288 | tf_op jit(solution)/shard_map/concatenate | solution.py:154
  65.2 8.3 %reshape.264 = f32[128,512]{1,0:T(8,128)S(1)} reshape(f32[16384,4]{1,0:T(8,128)} %copy.95) | data formatting | bytes 524288 | tf_op jit(solution)/shard_map/reshape | solution.py:118
  76.5 5.6 %reverse.1 = f32[8192,4]{0,1:T(4,128)S(1)} reverse(f32[8192,4]{0,1:T(4,128)S(1)} %bitcast.253), dimensions={0} | reverse | bytes 262144
  82.5 5.1 %copy.116 = f32[16384,4]{1,0:T(8,128)} copy(f32[16384,4]{0,1:T(4,128)S(1)} %concatenate.30) | data formatting | bytes 524288 | tf_op jit(solution)/shard_map/concatenate | solution.py:154
  87.6 8.3 %reshape.268 = f32[128,512]{1,0:T(8,128)S(1)} reshape(f32[16384,4]{1,0:T(8,128)} %copy.116) | data formatting | bytes 524288 | tf_op jit(solution)/shard_map/reshape | solution.py:118
  97.4 1.4 fusion.62
  98.8 1.4 fusion.66
  100.2 2.3 %convolution_convert_fusion.2 = bf16[256,128]{0,1:T(8,128)(2,1)} fusion(bf16[2048,128]{1,0:T(8,128)(2,1)} %param.18, bf16[256,2048]{1,0:T(8,128)(2,1)S(1)} %copy-done.1, f32[2048]{0:T(1024)S(1)} %copy-done.18, f32[256]{0:T(256)S(1)} %add_rsqrt_fusion.1), kind=kOutput, calls=%fused_computation.44 | convolution fusion | flops 136347648 | bytes 1647616 | tf_op jit(solution)/shard_map/dot_general | solution.py:203
  102.5 1.2 convolution_convert_fusion.3
  108.3 9.6 %all-to-all-start.1 = ((bf16[256,32,4]{0,2,1:T(4,128)(2,1)}), bf16[256,32,4]{0,2,1:T(4,128)(2,1)S(1)}, u32[]{:S(2)}, u32[]{:S(2)}) async-start(bf16[256,32,4]{0,2,1:T(4,128)(2,1)} %all_to_all.68), calls=%async_computation.1 | async-start | bytes 131072 | tf_op jit(solution)/shard_map/all_to_all | solution.py:221
  117.9 1.1 multiply_add_fusion.8
  119.0 2.6 %copy.89 = f32[8192,4]{1,0:T(8,128)} copy(f32[8192,4]{0,1:T(4,128)S(1)} %multiply_add_fusion.8) | data formatting | bytes 262144 | tf_op jit(solution)/shard_map/add | solution.py:52
  121.6 5.0 %reshape.263 = f32[64,512]{1,0:T(8,128)S(1)} reshape(f32[8192,4]{1,0:T(8,128)} %copy.89) | data formatting | bytes 262144 | tf_op jit(solution)/shard_map/reshape | solution.py:103
  129.1 0.7 convolution_add_fusion.7
  129.8 0.7 multiply_subtract_fusion.5
  130.5 0.7 fusion.29
  131.3 0.7 fusion.25
  132.0 0.7 fusion.14
  132.8 0.7 multiply_add_fusion.4
  134.7 5.7 %div.58 = f32[8192,4]{1,0:T(8,128)} reshape(f32[64,512]{1,0:T(8,128)S(1)} %fusion.17) | data formatting | bytes 262144 | tf_op jit(solution)/shard_map/div | solution.py:150
  140.3 2.8 %copy.111 = f32[8192,4]{0,1:T(4,128)S(1)} copy(f32[8192,4]{1,0:T(8,128)} %div.58) | data formatting | bytes 262144 | tf_op jit(solution)/shard_map/div | solution.py:150
  143.2 9.5 %all-to-all-start = ((bf16[256,32,4]{0,2,1:T(4,128)(2,1)}), bf16[256,32,4]{0,2,1:T(4,128)(2,1)S(1)}, u32[]{:S(2)}, u32[]{:S(2)}) async-start(bf16[256,32,4]{0,2,1:T(4,128)(2,1)} %all_to_all.64), calls=%async_computation | async-start | bytes 131072 | tf_op jit(solution)/shard_map/all_to_all | solution.py:222
  152.7 1.2 add_multiply_fusion
  154.0 2.6 %copy.112 = f32[8192,4]{1,0:T(8,128)} copy(f32[8192,4]{0,1:T(4,128)S(1)} %add_multiply_fusion) | data formatting | bytes 262144 | tf_op jit(solution)/shard_map/mul | solution.py:238
  156.6 4.9 %reshape.267 = f32[64,512]{1,0:T(8,128)S(1)} reshape(f32[8192,4]{1,0:T(8,128)} %copy.112) | data formatting | bytes 262144 | tf_op jit(solution)/shard_map/reshape | solution.py:103
  164.0 0.7 convolution_add_fusion.4
  164.7 0.7 multiply_subtract_fusion.1
  165.5 0.7 fusion.23
  166.2 0.7 fusion.19
  167.0 0.7 fusion.12
  167.7 0.8 multiply_add_fusion
  169.6 5.7 %div.60 = f32[8192,4]{1,0:T(8,128)} reshape(f32[64,512]{1,0:T(8,128)S(1)} %fusion.16) | data formatting | bytes 262144 | tf_op jit(solution)/shard_map/div | solution.py:150
  175.3 2.9 %copy.132 = f32[8192,4]{0,1:T(4,128)S(1)} copy(f32[8192,4]{1,0:T(8,128)} %div.60) | data formatting | bytes 262144 | tf_op jit(solution)/shard_map/div | solution.py:150
  178.3 17.8 %all_to_all.86 = bf16[32,256,4]{1,2,0:T(4,128)(2,1)S(1)} all-to-all(bf16[32,256,4]{1,2,0:T(4,128)(2,1)S(1)} %bitcast.257), channel_id=1, replica_groups=mesh['row'=32,'col'=8] {'row'}, dimensions={0} | all-to-all | bytes 131072 | tf_op jit(solution)/shard_map/all_to_all | solution.py:247
  196.9 12.9 %all_to_all.87 = bf16[8,32,128]{2,1,0:T(8,128)(2,1)S(1)} all-to-all(bf16[8,32,128]{2,1,0:T(8,128)(2,1)S(1)} %copy.134), channel_id=1, replica_groups=mesh['row'=32,'col'=8] {'col'}, dimensions={0} | all-to-all | bytes 131072 | tf_op jit(solution)/shard_map/all_to_all | solution.py:254
  209.8 3.7 %convolution_convert_fusion = bf16[32,2048]{1,0:T(8,128)(2,1)} fusion(bf16[1024,2048]{1,0:T(8,128)(2,1)} %param.31, bf16[8,32,128]{2,1,0:T(8,128)(2,1)S(1)} %all_to_all.87), kind=kOutput, calls=%fused_computation.10 | convolution fusion | flops 134283264 | bytes 4390912 | tf_op jit(solution)/shard_map/dot_general | solution.py:255
  (108 shorter events, 19.7 us)
Async XLA Ops:
  0.0 1.6 copy-start
  1.6 18.4 %copy-start.8 = (f32[33,64]{1,0:T(8,128)S(1)}, f32[33,64]{1,0:T(8,128)}, u32[]{:S(2)}) copy-start(f32[33,64]{1,0:T(8,128)} %param.23) | copy-start | bytes 25348
  1.6 18.4 %copy-start.11 = (f32[64]{0:T(128)S(1)}, f32[64]{0:T(128)}, u32[]{:S(2)}) copy-start(f32[64]{0:T(128)} %param.27) | copy-start | bytes 772
  1.6 18.4 %copy-start.14 = (f32[64]{0:T(128)S(1)}, f32[64]{0:T(128)}, u32[]{:S(2)}) copy-start(f32[64]{0:T(128)} %param.24) | copy-start | bytes 772
  4.1 104.2 %all-to-all-start.2 = ((bf16[256,32,4]{0,2,1:T(4,128)(2,1)}), bf16[256,32,4]{0,2,1:T(4,128)(2,1)}, u32[]{:S(2)}, u32[]{:S(2)}) async-start(bf16[256,32,4]{0,2,1:T(4,128)(2,1)} %all_to_all.72), calls=%async_computation.2 | async-start | bytes 131072 | tf_op jit(solution)/shard_map/all_to_all | solution.py:223
  18.0 10.7 %copy-start.7 = (f32[64,64]{1,0:T(8,128)S(1)}, f32[64,64]{1,0:T(8,128)}, u32[]{:S(2)}) copy-start(f32[64,64]{1,0:T(8,128)} %param.25) | copy-start | bytes 49156
  18.0 10.7 %copy-start.15 = (f32[64]{0:T(128)S(1)}, f32[64]{0:T(128)}, u32[]{:S(2)}) copy-start(f32[64]{0:T(128)} %param.26) | copy-start | bytes 772
  28.7 9.0 %copy-start.9 = (f32[2,2,64,4]{2,3,1,0:T(4,128)S(1)}, f32[2,2,64,4]{2,3,1,0:T(4,128)}, u32[]{:S(2)}) copy-start(f32[2,2,64,4]{2,3,1,0:T(4,128)} %param.28) | copy-start | bytes 12292
  96.0 4.2 %copy-start.1 = (bf16[256,2048]{1,0:T(8,128)(2,1)S(1)}, bf16[256,2048]{1,0:T(8,128)(2,1)}, u32[]{:S(2)}) copy-start(bf16[256,2048]{1,0:T(8,128)(2,1)} %param.16) | copy-start | bytes 3145732
  96.0 4.2 %copy-start.18 = (f32[2048]{0:T(1024)S(1)}, f32[2048]{0:T(1024)}, u32[]{:S(2)}) copy-start(f32[2048]{0:T(1024)} %param.17) | copy-start | bytes 24580
  100.2 2.3 %copy-start.17 = (bf16[2048,128]{1,0:T(8,128)(2,1)S(1)}, bf16[2048,128]{1,0:T(8,128)(2,1)}, u32[]{:S(2)}) copy-start(bf16[2048,128]{1,0:T(8,128)(2,1)} %param.19) | copy-start | bytes 1572868
  102.5 2.6 %copy-start.3 = (f32[128,128,4]{1,0,2:T(8,128)S(1)}, f32[128,128,4]{1,0,2:T(8,128)}, u32[]{:S(2)}) copy-start(f32[128,128,4]{1,0,2:T(8,128)} %fusion.62) | copy-start | bytes 786436
  103.7 2.1 copy-start.2
  103.7 2.8 %copy-start.12 = (f32[3,128]{1,0:T(4,128)S(1)}, f32[3,128]{1,0:T(4,128)}, u32[]{:S(2)}) copy-start(f32[3,128]{1,0:T(4,128)} %param.22) | copy-start | bytes 4612
  103.7 2.9 %copy-start.13 = (f32[2,4]{1,0:T(2,128)S(1)}, f32[2,4]{1,0:T(2,128)}, u32[]{:S(2)}) copy-start(f32[2,4]{1,0:T(2,128)} %param.29) | copy-start | bytes 100
  103.7 2.9 %copy-start.10 = (bf16[3,3,128]{2,1,0:T(4,128)(2,1)S(1)}, bf16[3,3,128]{2,1,0:T(4,128)(2,1)}, u32[]{:S(2)}) copy-start(bf16[3,3,128]{2,1,0:T(4,128)(2,1)} %param.21) | copy-start | bytes 6916
  104.4 2.3 %copy-start.6 = (bf16[256,128]{0,1:T(8,128)(2,1)S(1)}, bf16[256,128]{0,1:T(8,128)(2,1)}, u32[]{:S(2)}) copy-start(bf16[256,128]{0,1:T(8,128)(2,1)} %convolution_convert_fusion.2) | copy-start | bytes 196612
  104.4 2.9 %copy-start.5 = (bf16[256,128]{0,1:T(8,128)(2,1)S(1)}, bf16[256,128]{0,1:T(8,128)(2,1)}, u32[]{:S(2)}) copy-start(bf16[256,128]{0,1:T(8,128)(2,1)} %convolution_convert_fusion.3) | copy-start | bytes 196612
  108.3 34.9 %all-to-all-start.1 = ((bf16[256,32,4]{0,2,1:T(4,128)(2,1)}), bf16[256,32,4]{0,2,1:T(4,128)(2,1)S(1)}, u32[]{:S(2)}, u32[]{:S(2)}) async-start(bf16[256,32,4]{0,2,1:T(4,128)(2,1)} %all_to_all.68), calls=%async_computation.1 | async-start | bytes 131072 | tf_op jit(solution)/shard_map/all_to_all | solution.py:221
  121.6 5.7 %copy-start.4 = (f32[128,128]{0,1:T(8,128)S(1)}, f32[128,128]{0,1:T(8,128)}, u32[]{:S(2)}) copy-start(f32[128,128]{0,1:T(8,128)} %fusion.96) | copy-start | bytes 196612
  143.2 35.0 %all-to-all-start = ((bf16[256,32,4]{0,2,1:T(4,128)(2,1)}), bf16[256,32,4]{0,2,1:T(4,128)(2,1)S(1)}, u32[]{:S(2)}, u32[]{:S(2)}) async-start(bf16[256,32,4]{0,2,1:T(4,128)(2,1)} %all_to_all.64), calls=%async_computation | async-start | bytes 131072 | tf_op jit(solution)/shard_map/all_to_all | solution.py:222
  175.3 21.2 %copy-start.16 = (f32[128]{0:T(128)S(1)}, f32[128]{0:T(128)}, u32[]{:S(2)}) copy-start(f32[128]{0:T(128)} %param.30) | copy-start | bytes 1540
where the time goes:
time: 218 us; the launch traced here: 214 us
  local copies, waits for them, and re-layouts  75.2 us (34%)
  matrix products  67.1 us (31%)
  starting transfers between devices  31.1 us (14%)
  blocking collectives  30.7 us (14%)
  other arithmetic  8.72 us (4%)
    all_to_all x1, blocking collectives, local(): lax.all_to_all(for_sending(signal), 'row', split_axis=0, concat_axis=1, t...  17.8 us
    div x4, local copies, waits for them, and re-layouts, inverse(): values.reshape(half_rows * minor_size, channels) / (major_size * minor_size)  17 us
    reshape x2, local copies, waits for them, and re-layouts, forward_taps(): flattened = circular_taps.reshape(major_size, minor_size * channels)  16.7 us
    dot_general x2, matrix products, channel_taps(): jnp.dot(hidden, filter_weight[order_index, 0], precision=HIGHEST) * window  13.7 us
    all_to_all x1, blocking collectives, local(): lax.all_to_all(mix_local, 'col', split_axis=0, concat_axis=1, tiled=True)  12.9 us
    all_to_all x1, starting transfers between devices, local(): lax.all_to_all(gate_value, 'row', split_axis=1, concat_axis=0, tiled=True)  12 us
    unnamed x42, local copies, waits for them, and re-layouts  11.5 us
    concatenate x4, local copies, waits for them, and re-layouts, two_sided(): jnp.concatenate([forward, jnp.zeros_like(forward[:1]), backward[:0:-1]],...  10.7 us
  transfers between devices with their start and end apart: 3, of which 0 were waited for; matrix products, arithmetic and copies ran while one was open for 66% of the time, Pallas kernels for 0%

commit v1 on v0

v1 whole, which is shorter than its diff:
```python
import functools
import math

import jax
import jax.numpy as jnp
from jax import lax
from jax.experimental import pallas as pl
from jax.experimental.pallas import tpu as pltpu
from jax.sharding import PartitionSpec as P

CHANNELS = 1024
FREQ_BANDS = 16
NORM_EPS = 1e-06
DECAY_SLOW = math.log(0.01) / 1.5
DECAY_FAST = math.log(0.01) / 0.3

F32 = jnp.float32
BF16 = jnp.bfloat16

SIN_COEFFS = (
    6.283182818555376,
    -41.34142139902321,
    81.59618388026023,
    -76.58010058967308,
    41.20539511150987,
    -12.271262699024827,
)


def sin_turns(turns):
    r = turns - jnp.floor(turns + 0.5)
    s = r * r
    acc = jnp.full_like(s, SIN_COEFFS[-1])
    for coeff in SIN_COEFFS[-2::-1]:
        acc = acc * s + coeff
    return acc * r


def split(value):
    high = value.astype(BF16)
    low = (value - high.astype(F32)).astype(BF16)
    return high, low


def iota(shape, dim):
    return lax.broadcasted_iota(jnp.int32, shape, dim)


def to_turns(index, period):
    return (index & (period - 1)).astype(F32) * (1.0 / period)


def row_dft_table():
    shape = (128, 192)
    k1, n1 = iota(shape, 0) & 63, iota(shape, 1) & 63
    turns = to_turns((2 * k1 + 1) * n1, 256)
    value = sin_turns(turns + jnp.where(iota(shape, 0) < 64, 0.25, 0.5))
    high = value.astype(BF16).astype(F32)
    return jnp.where(iota(shape, 1) < 128, high, value - high).astype(BF16)


def row_inverse_table(scale):
    shape = (64, 384)
    n1, k1 = iota(shape, 0), iota(shape, 1) & 63
    turns = to_turns((2 * k1 + 1) * n1, 256)
    value = sin_turns(turns + jnp.where((iota(shape, 1) & 64) == 0, 0.25, 0.5)) * scale
    high = value.astype(BF16).astype(F32)
    return jnp.where(iota(shape, 1) < 256, high, value - high).astype(BF16)


def twiddles():
    shape = (64, 128)
    turns = to_turns((2 * iota(shape, 0) + 1) * iota(shape, 1), 32768)
    return sin_turns(turns + 0.25), sin_turns(turns)


def lane_dft():
    shape = (128, 128)
    turns = to_turns(iota(shape, 0) * iota(shape, 1), 128)
    return split(sin_turns(turns + 0.25)), split(sin_turns(turns))


def dot(left, right):
    return jnp.dot(left, right, preferred_element_type=F32)


def stack3(value):
    high, low = split(value)
    return jnp.concatenate([high, low, high], axis=0)


def lanes3(value):
    high, low = split(value)
    return jnp.concatenate([high, low, high], axis=1)


def project_kernel(tokens, gain, w0, w1, w2, out, scratch):
    wide = tokens[...].astype(F32)
    scale = lax.rsqrt(jnp.mean(wide * wide, axis=1, keepdims=True) + NORM_EPS)
    normed = (wide * scale * gain[...]).astype(BF16)
    weights = jnp.concatenate([w0[...], w1[...], w2[...]], axis=1)
    gates = dot(normed, weights)
    for half in range(2):
        for branch in range(3):
            block = gates[half * 128 : half * 128 + 128, branch * 128 : branch * 128 + 128].T
            for peer in range(32):
                start = peer * 24 + half * 12 + branch * 4
                scratch[start : start + 4, :] = block[peer * 4 : peer * 4 + 4, :]
    out[...] = scratch[...].astype(BF16)


def filter_kernel(decay, ew, eb, iw, ib, freq, fw, hre, him, build, lhs1, lhs2, taps):
    length = 8192
    turns_of = freq[...] * (1.0 / (2.0 * math.pi))

    def high_of(value):
        return value.astype(BF16).astype(F32)

    embed = ew[...] * turns_of
    embed_bias = eb[...] * turns_of
    build[...] = jnp.zeros_like(build)
    build[0:33, 0:64] = high_of(embed)
    build[33:34, 0:64] = high_of(embed_bias)
    build[48:81, 0:64] = high_of(embed)
    build[96:129, 0:64] = embed - high_of(embed)
    build[129:130, 0:64] = embed_bias - high_of(embed_bias)
    lhs1[...] = build[...].T[0:64, :].astype(BF16)
    inner = iw[...] * turns_of
    inner_bias = ib[...] * turns_of
    build[...] = jnp.zeros_like(build)
    build[0:64, 0:64] = high_of(inner)
    build[64:128, 0:64] = high_of(inner)
    build[128:192, 0:64] = inner - high_of(inner)
    build[192:193, 0:64] = high_of(inner_bias)
    build[193:194, 0:64] = inner_bias - high_of(inner_bias)
    lhs2[...] = build[...].T[0:64, :].astype(BF16)
    left1 = lhs1[:, 0:144]
    left2 = lhs2[:, 0:208]
    parts = []
    for order in range(2):
        parts.append(fw[order, 0] + fw[order, 1])
        parts.append(fw[order, 0] - fw[order, 1])
    fweights = jnp.concatenate(parts, axis=0)
    fhigh, flow = split(fweights)
    left3 = jnp.concatenate([fhigh, fhigh, flow], axis=1)

    chunk = 1024
    row = iota((48, chunk), 0)
    band_index = jnp.where(row < 17, row - 1, row - 17).astype(F32)
    band_step = (FREQ_BANDS - 1 - 0.0001) / (FREQ_BANDS - 1)
    band = (0.0001 + band_index * band_step) * (1.0 / length)
    phase = jnp.where(row < 17, 0.25, 0.5)
    ones16 = jnp.ones((16, chunk), BF16)
    crow = iota((8, chunk), 0) & 3
    rate = jnp.where(
        crow < 2,
        jnp.where(crow == 0, decay[0], decay[1]),
        jnp.where(crow == 2, decay[2], decay[3]),
    )
    for step in range(length // chunk):
        position = (iota((1, chunk), 1) + step * chunk).astype(F32)
        ramp = position * (1.0 / (length - 1))
        feature = sin_turns(band * position + phase)
        feature = jnp.where(row == 0, ramp, jnp.where(row == 33, 1.0, feature))
        hidden = sin_turns(dot(left1, stack3(feature)))
        hidden = sin_turns(dot(left2, jnp.concatenate([stack3(hidden), ones16], axis=0)))
        value = dot(left3, stack3(hidden))
        window = jnp.exp(ramp * -rate)
        value = value * jnp.concatenate([window, window], axis=0)
        for block in range(chunk // 128):
            piece = value[:, block * 128 : block * 128 + 128]
            n1 = step * (chunk // 128) + block
            if n1 == 0:
                swapped = jnp.concatenate([piece[4:8], piece[0:4], piece[12:16], piece[8:12]], axis=0)
                piece = jnp.where(iota((16, 128), 1) == 0, 0.5 * (piece + swapped), piece)
            taps[n1 * 16 : n1 * 16 + 16, :] = piece

    spread = jnp.concatenate([taps[pl.ds(r, 64, stride=16), :] for r in range(16)], axis=1)
    stage = dot(row_dft_table(), stack3(spread))
    tw_cos, tw_sin = twiddles()
    (cos_high, cos_low), (sin_high, sin_low) = lane_dft()
    real_table = jnp.concatenate([cos_high, sin_high, cos_high, sin_high, cos_low, sin_low], axis=0)
    imag_table = jnp.concatenate([-sin_high, cos_high, -sin_high, cos_high, -sin_low, cos_low], axis=0)
    for kind, table, out in ((0, real_table, hre), (1, imag_table, him)):
        reals, imags = [], []
        for order in range(2):
            for channel in range(4):
                lane = (order * 8 + kind * 4 + channel) * 128
                real, imag = stage[0:64, lane : lane + 128], stage[64:128, lane : lane + 128]
                reals.append(real * tw_cos + imag * tw_sin)
                imags.append(imag * tw_cos - real * tw_sin)
        left = jnp.concatenate([jnp.concatenate(reals, axis=0), jnp.concatenate(imags, axis=0)], axis=1)
        out[...] = dot(lanes3(left), table)


def shifted(value, amount):
    size = 128
    lane, row = iota(value.shape, 1), iota(value.shape, 0)
    rolled = pltpu.roll(value, amount % size, 1)
    carried = pltpu.roll(rolled, amount % 64, 0)
    edge_lane = 0 if amount == 1 else size - 1
    edge_row = 0 if amount == 1 else 63
    carried = jnp.where(row == edge_row, 0.0, carried)
    return jnp.where(lane == edge_lane, carried, rolled)


def conv_kernel(scalars, moved, hre, him, out, wide, result):
    wide[...] = moved[...].astype(F32)
    smoothed = []
    for branch in range(3):
        rows = []
        for channel in range(4):
            value = wide[pl.ds(branch * 4 + channel, 64, stride=12), :]
            base = (branch * 4 + channel) * 4
            total = scalars[base] + shifted(value, 1) * scalars[base + 1]
            total = total + value * scalars[base + 2]
            total = total + shifted(value, -1) * scalars[base + 3]
            rows.append(total)
        smoothed.append(rows)
    forward_rows = row_dft_table()
    inverse_rows = row_inverse_table(1.0 / 8192)
    tw_cos, tw_sin = twiddles()
    (cos_high, cos_low), (sin_high, sin_low) = lane_dft()

    def table(sign):
        def part(cos, sin):
            top = jnp.concatenate([cos, -sin if sign > 0 else sin], axis=1)
            bottom = jnp.concatenate([sin if sign > 0 else -sin, cos], axis=1)
            return jnp.concatenate([top, bottom], axis=0)

        high, low = part(cos_high, sin_high), part(cos_low, sin_low)
        return jnp.concatenate([high, high, low], axis=0)

    forward_lanes, inverse_lanes = table(1), table(-1)
    signal = smoothed[2]
    for order in range(2):
        stage = dot(forward_rows, stack3(jnp.concatenate(signal, axis=1)))
        reals, imags = [], []
        for channel in range(4):
            real = stage[0:64, channel * 128 : channel * 128 + 128]
            imag = stage[64:128, channel * 128 : channel * 128 + 128]
            reals.append(real * tw_cos + imag * tw_sin)
            imags.append(imag * tw_cos - real * tw_sin)
        left = jnp.concatenate([jnp.concatenate(reals, axis=0), jnp.concatenate(imags, axis=0)], axis=1)
        spectrum = dot(lanes3(left), forward_lanes)
        real, imag = spectrum[:, 0:128], spectrum[:, 128:256]
        tap_real = hre[order * 256 : order * 256 + 256, :]
        tap_imag = him[order * 256 : order * 256 + 256, :]
        left = jnp.concatenate(
            [real * tap_real - imag * tap_imag, real * tap_imag + imag * tap_real], axis=1
        )
        back = dot(lanes3(left), inverse_lanes)
        columns = []
        for channel in range(4):
            real = back[channel * 64 : channel * 64 + 64, 0:128]
            imag = back[channel * 64 : channel * 64 + 64, 128:256]
            columns.append(
                jnp.concatenate([real * tw_cos - imag * tw_sin, real * tw_sin + imag * tw_cos], axis=0)
            )
        values = dot(inverse_rows, stack3(jnp.concatenate(columns, axis=1)))
        following = []
        for channel in range(4):
            skip = scalars[48 + order * 4 + channel]
            conv = values[:, channel * 128 : channel * 128 + 128] + signal[channel] * skip
            following.append(smoothed[order][channel] * conv)
        signal = following
    for channel in range(4):
        result[pl.ds(channel, 64, stride=4), :] = signal[channel]
    out[...] = result[...].astype(BF16)


def norm_kernel(moved, gain, out, wide, ordered):
    wide[...] = moved[...].astype(F32)
    for half in range(2):
        for channel in range(4):
            ordered[pl.ds(half * 128 + channel, 32, stride=4), :] = wide[
                pl.ds(half * 4 + channel, 32, stride=8), :
            ]
    for half in range(2):
        value = ordered[half * 128 : half * 128 + 128, :]
        scale = lax.rsqrt(jnp.mean(value * value, axis=0, keepdims=True) + NORM_EPS)
        out[half * 128 : half * 128 + 128, :] = ((value * scale).T * gain[...]).astype(BF16)


def output_kernel(mixed, weight, out):
    left = jnp.concatenate([mixed[c * 32 : c * 32 + 32, :] for c in range(8)], axis=1)
    out[...] = dot(left, weight[...]).astype(BF16)


VMEM = pl.BlockSpec(memory_space=pltpu.VMEM)
SMEM = pl.BlockSpec(memory_space=pltpu.SMEM)


def run(kernel, out_shape, in_specs, scratch, name, interpret=False):
    multi = isinstance(out_shape, (tuple, list))
    return pl.pallas_call(
        kernel,
        out_shape=out_shape,
        in_specs=in_specs,
        out_specs=tuple(VMEM for _ in out_shape) if multi else VMEM,
        scratch_shapes=scratch,
        name=name,
        interpret=interpret,
    )


def shape_of(shape, dtype):
    return jax.ShapeDtypeStruct(shape, dtype)


def local(
    tokens,
    norm_gain,
    first_gate,
    second_gate,
    value_weight,
    short_weight,
    short_bias,
    embed_weight,
    embed_bias,
    inner_weight,
    inner_bias,
    filter_freq,
    filter_weight,
    filter_skip,
    output_gain,
    output_weight,
):
    row_index = lax.axis_index("row")
    col_index = lax.axis_index("col")
    sent = run(
        project_kernel, shape_of((768, 128), BF16), [VMEM] * 5, [pltpu.VMEM((768, 128), F32)], "project"
    )(tokens, norm_gain.reshape(1, -1), first_gate, second_gate, value_weight)
    moved = lax.all_to_all(
        sent.reshape(32, 24, 128), "row", split_axis=0, concat_axis=0, tiled=True
    ).reshape(768, 128)

    channel = ((col_index * 32 + row_index) * 4 + jnp.arange(4)).astype(F32)
    decay = -(DECAY_SLOW + (DECAY_FAST - DECAY_SLOW) * (channel * (1.0 / (CHANNELS - 1))))
    hre, him = run(
        filter_kernel,
        (shape_of((512, 128), F32), shape_of((512, 128), F32)),
        [SMEM] + [VMEM] * 6,
        [
            pltpu.VMEM((256, 128), F32),
            pltpu.VMEM((64, 256), BF16),
            pltpu.VMEM((64, 256), BF16),
            pltpu.VMEM((1024, 128), F32),
        ],
        "filters",
    )(
        decay,
        embed_weight,
        embed_bias.reshape(1, -1),
        inner_weight,
        inner_bias.reshape(1, -1),
        filter_freq.reshape(1, -1),
        filter_weight.transpose(0, 1, 3, 2),
    )
    weights_own = lax.dynamic_slice_in_dim(short_weight, row_index * 4, 4, 2).astype(F32)
    bias_own = lax.dynamic_slice_in_dim(short_bias, row_index * 4, 4, 1)
    taps_own = jnp.concatenate([bias_own[:, None, :], weights_own], axis=1)
    scalars = jnp.concatenate([taps_own.transpose(0, 2, 1).reshape(-1), filter_skip.reshape(-1)])
    mixed = run(
        conv_kernel,
        shape_of((256, 128), BF16),
        [SMEM] + [VMEM] * 3,
        [pltpu.VMEM((768, 128), F32), pltpu.VMEM((256, 128), F32)],
        "convolve",
    )(scalars, moved, hre, him)
    result = lax.all_to_all(
        mixed.reshape(32, 8, 128), "row", split_axis=0, concat_axis=0, tiled=True
    ).reshape(256, 128)
    normed = run(
        norm_kernel,
        shape_of((256, 128), BF16),
        [VMEM] * 2,
        [pltpu.VMEM((256, 128), F32), pltpu.VMEM((256, 128), F32)],
        "groupnorm",
    )(result, output_gain.reshape(1, -1))
    gathered = lax.all_to_all(
        normed.reshape(8, 32, 128), "col", split_axis=0, concat_axis=0, tiled=True
    ).reshape(256, 128)
    return run(output_kernel, shape_of((32, 2048), BF16), [VMEM] * 2, [], "output")(
        gathered, output_weight
    )


def solution(mesh):
    in_specs = (
        P("row", None),
        P(),
        P(None, "col"),
        P(None, "col"),
        P(None, "col"),
        P(None, None, "col"),
        P(None, "col"),
        P(),
        P(),
        P(),
        P(),
        P(),
        P(None, None, None, ("col", "row")),
        P(None, ("col", "row")),
        P("col"),
        P(),
    )
    out_specs = P(("row", "col"), None)
    return jax.shard_map(local, mesh=mesh, in_specs=in_specs, out_specs=out_specs, check_vma=False)
```

time: 218 us -> 66.5 us (0.31); the launches traced: 214 us -> 66 us
  local copies, waits for them, and re-layouts: 75.2 us -> 1.71 us
  matrix products: 67.1 us -> 0 us
  Pallas kernels: 0 us -> 20.4 us
  starting transfers between devices: 31.1 us -> 11.9 us
  other arithmetic: 8.72 us -> 1.85 us
    dot_general x46 -> x0, matrix products: 67.1 us -> none  [the longest x2 13.7 us: channel_taps(): jnp.dot(hidden, filter_weight[order_index, 0], precision=HIGHEST) * window]
    reshape x4 -> x2, local copies, waits for them, and re-layouts: 26.6 us -> 0.85 us  [the longest x1 0.76 us: local(): filter_skip.reshape(-1)]
    pallas_call x0 -> x5, Pallas kernels: none -> 20.4 us  [the longest x1 7.73 us: local(): run(filter_kernel, (shape_of((512, 128), F32), shape_of((512, 128), F32))...]
    all_to_all x3 -> x1, starting transfers between devices: 31.1 us -> 11.9 us  [local(): lax.all_to_all(sent.reshape(32, 24, 128), 'row', split_axis=0, concat_axi...]
    div x4 -> x0, local copies, waits for them, and re-layouts: 17 us -> none  [inverse(): values.reshape(half_rows * minor_size, channels) / (major_size * minor_size)]
    unnamed x42 -> x4, local copies, waits for them, and re-layouts: 11.5 us -> 0.68 us
    concatenate x4 -> x0, local copies, waits for them, and re-layouts: 10.7 us -> none  [two_sided(): jnp.concatenate([forward, jnp.zeros_like(forward[:1]), backward[:0:-1]],...]
    cos x3 -> x0, other arithmetic: 3.05 us -> none  [the longest x1 1.9 us: position_features(): jnp.cos(band_freqs * angles)]
  transfers between devices with their start and end apart: 3 -> 1, of which waited for: 0 -> 1; matrix products, arithmetic and copies ran while one was open for 66% -> 4% of each run, Pallas kernels for 0% -> 12%
where the time goes in v1:
time: 66.5 us; the launch traced here: 66 us
  blocking collectives  30 us (45%)
  Pallas kernels  20.4 us (31%)
  starting transfers between devices  11.9 us (18%)
  other arithmetic  1.85 us (3%)
  local copies, waits for them, and re-layouts  1.71 us (3%)
    all_to_all x1, blocking collectives, local(): lax.all_to_all(mixed.reshape(32, 8, 128), 'row', split_axis=0, concat_axi...  17.9 us
    all_to_all x1, blocking collectives, local(): lax.all_to_all(normed.reshape(8, 32, 128), 'col', split_axis=0, concat_ax...  12.1 us
    all_to_all x1, starting transfers between devices, local(): lax.all_to_all(sent.reshape(32, 24, 128), 'row', split_axis=0, concat_axi...  11.9 us
    pallas_call x1, Pallas kernels, local(): run(filter_kernel, (shape_of((512, 128), F32), shape_of((512, 128), F32))...  7.73 us
    pallas_call x1, Pallas kernels, local(): run(conv_kernel, shape_of((256, 128), BF16), [SMEM] + [VMEM] * 3, [pltpu....  3.9 us
    pallas_call x1, Pallas kernels, local(): run(output_kernel, shape_of((32, 2048), BF16), [VMEM] * 2, [], 'output')  3.71 us
    pallas_call x1, Pallas kernels, local(): run(project_kernel, shape_of((768, 128), BF16), [VMEM] * 5, [pltpu.VMEM((...  3.46 us
    pallas_call x1, Pallas kernels, local(): run(norm_kernel, shape_of((256, 128), BF16), [VMEM] * 2, [pltpu.VMEM((256...  1.65 us
  transfers between devices with their start and end apart: 1, of which 1 were waited for; matrix products, arithmetic and copies ran while one was open for 4% of the time, Pallas kernels for 12%

profile of v1, /device:TPU:1, one launch (start us, length us, event | category | flops | bytes accessed | tf_op | source)
XLA Modules:
  0.0 66.0 jit_solution(4220552899828288177)
XLA Ops:
  0.0 0.0 copy-start
  0.0 3.5 %project.1 = bf16[768,128]{1,0:T(8,128)(2,1)} custom-call(bf16[256,2048]{1,0:T(8,128)(2,1)} %tokens.1, f32[1,2048]{1,0:T(1,128)} %bitcast.22, bf16[2048,128]{1,0:T(8,128)(2,1)} %w0.1, bf16[2048,128]{1,0:T(8,128)(2,1)} %w1.1, bf16[2048,128]{1,0:T(8,128)(2,1)} %w2.1), custom_call_target="tpu_custom_call" | custom-call | tf_op jit(solution)/shard_map/project/pallas_call | solution.py:331
  3.5 11.9 %all-to-all-start = ((bf16[32,24,128]{2,1,0:T(8,128)(2,1)}), bf16[32,24,128]{2,1,0:T(8,128)(2,1)S(1)}, u32[]{:S(2)}, u32[]{:S(2)}) async-start(bf16[32,24,128]{2,1,0:T(8,128)(2,1)} %bitcast.17), calls=%async_computation | async-start | bytes 393216 | tf_op jit(solution)/shard_map/all_to_all | solution.py:334
  15.3 0.8 %dynamic-slice_convert_fusion = f32[3,3,4]{2,1,0:T(4,128)S(1)} fusion(bf16[3,3,128]{2,1,0:T(4,128)(2,1)} %param.21, s32[]{:T(128)S(6)} %select_n.4), kind=kLoop, calls=%fused_computation.1 | loop fusion | flops 36 | bytes 220 | tf_op jit(solution)/shard_map/convert_element_type | solution.py:360
  16.1 0.0 copy-done
  16.1 0.1 dynamic-slice_bitcast_fusion
  16.2 0.8 %reshape.40 = f32[8]{0:T(128)S(1)} reshape(f32[2,4]{1,0:T(2,128)} %param.29) | data formatting | bytes 64 | tf_op jit(solution)/shard_map/reshape | solution.py:363
  16.9 0.1 copy.18
  17.1 0.1 reshape.39
  17.1 0.5 add_negate_fusion.decay
  17.7 7.7 %filters.1 = (f32[512,128]{1,0:T(8,128)}, f32[512,128]{1,0:T(8,128)}) custom-call(f32[4]{0:T(128)} %add_negate_fusion.decay, f32[33,64]{1,0:T(8,128)} %ew.1, f32[1,64]{1,0:T(1,128)} %bitcast.24, f32[64,64]{1,0:T(8,128)} %iw.1, f32[1,64]{1,0:T(1,128)} %bitcast.25, f32[1,64]{1,0:T(1,128)} %bitcast.26, f32[2,2,4,64]{3,2,1,0:T(4,128)} %bitcast.23), custom_call_target="tpu_custom_call" | custom-call | tf_op jit(solution)/shard_map/filters/pallas_call | solution.py:340
  25.4 0.6 pad_maximum_fusion.scalars
  26.0 0.1 all-to-all-done
  26.0 0.0 copy-start.1
  26.0 0.7 %copy-done.1 = bf16[32,24,128]{2,1,0:T(8,128)(2,1)} copy-done((bf16[32,24,128]{2,1,0:T(8,128)(2,1)}, bf16[32,24,128]{2,1,0:T(8,128)(2,1)S(1)}, u32[]{:S(2)}) %copy-start.1) | copy-done | bytes 196632
  26.7 3.9 %convolve.1 = bf16[256,128]{1,0:T(8,128)(2,1)} custom-call(f32[56]{0:T(128)} %pad_maximum_fusion.scalars, bf16[768,128]{1,0:T(8,128)(2,1)} %bitcast.16, f32[512,128]{1,0:T(8,128)} %get-tuple-element.7.hre, f32[512,128]{1,0:T(8,128)} %get-tuple-element.8.him), custom_call_target="tpu_custom_call" | custom-call | tf_op jit(solution)/shard_map/convolve/pallas_call | solution.py:364
  30.6 17.9 %all_to_all.15 = bf16[32,8,128]{2,1,0:T(8,128)(2,1)} all-to-all(bf16[32,8,128]{2,1,0:T(8,128)(2,1)} %bitcast.21), channel_id=1, replica_groups=mesh['row'=32,'col'=8] {'row'}, dimensions={0} | all-to-all | bytes 131072 | tf_op jit(solution)/shard_map/all_to_all | solution.py:371
  48.5 1.6 %groupnorm.1 = bf16[256,128]{1,0:T(8,128)(2,1)} custom-call(bf16[256,128]{1,0:T(8,128)(2,1)} %bitcast.19, f32[1,128]{1,0:T(1,128)} %bitcast.27), custom_call_target="tpu_custom_call" | custom-call | tf_op jit(solution)/shard_map/groupnorm/pallas_call | solution.py:374
  50.2 12.1 %all_to_all.16 = bf16[8,32,128]{2,1,0:T(8,128)(2,1)} all-to-all(bf16[8,32,128]{2,1,0:T(8,128)(2,1)} %bitcast.20), channel_id=1, replica_groups=mesh['row'=32,'col'=8] {'col'}, dimensions={0} | all-to-all | bytes 131072 | tf_op jit(solution)/shard_map/all_to_all | solution.py:381
  62.3 3.7 %output.1 = bf16[32,2048]{1,0:T(8,128)(2,1)} custom-call(bf16[256,128]{1,0:T(8,128)(2,1)} %bitcast.18, bf16[1024,2048]{1,0:T(8,128)(2,1)} %weight.1), custom_call_target="tpu_custom_call" | custom-call | tf_op jit(solution)/shard_map/output/pallas_call | solution.py:384
  (2 shorter events, 0.0 us)
Async XLA Ops:
  0.0 16.1 %copy-start = (f32[3,128]{1,0:T(4,128)S(1)}, f32[3,128]{1,0:T(4,128)}, u32[]{:S(2)}) copy-start(f32[3,128]{1,0:T(4,128)} %param.22) | copy-start | bytes 4612
  3.5 22.6 %all-to-all-start = ((bf16[32,24,128]{2,1,0:T(8,128)(2,1)}), bf16[32,24,128]{2,1,0:T(8,128)(2,1)S(1)}, u32[]{:S(2)}, u32[]{:S(2)}) async-start(bf16[32,24,128]{2,1,0:T(8,128)(2,1)} %bitcast.17), calls=%async_computation | async-start | bytes 393216 | tf_op jit(solution)/shard_map/all_to_all | solution.py:334
  26.0 0.7 %copy-start.1 = (bf16[32,24,128]{2,1,0:T(8,128)(2,1)}, bf16[32,24,128]{2,1,0:T(8,128)(2,1)S(1)}, u32[]{:S(2)}) copy-start(bf16[32,24,128]{2,1,0:T(8,128)(2,1)S(1)} %all-to-all-done) | copy-start | bytes 589828

commit v2 on v1

v2 whole, which is shorter than its diff:
```python
import functools
import math

import jax
import jax.numpy as jnp
from jax import lax
from jax.experimental import pallas as pl
from jax.experimental.pallas import tpu as pltpu
from jax.sharding import PartitionSpec as P

CHANNELS = 1024
FREQ_BANDS = 16
NORM_EPS = 1e-06
DECAY_SLOW = math.log(0.01) / 1.5
DECAY_FAST = math.log(0.01) / 0.3

F32 = jnp.float32
BF16 = jnp.bfloat16

SIN_COEFFS = (
    6.283182818555376,
    -41.34142139902321,
    81.59618388026023,
    -76.58010058967308,
    41.20539511150987,
    -12.271262699024827,
)


def sin_turns(turns):
    r = turns - jnp.floor(turns + 0.5)
    s = r * r
    acc = jnp.full_like(s, SIN_COEFFS[-1])
    for coeff in SIN_COEFFS[-2::-1]:
        acc = acc * s + coeff
    return acc * r


def split(value):
    high = value.astype(BF16)
    low = (value - high.astype(F32)).astype(BF16)
    return high, low


def iota(shape, dim):
    return lax.broadcasted_iota(jnp.int32, shape, dim)


def to_turns(index, period):
    return (index & (period - 1)).astype(F32) * (1.0 / period)


def row_dft_table():
    shape = (128, 192)
    k1, n1 = iota(shape, 0) & 63, iota(shape, 1) & 63
    turns = to_turns((2 * k1 + 1) * n1, 256)
    value = sin_turns(turns + jnp.where(iota(shape, 0) < 64, 0.25, 0.5))
    high = value.astype(BF16).astype(F32)
    return jnp.where(iota(shape, 1) < 128, high, value - high).astype(BF16)


def row_inverse_table(scale):
    shape = (64, 384)
    n1, k1 = iota(shape, 0), iota(shape, 1) & 63
    turns = to_turns((2 * k1 + 1) * n1, 256)
    value = sin_turns(turns + jnp.where((iota(shape, 1) & 64) == 0, 0.25, 0.5)) * scale
    high = value.astype(BF16).astype(F32)
    return jnp.where(iota(shape, 1) < 256, high, value - high).astype(BF16)


def twiddles():
    shape = (64, 128)
    turns = to_turns((2 * iota(shape, 0) + 1) * iota(shape, 1), 32768)
    return sin_turns(turns + 0.25), sin_turns(turns)


def lane_dft():
    shape = (128, 128)
    turns = to_turns(iota(shape, 0) * iota(shape, 1), 128)
    return split(sin_turns(turns + 0.25)), split(sin_turns(turns))


def dot(left, right):
    return jnp.dot(left, right, preferred_element_type=F32)


def stack3(value):
    high, low = split(value)
    return jnp.concatenate([high, low, high], axis=0)


def lanes3(value):
    high, low = split(value)
    return jnp.concatenate([high, low, high], axis=1)


def project_kernel(tokens, gain, w0, w1, w2, out, scratch):
    wide = tokens[...].astype(F32)
    scale = lax.rsqrt(jnp.mean(wide * wide, axis=1, keepdims=True) + NORM_EPS)
    normed = (wide * scale * gain[...]).astype(BF16)
    weights = jnp.concatenate([w0[...], w1[...], w2[...]], axis=1)
    gates = dot(normed, weights)
    for half in range(2):
        for branch in range(3):
            block = gates[half * 128 : half * 128 + 128, branch * 128 : branch * 128 + 128].T
            for peer in range(32):
                start = peer * 24 + half * 12 + branch * 4
                scratch[start : start + 4, :] = block[peer * 4 : peer * 4 + 4, :]
    out[...] = scratch[...].astype(BF16).reshape(32, 24, 128)


def lane_table(sign, cos, sin):
    def part(c, s):
        top = jnp.concatenate([c, -s if sign > 0 else s], axis=1)
        bottom = jnp.concatenate([s if sign > 0 else -s, c], axis=1)
        return jnp.concatenate([top, bottom], axis=0)

    high, low = part(cos[0], sin[0]), part(cos[1], sin[1])
    return jnp.concatenate([high, high, low], axis=0)


def filter_kernel(
    ew, eb, iw, ib, freq, fw, sw, sb, skip,
    hre, him, frows, irows, flanes, ilanes, twiddle, scalars,
    build, lhs1, lhs2, taps,
):
    length = 8192
    own = lax.axis_index("row") * 4
    first_channel = lax.axis_index("col") * 128 + own

    lines = []
    for branch in range(3):
        lines.append(sb[branch : branch + 1, :])
        lines.append(sw[branch].astype(F32))
    lines.append(jnp.zeros((4, 128), F32))
    lines = pltpu.roll(jnp.concatenate(lines, axis=0), (128 - own) % 128, 1)
    for channel in range(4):
        scalars[channel * 16 : channel * 16 + 16, :] = jnp.broadcast_to(
            lines[:, channel : channel + 1], (16, 128)
        )
        scalars[channel * 16 + 12 : channel * 16 + 14, :] = jnp.broadcast_to(
            skip[:, channel : channel + 1], (2, 128)
        )

    frows[...] = row_dft_table()
    irows[...] = row_inverse_table(1.0 / 8192)
    tw_cos, tw_sin = twiddles()
    twiddle[0:64, :] = tw_cos
    twiddle[64:128, :] = tw_sin
    cos, sin = lane_dft()
    flanes[...] = lane_table(1, cos, sin)
    ilanes[...] = lane_table(-1, cos, sin)

    def high_of(value):
        return value.astype(BF16).astype(F32)

    turns_of = freq[...] * (1.0 / (2.0 * math.pi))
    build[...] = jnp.zeros_like(build)
    embed = ew[...] * turns_of
    bias = eb[...] * turns_of
    rows = jnp.concatenate([embed[1:33], embed[0:1], bias], axis=0)
    build[0:34, 0:64] = high_of(rows)
    build[48:82, 0:64] = high_of(rows)
    build[96:130, 0:64] = rows - high_of(rows)
    lhs1[...] = build[...].T[0:64, :].astype(BF16)
    inner = iw[...] * turns_of
    bias = ib[...] * turns_of
    build[...] = jnp.zeros_like(build)
    build[0:64, 0:64] = high_of(inner)
    build[64:128, 0:64] = high_of(inner)
    build[128:192, 0:64] = inner - high_of(inner)
    build[192:193, 0:64] = high_of(bias)
    build[193:194, 0:64] = bias - high_of(bias)
    lhs2[...] = build[...].T[0:64, :].astype(BF16)
    left1 = lhs1[:, 0:144]
    left2 = lhs2[:, 0:208]
    parts = []
    for order in range(2):
        parts.append(fw[order, 0] + fw[order, 1])
        parts.append(fw[order, 0] - fw[order, 1])
    fhigh, flow = split(jnp.concatenate(parts, axis=0))
    left3 = jnp.concatenate([fhigh, fhigh, flow], axis=1)

    band_step = (FREQ_BANDS - 1 - 0.0001) / (FREQ_BANDS - 1)
    band = 0.0001 + iota((16, 128), 0).astype(F32) * band_step
    lane = iota((16, 128), 1).astype(F32)
    coarse = band * (lane * (128.0 / length))
    fine = band * (lane * (1.0 / length))
    coarse_cos, coarse_sin = sin_turns(coarse + 0.25), sin_turns(coarse)
    fine_cos, fine_sin = sin_turns(fine + 0.25), sin_turns(fine)
    row = iota((16, 128), 0)
    extra = jnp.where(row == 0, lane * (1.0 / (length - 1)), jnp.where(row == 1, 1.0, 0.0))
    extra_step = jnp.where(row == 0, 128.0 / (length - 1), 0.0)

    rate_step = (DECAY_SLOW - DECAY_FAST) / (CHANNELS - 1)
    channel_row = (iota((8, 128), 0) & 3) + first_channel
    rate = -DECAY_SLOW + channel_row.astype(F32) * rate_step
    ramp = iota((8, 128), 1).astype(F32) * (1.0 / (length - 1))

    chunk = 1024
    blocks = chunk // 128
    ones16 = jnp.ones((16, chunk), BF16)
    for step in range(length // chunk):
        feature = []
        for block in range(blocks):
            n1 = step * blocks + block
            ca = jnp.broadcast_to(coarse_cos[:, n1 : n1 + 1], (16, 128))
            sa = jnp.broadcast_to(coarse_sin[:, n1 : n1 + 1], (16, 128))
            feature.append(
                jnp.concatenate(
                    [
                        ca * fine_cos - sa * fine_sin,
                        -(sa * fine_cos + ca * fine_sin),
                        extra + extra_step * float(n1),
                    ],
                    axis=0,
                )
            )
        hidden = sin_turns(dot(left1, stack3(jnp.concatenate(feature, axis=1))))
        hidden = sin_turns(dot(left2, jnp.concatenate([stack3(hidden), ones16], axis=0)))
        value = dot(left3, stack3(hidden))
        for block in range(blocks):
            n1 = step * blocks + block
            window = jnp.exp((ramp + n1 * 128.0 / (length - 1)) * -rate)
            piece = value[:, block * 128 : block * 128 + 128] * jnp.concatenate([window, window], axis=0)
            if n1 == 0:
                swapped = jnp.concatenate([piece[4:8], piece[0:4], piece[12:16], piece[8:12]], axis=0)
                piece = jnp.where(iota((16, 128), 1) == 0, 0.5 * (piece + swapped), piece)
            taps[n1 * 16 : n1 * 16 + 16, :] = piece

    spread = jnp.concatenate([taps[pl.ds(r, 64, stride=16), :] for r in range(16)], axis=1)
    stage = dot(frows[...], stack3(spread))
    (cos_high, cos_low), (sin_high, sin_low) = cos, sin
    real_table = jnp.concatenate([cos_high, sin_high, cos_high, sin_high, cos_low, sin_low], axis=0)
    imag_table = jnp.concatenate([-sin_high, cos_high, -sin_high, cos_high, -sin_low, cos_low], axis=0)
    for kind, table, out in ((0, real_table, hre), (1, imag_table, him)):
        reals, imags = [], []
        for order in range(2):
            for channel in range(4):
                at = (order * 8 + kind * 4 + channel) * 128
                real, imag = stage[0:64, at : at + 128], stage[64:128, at : at + 128]
                reals.append(real * tw_cos + imag * tw_sin)
                imags.append(imag * tw_cos - real * tw_sin)
        left = jnp.concatenate([jnp.concatenate(reals, axis=0), jnp.concatenate(imags, axis=0)], axis=1)
        out[...] = dot(lanes3(left), table)


def shifted(value, amount):
    size = 128
    lane, row = iota(value.shape, 1), iota(value.shape, 0)
    rolled = pltpu.roll(value, amount % size, 1)
    carried = pltpu.roll(rolled, amount % 64, 0)
    edge_lane = 0 if amount == 1 else size - 1
    edge_row = 0 if amount == 1 else 63
    carried = jnp.where(row == edge_row, 0.0, carried)
    return jnp.where(lane == edge_lane, carried, rolled)


def conv_kernel(
    moved, hre, him, frows, irows, flanes, ilanes, twiddle, scalars, weight, out, kept, wide, result, arrived
):
    fetch = pltpu.make_async_copy(weight, kept, arrived)
    fetch.start()
    wide[...] = moved[...].astype(F32).reshape(768, 128)
    smoothed = []
    for branch in range(3):
        rows = []
        for channel in range(4):
            value = wide[pl.ds(branch * 4 + channel, 64, stride=12), :]
            base = channel * 16 + branch * 4
            total = scalars[base : base + 1, :] + shifted(value, 1) * scalars[base + 1 : base + 2, :]
            total = total + value * scalars[base + 2 : base + 3, :]
            total = total + shifted(value, -1) * scalars[base + 3 : base + 4, :]
            rows.append(total)
        smoothed.append(rows)
    forward_rows, inverse_rows = frows[...], irows[...]
    forward_lanes, inverse_lanes = flanes[...], ilanes[...]
    tw_cos, tw_sin = twiddle[0:64, :], twiddle[64:128, :]
    signal = smoothed[2]
    for order in range(2):
        stage = dot(forward_rows, stack3(jnp.concatenate(signal, axis=1)))
        reals, imags = [], []
        for channel in range(4):
            real = stage[0:64, channel * 128 : channel * 128 + 128]
            imag = stage[64:128, channel * 128 : channel * 128 + 128]
            reals.append(real * tw_cos + imag * tw_sin)
            imags.append(imag * tw_cos - real * tw_sin)
        left = jnp.concatenate([jnp.concatenate(reals, axis=0), jnp.concatenate(imags, axis=0)], axis=1)
        spectrum = dot(lanes3(left), forward_lanes)
        real, imag = spectrum[:, 0:128], spectrum[:, 128:256]
        tap_real = hre[order * 256 : order * 256 + 256, :]
        tap_imag = him[order * 256 : order * 256 + 256, :]
        left = jnp.concatenate(
            [real * tap_real - imag * tap_imag, real * tap_imag + imag * tap_real], axis=1
        )
        back = dot(lanes3(left), inverse_lanes)
        columns = []
        for channel in range(4):
            real = back[channel * 64 : channel * 64 + 64, 0:128]
            imag = back[channel * 64 : channel * 64 + 64, 128:256]
            columns.append(
                jnp.concatenate([real * tw_cos - imag * tw_sin, real * tw_sin + imag * tw_cos], axis=0)
            )
        values = dot(inverse_rows, stack3(jnp.concatenate(columns, axis=1)))
        following = []
        for channel in range(4):
            at = channel * 16 + 12 + order
            skip = scalars[at : at + 1, :]
            conv = values[:, channel * 128 : channel * 128 + 128] + signal[channel] * skip
            following.append(smoothed[order][channel] * conv)
        signal = following
    for channel in range(4):
        result[pl.ds(channel, 64, stride=4), :] = signal[channel]
    out[...] = result[...].astype(BF16).reshape(32, 8, 128)
    fetch.wait()


def norm_kernel(moved, gain, out, wide, ordered):
    wide[...] = moved[...].astype(F32).reshape(256, 128)
    for half in range(2):
        for channel in range(4):
            ordered[pl.ds(half * 128 + channel, 32, stride=4), :] = wide[
                pl.ds(half * 4 + channel, 32, stride=8), :
            ]
    for half in range(2):
        value = ordered[half * 128 : half * 128 + 128, :]
        scale = lax.rsqrt(jnp.mean(value * value, axis=0, keepdims=True) + NORM_EPS)
        normed = ((value * scale).T * gain[...]).astype(BF16)
        out[half * 4 : half * 4 + 4] = normed.reshape(4, 32, 128)


def output_kernel(mixed, weight, out):
    left = jnp.concatenate([mixed[c] for c in range(8)], axis=1)
    out[...] = dot(left, weight[...]).astype(BF16)


VMEM = pl.BlockSpec(memory_space=pltpu.VMEM)
HBM = pl.BlockSpec(memory_space=pltpu.HBM)


def run(kernel, out_shape, inputs, scratch, name, unread=0):
    multi = isinstance(out_shape, (tuple, list))
    return pl.pallas_call(
        kernel,
        out_shape=out_shape,
        in_specs=[VMEM] * (len(inputs) - unread) + [HBM] * unread,
        out_specs=tuple(VMEM for _ in out_shape) if multi else VMEM,
        scratch_shapes=scratch,
        name=name,
        compiler_params=pltpu.CompilerParams(vmem_limit_bytes=24 * 1024 * 1024),
    )(*inputs)


def near(value):
    return pltpu.with_memory_space_constraint(value, pltpu.VMEM)


def far(*values):
    return tuple(pltpu.with_memory_space_constraint(value, pltpu.HBM) for value in values)


def local(
    tokens,
    norm_gain,
    first_gate,
    second_gate,
    value_weight,
    short_weight,
    short_bias,
    embed_weight,
    embed_bias,
    inner_weight,
    inner_bias,
    filter_freq,
    filter_weight,
    filter_skip,
    output_gain,
    output_weight,
):
    sent = run(
        project_kernel,
        pltpu.VMEM((32, 24, 128), BF16),
        far(tokens, norm_gain.reshape(1, -1), first_gate, second_gate, value_weight),
        [pltpu.VMEM((768, 128), F32)],
        "project",
    )
    moved = lax.all_to_all(sent, "row", split_axis=0, concat_axis=0, tiled=True)
    prepared = run(
        filter_kernel,
        (
            pltpu.VMEM((512, 128), F32),
            pltpu.VMEM((512, 128), F32),
            pltpu.VMEM((128, 192), BF16),
            pltpu.VMEM((64, 384), BF16),
            pltpu.VMEM((768, 256), BF16),
            pltpu.VMEM((768, 256), BF16),
            pltpu.VMEM((128, 128), F32),
            pltpu.VMEM((64, 128), F32),
        ),
        far(
            embed_weight,
            embed_bias.reshape(1, -1),
            inner_weight,
            inner_bias.reshape(1, -1),
            filter_freq.reshape(1, -1),
            filter_weight.transpose(0, 1, 3, 2),
            short_weight,
            short_bias,
            filter_skip,
        ),
        [
            pltpu.VMEM((256, 128), F32),
            pltpu.VMEM((64, 256), BF16),
            pltpu.VMEM((64, 256), BF16),
            pltpu.VMEM((1024, 128), F32),
        ],
        "filters",
    )
    mixed, kept = run(
        conv_kernel,
        (pltpu.VMEM((32, 8, 128), BF16), pltpu.VMEM((1024, 2048), BF16)),
        (*(near(value) for value in (moved, *prepared)), *far(output_weight)),
        [pltpu.VMEM((768, 128), F32), pltpu.VMEM((256, 128), F32), pltpu.SemaphoreType.DMA],
        "convolve",
        1,
    )
    result = lax.all_to_all(mixed, "row", split_axis=0, concat_axis=0, tiled=True)
    normed = run(
        norm_kernel,
        pltpu.VMEM((8, 32, 128), BF16),
        (near(result), *far(output_gain.reshape(1, -1))),
        [pltpu.VMEM((256, 128), F32), pltpu.VMEM((256, 128), F32)],
        "groupnorm",
    )
    gathered = lax.all_to_all(normed, "col", split_axis=0, concat_axis=0, tiled=True)
    return run(
        output_kernel,
        jax.ShapeDtypeStruct((32, 2048), BF16),
        (near(gathered), near(kept)),
        [],
        "output",
    )


def solution(mesh):
    in_specs = (
        P("row", None),
        P(),
        P(None, "col"),
        P(None, "col"),
        P(None, "col"),
        P(None, None, "col"),
        P(None, "col"),
        P(),
        P(),
        P(),
        P(),
        P(),
        P(None, None, None, ("col", "row")),
        P(None, ("col", "row")),
        P("col"),
        P(),
    )
    out_specs = P(("row", "col"), None)
    return jax.shard_map(local, mesh=mesh, in_specs=in_specs, out_specs=out_specs, check_vma=False)
```

time: 66.5 us -> 56.4 us (0.85)
  Pallas kernels: 20.4 us -> 14.7 us
  blocking collectives: 30 us -> 25.5 us
  waiting for transfers between devices: 0.08 us -> 4 us
  other arithmetic: 1.85 us -> 0 us
  local copies, waits for them, and re-layouts: 1.71 us -> 0 us
    pallas_call x5, Pallas kernels: 20.4 us -> 14.7 us  [run(): pl.pallas_call(kernel, out_shape=out_shape, in_specs=[VMEM] * (len(inputs...]
    all_to_all x2, blocking collectives: 30 us -> 25.5 us  [the longest x1 13.7 us: local(): lax.all_to_all(mixed, 'row', split_axis=0, concat_axis=0, tiled=True)]
    all_to_all x1, waiting for transfers between devices: 0.08 us -> 4 us  [local(): moved = lax.all_to_all(sent, 'row', split_axis=0, concat_axis=0, tiled=True)]
    reshape x2 -> x0, local copies, waits for them, and re-layouts: 0.85 us -> none  [the longest x1 0.76 us: local(): filter_skip.reshape(-1)]
    convert_element_type x1 -> x0, other arithmetic: 0.76 us -> none  [local(): lax.dynamic_slice_in_dim(short_weight, row_index * 4, 4, 2).astype(F32)]
    unnamed x4 -> x0, local copies, waits for them, and re-layouts: 0.68 us -> none
  transfers between devices with their start and end apart: 1 -> 1, of which waited for: 1 -> 1; matrix products, arithmetic and copies ran while one was open for 4% -> 0% of each run, Pallas kernels for 12% -> 12%
where the time goes in v2:
time: 56.4 us; the launch traced here: 56 us
  blocking collectives  25.5 us (45%)
  Pallas kernels  14.7 us (26%)
  starting transfers between devices  11.9 us (21%)
  waiting for transfers between devices  4 us (7%)
    pallas_call x5, Pallas kernels, run(): pl.pallas_call(kernel, out_shape=out_shape, in_specs=[VMEM] * (len(inputs...  14.7 us
    all_to_all x1, blocking collectives, local(): lax.all_to_all(mixed, 'row', split_axis=0, concat_axis=0, tiled=True)  13.7 us
    all_to_all x1, starting transfers between devices, local(): moved = lax.all_to_all(sent, 'row', split_axis=0, concat_axis=0, tiled=True)  11.9 us
    all_to_all x1, blocking collectives, local(): lax.all_to_all(normed, 'col', split_axis=0, concat_axis=0, tiled=True)  11.8 us
    all_to_all x1, waiting for transfers between devices, local(): moved = lax.all_to_all(sent, 'row', split_axis=0, concat_axis=0, tiled=True)  4 us
  transfers between devices with their start and end apart: 1, of which 1 were waited for; matrix products, arithmetic and copies ran while one was open for 0% of the time, Pallas kernels for 12%

profile of v2, /device:TPU:1, one launch (start us, length us, event | category | flops | bytes accessed | tf_op | source)
XLA Modules:
  0.0 56.0 jit_solution(9330148140147469448)
XLA Ops:
  0.0 3.4 %project.1 = bf16[32,24,128]{2,1,0:T(8,128)(2,1)} custom-call(bf16[256,2048]{1,0:T(8,128)(2,1)} %tokens.1, f32[1,2048]{1,0:T(1,128)} %bitcast.6, bf16[2048,128]{1,0:T(8,128)(2,1)} %w0.1, bf16[2048,128]{1,0:T(8,128)(2,1)} %w1.1, bf16[2048,128]{1,0:T(8,128)(2,1)} %w2.1), custom_call_target="tpu_custom_call" | custom-call | tf_op jit(solution)/shard_map/project/pallas_call | solution.py:343
  3.4 11.9 %all-to-all-start = ((bf16[32,24,128]{2,1,0:T(8,128)(2,1)}), bf16[32,24,128]{2,1,0:T(8,128)(2,1)S(1)}, u32[]{:S(2)}, u32[]{:S(2)}) async-start(bf16[32,24,128]{2,1,0:T(8,128)(2,1)} %project.1), calls=%async_computation | async-start | bytes 393216 | tf_op jit(solution)/shard_map/all_to_all | solution.py:387
  15.3 6.7 %filters.1 = (f32[512,128]{1,0:T(8,128)S(1)}, f32[512,128]{1,0:T(8,128)S(1)}, bf16[128,192]{1,0:T(8,128)(2,1)S(1)}, bf16[64,384]{1,0:T(8,128)(2,1)S(1)}, bf16[76...) custom-call(f32[33,64]{1,0:T(8,128)} %ew.1, ...), custom_call_target="tpu_custom_call" | custom-call | tf_op jit(solution)/shard_map/filters/pallas_call | solution.py:343
  22.0 4.0 %all-to-all-done.moved = bf16[32,24,128]{2,1,0:T(8,128)(2,1)S(1)} async-done(((bf16[32,24,128]{2,1,0:T(8,128)(2,1)}), bf16[32,24,128]{2,1,0:T(8,128)(2,1)S(1)}, u32[]{:S(2)}, u32[]{:S(2)}) %all-to-all-start) | async-done | bytes 196640 | tf_op jit(solution)/shard_map/all_to_all | solution.py:387
  26.0 2.2 %convolve.1 = (bf16[32,8,128]{2,1,0:T(8,128)(2,1)S(1)}, bf16[1024,2048]{1,0:T(8,128)(2,1)S(1)}) custom-call(bf16[32,24,128]{2,1,0:T(8,128)(2,1)S(1)} %all-to-all-done.moved, f32[512,128]{1,0:T(8,128)S(1)} %get-tuple-element.15.hre, f32[512,128]{1,0:T(8,128)S(1)} %get-tuple-element.16.him, bf16[128,192]{1,0:T(8,128)(2,1)S(1)} %get-tuple-element.17.frows, ...), custom_call_target="tpu_custom_call" | custom-call | tf_op jit(solution)/shard_map/convolve/pallas_call | solution.py:343
  28.2 13.7 %all_to_all.15.moved = bf16[32,8,128]{2,1,0:T(8,128)(2,1)S(1)} all-to-all(bf16[32,8,128]{2,1,0:T(8,128)(2,1)S(1)} %get-tuple-element.23), channel_id=1, replica_groups=mesh['row'=32,'col'=8] {'row'}, dimensions={0} | all-to-all | bytes 131072 | tf_op jit(solution)/shard_map/all_to_all | solution.py:427
  41.9 0.8 %groupnorm.1 = bf16[8,32,128]{2,1,0:T(8,128)(2,1)S(1)} custom-call(bf16[32,8,128]{2,1,0:T(8,128)(2,1)S(1)} %all_to_all.15.moved, f32[1,128]{1,0:T(1,128)} %bitcast.11), custom_call_target="tpu_custom_call" | custom-call | tf_op jit(solution)/shard_map/groupnorm/pallas_call | solution.py:343
  42.8 11.8 %all_to_all.16.mixed = bf16[8,32,128]{2,1,0:T(8,128)(2,1)S(1)} all-to-all(bf16[8,32,128]{2,1,0:T(8,128)(2,1)S(1)} %groupnorm.1), channel_id=1, replica_groups=mesh['row'=32,'col'=8] {'col'}, dimensions={0} | all-to-all | bytes 131072 | tf_op jit(solution)/shard_map/all_to_all | solution.py:435
  54.5 1.5 %output.1 = bf16[32,2048]{1,0:T(8,128)(2,1)} custom-call(bf16[8,32,128]{2,1,0:T(8,128)(2,1)S(1)} %all_to_all.16.mixed, bf16[1024,2048]{1,0:T(8,128)(2,1)S(1)} %get-tuple-element.24.weight), custom_call_target="tpu_custom_call" | custom-call | tf_op jit(solution)/shard_map/output/pallas_call | solution.py:343
Async XLA Ops:
  3.4 22.6 %all-to-all-start = ((bf16[32,24,128]{2,1,0:T(8,128)(2,1)}), bf16[32,24,128]{2,1,0:T(8,128)(2,1)S(1)}, u32[]{:S(2)}, u32[]{:S(2)}) async-start(bf16[32,24,128]{2,1,0:T(8,128)(2,1)} %project.1), calls=%async_computation | async-start | bytes 393216 | tf_op jit(solution)/shard_map/all_to_all | solution.py:387

commit v3 on v2

--- a/solution.py
+++ b/solution.py
@@ -94,19 +94,45 @@
     return jnp.concatenate([high, low, high], axis=1)
 
 
-def project_kernel(tokens, gain, w0, w1, w2, out, scratch):
-    wide = tokens[...].astype(F32)
-    scale = lax.rsqrt(jnp.mean(wide * wide, axis=1, keepdims=True) + NORM_EPS)
-    normed = (wide * scale * gain[...]).astype(BF16)
-    weights = jnp.concatenate([w0[...], w1[...], w2[...]], axis=1)
-    gates = dot(normed, weights)
+def project_kernel(*refs):
+    count = len(refs) - 15
+    tokens, gain, w0, w1, w2 = refs[0:5]
+    small = refs[5 : 5 + count // 2]
+    out = refs[5 + count // 2]
+    carried = refs[6 + count // 2 : 6 + count]
+    near_tokens, near_gain, n0, n1, n2, normed, scratch, arrived, carry = refs[6 + count :]
+    rows = 64
+    copies = [pltpu.make_async_copy(gain, near_gain, arrived.at[0])]
+    for part in range(4):
+        where = pl.ds(part * rows, rows)
+        copies.append(pltpu.make_async_copy(tokens.at[where], near_tokens.at[where], arrived.at[part + 1]))
+    for index, (source, target) in enumerate(((w0, n0), (w1, n1), (w2, n2))):
+        copies.append(pltpu.make_async_copy(source, target, arrived.at[index + 5]))
+    carries = [
+        pltpu.make_async_copy(source, target, carry.at[index])
+        for index, (source, target) in enumerate(zip(small, carried))
+    ]
+    for copy in copies + carries:
+        copy.start()
+    copies[0].wait()
+    for part in range(4):
+        copies[part + 1].wait()
+        wide = near_tokens[part * rows : part * rows + rows, :].astype(F32)
+        scale = lax.rsqrt(jnp.mean(wide * wide, axis=1, keepdims=True) + NORM_EPS)
+        normed[part * rows : part * rows + rows, :] = (wide * scale * near_gain[...]).astype(BF16)
+    for copy in copies[5:]:
+        copy.wait()
+    weights = jnp.concatenate([n0[...], n1[...], n2[...]], axis=1)
     for half in range(2):
+        gates = dot(normed[half * 128 : half * 128 + 128, :], weights)
         for branch in range(3):
-            block = gates[half * 128 : half * 128 + 128, branch * 128 : branch * 128 + 128].T
+            block = gates[:, branch * 128 : branch * 128 + 128].T
             for peer in range(32):
                 start = peer * 24 + half * 12 + branch * 4
                 scratch[start : start + 4, :] = block[peer * 4 : peer * 4 + 4, :]
     out[...] = scratch[...].astype(BF16).reshape(32, 24, 128)
+    for copy in carries:
+        copy.wait()
 
 
 def lane_table(sign, cos, sin):
@@ -179,7 +205,7 @@
         parts.append(fw[order, 0] + fw[order, 1])
         parts.append(fw[order, 0] - fw[order, 1])
     fhigh, flow = split(jnp.concatenate(parts, axis=0))
-    left3 = jnp.concatenate([fhigh, fhigh, flow], axis=1)
+    left3 = jnp.concatenate([fhigh, flow], axis=1)
 
     band_step = (FREQ_BANDS - 1 - 0.0001) / (FREQ_BANDS - 1)
     band = 0.0001 + iota((16, 128), 0).astype(F32) * band_step
@@ -218,7 +244,8 @@
             )
         hidden = sin_turns(dot(left1, stack3(jnp.concatenate(feature, axis=1))))
         hidden = sin_turns(dot(left2, jnp.concatenate([stack3(hidden), ones16], axis=0)))
-        value = dot(left3, stack3(hidden))
+        high = hidden.astype(BF16)
+        value = dot(left3, jnp.concatenate([high, high], axis=0))
         for block in range(blocks):
             n1 = step * blocks + block
             window = jnp.exp((ramp + n1 * 128.0 / (length - 1)) * -rate)
@@ -231,8 +258,8 @@
     spread = jnp.concatenate([taps[pl.ds(r, 64, stride=16), :] for r in range(16)], axis=1)
     stage = dot(frows[...], stack3(spread))
     (cos_high, cos_low), (sin_high, sin_low) = cos, sin
-    real_table = jnp.concatenate([cos_high, sin_high, cos_high, sin_high, cos_low, sin_low], axis=0)
-    imag_table = jnp.concatenate([-sin_high, cos_high, -sin_high, cos_high, -sin_low, cos_low], axis=0)
+    real_table = jnp.concatenate([cos_high, sin_high, cos_low, sin_low], axis=0)
+    imag_table = jnp.concatenate([-sin_high, cos_high, -sin_low, cos_low], axis=0)
     for kind, table, out in ((0, real_table, hre), (1, imag_table, him)):
         reals, imags = [], []
         for order in range(2):
@@ -242,7 +269,8 @@
                 reals.append(real * tw_cos + imag * tw_sin)
                 imags.append(imag * tw_cos - real * tw_sin)
         left = jnp.concatenate([jnp.concatenate(reals, axis=0), jnp.concatenate(imags, axis=0)], axis=1)
-        out[...] = dot(lanes3(left), table)
+        left = left.astype(BF16)
+        out[...] = dot(jnp.concatenate([left, left], axis=1), table)
 
 
 def shifted(value, amount):
@@ -278,36 +306,36 @@
     tw_cos, tw_sin = twiddle[0:64, :], twiddle[64:128, :]
     signal = smoothed[2]
     for order in range(2):
-        stage = dot(forward_rows, stack3(jnp.concatenate(signal, axis=1)))
-        reals, imags = [], []
-        for channel in range(4):
-            real = stage[0:64, channel * 128 : channel * 128 + 128]
-            imag = stage[64:128, channel * 128 : channel * 128 + 128]
-            reals.append(real * tw_cos + imag * tw_sin)
-            imags.append(imag * tw_cos - real * tw_sin)
-        left = jnp.concatenate([jnp.concatenate(reals, axis=0), jnp.concatenate(imags, axis=0)], axis=1)
-        spectrum = dot(lanes3(left), forward_lanes)
-        real, imag = spectrum[:, 0:128], spectrum[:, 128:256]
-        tap_real = hre[order * 256 : order * 256 + 256, :]
-        tap_imag = him[order * 256 : order * 256 + 256, :]
-        left = jnp.concatenate(
-            [real * tap_real - imag * tap_imag, real * tap_imag + imag * tap_real], axis=1
-        )
-        back = dot(lanes3(left), inverse_lanes)
-        columns = []
-        for channel in range(4):
-            real = back[channel * 64 : channel * 64 + 64, 0:128]
-            imag = back[channel * 64 : channel * 64 + 64, 128:256]
-            columns.append(
-                jnp.concatenate([real * tw_cos - imag * tw_sin, real * tw_sin + imag * tw_cos], axis=0)
+        following = []
+        for pair in ((0, 1), (2, 3)):
+            stage = dot(forward_rows, stack3(jnp.concatenate([signal[c] for c in pair], axis=1)))
+            reals, imags = [], []
+            for place in range(2):
+                real = stage[0:64, place * 128 : place * 128 + 128]
+                imag = stage[64:128, place * 128 : place * 128 + 128]
+                reals.append(real * tw_cos + imag * tw_sin)
+                imags.append(imag * tw_cos - real * tw_sin)
+            left = jnp.concatenate([jnp.concatenate(reals, axis=0), jnp.concatenate(imags, axis=0)], axis=1)
+            spectrum = dot(lanes3(left), forward_lanes)
+            real, imag = spectrum[:, 0:128], spectrum[:, 128:256]
+            at = order * 256 + pair[0] * 64
+            tap_real, tap_imag = hre[at : at + 128, :], him[at : at + 128, :]
+            left = jnp.concatenate(
+                [real * tap_real - imag * tap_imag, real * tap_imag + imag * tap_real], axis=1
             )
-        values = dot(inverse_rows, stack3(jnp.concatenate(columns, axis=1)))
-        following = []
-        for channel in range(4):
-            at = channel * 16 + 12 + order
-            skip = scalars[at : at + 1, :]
-            conv = values[:, channel * 128 : channel * 128 + 128] + signal[channel] * skip
-            following.append(smoothed[order][channel] * conv)
+            back = dot(lanes3(left), inverse_lanes)
+            columns = []
+            for place in range(2):
+                real = back[place * 64 : place * 64 + 64, 0:128]
+                imag = back[place * 64 : place * 64 + 64, 128:256]
+                columns.append(
+                    jnp.concatenate([real * tw_cos - imag * tw_sin, real * tw_sin + imag * tw_cos], axis=0)
+                )
+            values = dot(inverse_rows, stack3(jnp.concatenate(columns, axis=1)))
+            for place, channel in enumerate(pair):
+                at = channel * 16 + 12 + order
+                conv = values[:, place * 128 : place * 128 + 128] + signal[channel] * scalars[at : at + 1, :]
+                following.append(smoothed[order][channel] * conv)
         signal = following
     for channel in range(4):
         result[pl.ds(channel, 64, stride=4), :] = signal[channel]
@@ -377,12 +405,35 @@
     output_gain,
     output_weight,
 ):
-    sent = run(
+    small = (
+        embed_weight,
+        embed_bias.reshape(1, -1),
+        inner_weight,
+        inner_bias.reshape(1, -1),
+        filter_freq.reshape(1, -1),
+        filter_weight.transpose(0, 1, 3, 2),
+        short_weight,
+        short_bias,
+        filter_skip,
+        output_gain.reshape(1, -1),
+    )
+    sent, *small = run(
         project_kernel,
-        pltpu.VMEM((32, 24, 128), BF16),
-        far(tokens, norm_gain.reshape(1, -1), first_gate, second_gate, value_weight),
-        [pltpu.VMEM((768, 128), F32)],
+        (pltpu.VMEM((32, 24, 128), BF16), *(pltpu.VMEM(value.shape, value.dtype) for value in small)),
+        far(tokens, norm_gain.reshape(1, -1), first_gate, second_gate, value_weight, *small),
+        [
+            pltpu.VMEM((256, 2048), BF16),
+            pltpu.VMEM((1, 2048), F32),
+            pltpu.VMEM((2048, 128), BF16),
+            pltpu.VMEM((2048, 128), BF16),
+            pltpu.VMEM((2048, 128), BF16),
+            pltpu.VMEM((256, 2048), BF16),
+            pltpu.VMEM((768, 128), F32),
+            pltpu.SemaphoreType.DMA((8,)),
+            pltpu.SemaphoreType.DMA((len(small),)),
+        ],
         "project",
+        5 + len(small),
     )
     moved = lax.all_to_all(sent, "row", split_axis=0, concat_axis=0, tiled=True)
     prepared = run(
@@ -397,17 +448,7 @@
             pltpu.VMEM((128, 128), F32),
             pltpu.VMEM((64, 128), F32),
         ),
-        far(
-            embed_weight,
-            embed_bias.reshape(1, -1),
-            inner_weight,
-            inner_bias.reshape(1, -1),
-            filter_freq.reshape(1, -1),
-            filter_weight.transpose(0, 1, 3, 2),
-            short_weight,
-            short_bias,
-            filter_skip,
-        ),
+        tuple(near(value) for value in small[:9]),
         [
             pltpu.VMEM((256, 128), F32),
             pltpu.VMEM((64, 256), BF16),
@@ -428,7 +469,7 @@
     normed = run(
         norm_kernel,
         pltpu.VMEM((8, 32, 128), BF16),
-        (near(result), *far(output_gain.reshape(1, -1))),
+        (near(result), near(small[9])),
         [pltpu.VMEM((256, 128), F32), pltpu.VMEM((256, 128), F32)],
         "groupnorm",
     )

time: 56.4 us -> 54.7 us (0.970)
  Pallas kernels: 14.7 us -> 13.1 us
  waiting for transfers between devices: 4 us -> 5.02 us
  blocking collectives: 25.5 us -> 24.5 us
    pallas_call x5, Pallas kernels: 14.7 us -> 13.1 us  [run(): pl.pallas_call(kernel, out_shape=out_shape, in_specs=[VMEM] * (len(inputs...]
    all_to_all x1, blocking collectives: 13.7 us -> 12.7 us  [local(): lax.all_to_all(mixed, 'row', split_axis=0, concat_axis=0, tiled=True)]
    all_to_all x1, waiting for transfers between devices: 4 us -> 5.02 us  [local(): moved = lax.all_to_all(sent, 'row', split_axis=0, concat_axis=0, tiled=True)]
  transfers between devices with their start and end apart: 1 -> 1, of which waited for: 1 -> 1; matrix products, arithmetic and copies ran while one was open for 0% -> 0% of each run, Pallas kernels for 12% -> 10%
where the time goes in v3:
time: 54.7 us; the launch traced here: 54.5 us
  blocking collectives  24.5 us (45%)
  Pallas kernels  13.1 us (24%)
  starting transfers between devices  11.9 us (22%)
  waiting for transfers between devices  5.02 us (9%)
    pallas_call x5, Pallas kernels, run(): pl.pallas_call(kernel, out_shape=out_shape, in_specs=[VMEM] * (len(inputs...  13.1 us
    all_to_all x1, blocking collectives, local(): lax.all_to_all(mixed, 'row', split_axis=0, concat_axis=0, tiled=True)  12.7 us
    all_to_all x1, starting transfers between devices, local(): moved = lax.all_to_all(sent, 'row', split_axis=0, concat_axis=0, tiled=True)  11.9 us
    all_to_all x1, blocking collectives, local(): lax.all_to_all(normed, 'col', split_axis=0, concat_axis=0, tiled=True)  11.8 us
    all_to_all x1, waiting for transfers between devices, local(): moved = lax.all_to_all(sent, 'row', split_axis=0, concat_axis=0, tiled=True)  5.02 us
  transfers between devices with their start and end apart: 1, of which 1 were waited for; matrix products, arithmetic and copies ran while one was open for 0% of the time, Pallas kernels for 10%

profile of v3, /device:TPU:1, one launch (start us, length us, event | category | flops | bytes accessed | tf_op | source)
XLA Modules:
  0.0 54.5 jit_solution(10548743981026649142)
XLA Ops:
  0.0 3.5 %project.1 = (bf16[32,24,128]{2,1,0:T(8,128)(2,1)}, f32[33,64]{1,0:T(8,128)S(1)}, f32[1,64]{1,0:T(1,128)S(1)}, f32[64,64]{1,0:T(8,128)S(1)}, f32[1,64]{1,0:T(1,1...) custom-call(bf16[256,2048]{1,0:T(8,128)(2,1)} %refs_0_.1, ...), custom_call_target="tpu_custom_call" | custom-call | tf_op jit(solution)/shard_map/project/pallas_call | solution.py:371
  3.5 11.9 %all-to-all-start = ((bf16[32,24,128]{2,1,0:T(8,128)(2,1)}), bf16[32,24,128]{2,1,0:T(8,128)(2,1)S(1)}, u32[]{:S(2)}, u32[]{:S(2)}) async-start(bf16[32,24,128]{2,1,0:T(8,128)(2,1)} %get-tuple-element.26), calls=%async_computation | async-start | bytes 393216 | tf_op jit(solution)/shard_map/all_to_all | solution.py:438
  15.3 5.7 %filters.1 = (f32[512,128]{1,0:T(8,128)S(1)}, f32[512,128]{1,0:T(8,128)S(1)}, bf16[128,192]{1,0:T(8,128)(2,1)S(1)}, bf16[64,384]{1,0:T(8,128)(2,1)S(1)}, bf16[76...) custom-call(f32[33,64]{1,0:T(8,128)S(1)} %get-tuple-element.27.ew, ...), custom_call_target="tpu_custom_call" | custom-call | tf_op jit(solution)/shard_map/filters/pallas_call | solution.py:371
  21.0 5.0 %all-to-all-done.moved = bf16[32,24,128]{2,1,0:T(8,128)(2,1)S(1)} async-done(((bf16[32,24,128]{2,1,0:T(8,128)(2,1)}), bf16[32,24,128]{2,1,0:T(8,128)(2,1)S(1)}, u32[]{:S(2)}, u32[]{:S(2)}) %all-to-all-start) | async-done | bytes 196640 | tf_op jit(solution)/shard_map/all_to_all | solution.py:438
  26.1 2.3 %convolve.1 = (bf16[32,8,128]{2,1,0:T(8,128)(2,1)S(1)}, bf16[1024,2048]{1,0:T(8,128)(2,1)S(1)}) custom-call(bf16[32,24,128]{2,1,0:T(8,128)(2,1)S(1)} %all-to-all-done.moved, f32[512,128]{1,0:T(8,128)S(1)} %get-tuple-element.36.hre, f32[512,128]{1,0:T(8,128)S(1)} %get-tuple-element.37.him, bf16[128,192]{1,0:T(8,128)(2,1)S(1)} %get-tuple-element.38.frows, ...), custom_call_target="tpu_custom_call" | custom-call | tf_op jit(solution)/shard_map/convolve/pallas_call | solution.py:371
  28.3 12.7 %all_to_all.15.moved = bf16[32,8,128]{2,1,0:T(8,128)(2,1)S(1)} all-to-all(bf16[32,8,128]{2,1,0:T(8,128)(2,1)S(1)} %get-tuple-element.44), channel_id=1, replica_groups=mesh['row'=32,'col'=8] {'row'}, dimensions={0} | all-to-all | bytes 131072 | tf_op jit(solution)/shard_map/all_to_all | solution.py:468
  41.0 0.2 groupnorm.1
  41.2 11.8 %all_to_all.16.mixed = bf16[8,32,128]{2,1,0:T(8,128)(2,1)S(1)} all-to-all(bf16[8,32,128]{2,1,0:T(8,128)(2,1)S(1)} %groupnorm.1), channel_id=1, replica_groups=mesh['row'=32,'col'=8] {'col'}, dimensions={0} | all-to-all | bytes 131072 | tf_op jit(solution)/shard_map/all_to_all | solution.py:476
  53.0 1.5 %output.1 = bf16[32,2048]{1,0:T(8,128)(2,1)} custom-call(bf16[8,32,128]{2,1,0:T(8,128)(2,1)S(1)} %all_to_all.16.mixed, bf16[1024,2048]{1,0:T(8,128)(2,1)S(1)} %get-tuple-element.46.weight), custom_call_target="tpu_custom_call" | custom-call | tf_op jit(solution)/shard_map/output/pallas_call | solution.py:371
Async XLA Ops:
  3.5 22.6 %all-to-all-start = ((bf16[32,24,128]{2,1,0:T(8,128)(2,1)}), bf16[32,24,128]{2,1,0:T(8,128)(2,1)S(1)}, u32[]{:S(2)}, u32[]{:S(2)}) async-start(bf16[32,24,128]{2,1,0:T(8,128)(2,1)} %get-tuple-element.26), calls=%async_computation | async-start | bytes 393216 | tf_op jit(solution)/shard_map/all_to_all | solution.py:438

commit v4 on v3

--- a/solution.py
+++ b/solution.py
@@ -10,6 +10,7 @@
 
 CHANNELS = 1024
 FREQ_BANDS = 16
+EARLY = 384
 NORM_EPS = 1e-06
 DECAY_SLOW = math.log(0.01) / 1.5
 DECAY_FAST = math.log(0.01) / 0.3
@@ -17,23 +18,27 @@
 F32 = jnp.float32
 BF16 = jnp.bfloat16
 
-SIN_COEFFS = (
-    6.283182818555376,
-    -41.34142139902321,
-    81.59618388026023,
-    -76.58010058967308,
-    41.20539511150987,
-    -12.271262699024827,
+LONG_COEFFS = (
+    6.283185160089469,
+    -41.34165503141532,
+    81.60100407320796,
+    -76.54978229245017,
+    39.5367060575916,
 )
-
-
-def sin_turns(turns):
-    r = turns - jnp.floor(turns + 0.5)
+SHORT_COEFFS = (6.283164044302229, -41.33714237106961, 81.3407688866883, -70.99343326314641)
+
+
+def cos_turns(turns, coeffs=LONG_COEFFS):
+    r = 0.25 - jnp.abs(turns - jnp.round(turns))
     s = r * r
-    acc = jnp.full_like(s, SIN_COEFFS[-1])
-    for coeff in SIN_COEFFS[-2::-1]:
+    acc = s * coeffs[-1] + coeffs[-2]
+    for coeff in coeffs[-3::-1]:
         acc = acc * s + coeff
     return acc * r
+
+
+def sin_turns(turns):
+    return cos_turns(turns - 0.25)
 
 
 def split(value):
@@ -54,7 +59,7 @@
     shape = (128, 192)
     k1, n1 = iota(shape, 0) & 63, iota(shape, 1) & 63
     turns = to_turns((2 * k1 + 1) * n1, 256)
-    value = sin_turns(turns + jnp.where(iota(shape, 0) < 64, 0.25, 0.5))
+    value = cos_turns(turns + jnp.where(iota(shape, 0) < 64, 0.0, 0.25))
     high = value.astype(BF16).astype(F32)
     return jnp.where(iota(shape, 1) < 128, high, value - high).astype(BF16)
 
@@ -63,7 +68,7 @@
     shape = (64, 384)
     n1, k1 = iota(shape, 0), iota(shape, 1) & 63
     turns = to_turns((2 * k1 + 1) * n1, 256)
-    value = sin_turns(turns + jnp.where((iota(shape, 1) & 64) == 0, 0.25, 0.5)) * scale
+    value = cos_turns(turns + jnp.where((iota(shape, 1) & 64) == 0, 0.0, 0.25)) * scale
     high = value.astype(BF16).astype(F32)
     return jnp.where(iota(shape, 1) < 256, high, value - high).astype(BF16)
 
@@ -71,13 +76,13 @@
 def twiddles():
     shape = (64, 128)
     turns = to_turns((2 * iota(shape, 0) + 1) * iota(shape, 1), 32768)
-    return sin_turns(turns + 0.25), sin_turns(turns)
+    return cos_turns(turns), sin_turns(turns)
 
 
 def lane_dft():
     shape = (128, 128)
     turns = to_turns(iota(shape, 0) * iota(shape, 1), 128)
-    return split(sin_turns(turns + 0.25)), split(sin_turns(turns))
+    return split(cos_turns(turns)), split(sin_turns(turns))
 
 
 def dot(left, right):
@@ -146,11 +151,13 @@
 
 
 def filter_kernel(
-    ew, eb, iw, ib, freq, fw, sw, sb, skip,
-    hre, him, frows, irows, flanes, ilanes, twiddle, scalars,
-    build, lhs1, lhs2, taps,
+    ew, eb, iw, ib, freq, fw, sw, sb, skip, weight,
+    hre, him, frows, irows, flanes, ilanes, twiddle, scalars, kept,
+    build, lhs1, lhs2, taps, arrived,
 ):
     length = 8192
+    fetch = pltpu.make_async_copy(weight.at[0:EARLY], kept, arrived)
+    fetch.start()
     own = lax.axis_index("row") * 4
     first_channel = lax.axis_index("col") * 128 + own
 
@@ -183,14 +190,14 @@
     turns_of = freq[...] * (1.0 / (2.0 * math.pi))
     build[...] = jnp.zeros_like(build)
     embed = ew[...] * turns_of
-    bias = eb[...] * turns_of
+    bias = eb[...] * turns_of - 0.25
     rows = jnp.concatenate([embed[1:33], embed[0:1], bias], axis=0)
     build[0:34, 0:64] = high_of(rows)
     build[48:82, 0:64] = high_of(rows)
     build[96:130, 0:64] = rows - high_of(rows)
     lhs1[...] = build[...].T[0:64, :].astype(BF16)
     inner = iw[...] * turns_of
-    bias = ib[...] * turns_of
+    bias = ib[...] * turns_of - 0.25
     build[...] = jnp.zeros_like(build)
     build[0:64, 0:64] = high_of(inner)
     build[64:128, 0:64] = high_of(inner)
@@ -212,8 +219,8 @@
     lane = iota((16, 128), 1).astype(F32)
     coarse = band * (lane * (128.0 / length))
     fine = band * (lane * (1.0 / length))
-    coarse_cos, coarse_sin = sin_turns(coarse + 0.25), sin_turns(coarse)
-    fine_cos, fine_sin = sin_turns(fine + 0.25), sin_turns(fine)
+    coarse_cos, coarse_sin = cos_turns(coarse), sin_turns(coarse)
+    fine_cos, fine_sin = cos_turns(fine), sin_turns(fine)
     row = iota((16, 128), 0)
     extra = jnp.where(row == 0, lane * (1.0 / (length - 1)), jnp.where(row == 1, 1.0, 0.0))
     extra_step = jnp.where(row == 0, 128.0 / (length - 1), 0.0)
@@ -223,7 +230,7 @@
     rate = -DECAY_SLOW + channel_row.astype(F32) * rate_step
     ramp = iota((8, 128), 1).astype(F32) * (1.0 / (length - 1))
 
-    chunk = 1024
+    chunk = 4096
     blocks = chunk // 128
     ones16 = jnp.ones((16, chunk), BF16)
     for step in range(length // chunk):
@@ -242,8 +249,8 @@
                     axis=0,
                 )
             )
-        hidden = sin_turns(dot(left1, stack3(jnp.concatenate(feature, axis=1))))
-        hidden = sin_turns(dot(left2, jnp.concatenate([stack3(hidden), ones16], axis=0)))
+        hidden = cos_turns(dot(left1, stack3(jnp.concatenate(feature, axis=1))), SHORT_COEFFS)
+        hidden = cos_turns(dot(left2, jnp.concatenate([stack3(hidden), ones16], axis=0)), SHORT_COEFFS)
         high = hidden.astype(BF16)
         value = dot(left3, jnp.concatenate([high, high], axis=0))
         for block in range(blocks):
@@ -271,6 +278,7 @@
         left = jnp.concatenate([jnp.concatenate(reals, axis=0), jnp.concatenate(imags, axis=0)], axis=1)
         left = left.astype(BF16)
         out[...] = dot(jnp.concatenate([left, left], axis=1), table)
+    fetch.wait()
 
 
 def shifted(value, amount):
@@ -287,7 +295,7 @@
 def conv_kernel(
     moved, hre, him, frows, irows, flanes, ilanes, twiddle, scalars, weight, out, kept, wide, result, arrived
 ):
-    fetch = pltpu.make_async_copy(weight, kept, arrived)
+    fetch = pltpu.make_async_copy(weight.at[EARLY:1024], kept, arrived)
     fetch.start()
     wide[...] = moved[...].astype(F32).reshape(768, 128)
     smoothed = []
@@ -307,10 +315,10 @@
     signal = smoothed[2]
     for order in range(2):
         following = []
-        for pair in ((0, 1), (2, 3)):
+        for pair in ((0, 1, 2, 3),):
             stage = dot(forward_rows, stack3(jnp.concatenate([signal[c] for c in pair], axis=1)))
             reals, imags = [], []
-            for place in range(2):
+            for place in range(4):
                 real = stage[0:64, place * 128 : place * 128 + 128]
                 imag = stage[64:128, place * 128 : place * 128 + 128]
                 reals.append(real * tw_cos + imag * tw_sin)
@@ -319,13 +327,13 @@
             spectrum = dot(lanes3(left), forward_lanes)
             real, imag = spectrum[:, 0:128], spectrum[:, 128:256]
             at = order * 256 + pair[0] * 64
-            tap_real, tap_imag = hre[at : at + 128, :], him[at : at + 128, :]
+            tap_real, tap_imag = hre[at : at + 256, :], him[at : at + 256, :]
             left = jnp.concatenate(
                 [real * tap_real - imag * tap_imag, real * tap_imag + imag * tap_real], axis=1
             )
             back = dot(lanes3(left), inverse_lanes)
             columns = []
-            for place in range(2):
+            for place in range(4):
                 real = back[place * 64 : place * 64 + 64, 0:128]
                 imag = back[place * 64 : place * 64 + 64, 128:256]
                 columns.append(
@@ -357,9 +365,9 @@
         out[half * 4 : half * 4 + 4] = normed.reshape(4, 32, 128)
 
 
-def output_kernel(mixed, weight, out):
+def output_kernel(mixed, early, late, out):
     left = jnp.concatenate([mixed[c] for c in range(8)], axis=1)
-    out[...] = dot(left, weight[...]).astype(BF16)
+    out[...] = (dot(left[:, 0:EARLY], early[...]) + dot(left[:, EARLY:1024], late[...])).astype(BF16)
 
 
 VMEM = pl.BlockSpec(memory_space=pltpu.VMEM)
@@ -436,7 +444,7 @@
         5 + len(small),
     )
     moved = lax.all_to_all(sent, "row", split_axis=0, concat_axis=0, tiled=True)
-    prepared = run(
+    *prepared, kept_early = run(
         filter_kernel,
         (
             pltpu.VMEM((512, 128), F32),
@@ -447,19 +455,22 @@
             pltpu.VMEM((768, 256), BF16),
             pltpu.VMEM((128, 128), F32),
             pltpu.VMEM((64, 128), F32),
+            pltpu.VMEM((EARLY, 2048), BF16),
         ),
-        tuple(near(value) for value in small[:9]),
+        (*(near(value) for value in small[:9]), *far(output_weight)),
         [
             pltpu.VMEM((256, 128), F32),
             pltpu.VMEM((64, 256), BF16),
             pltpu.VMEM((64, 256), BF16),
             pltpu.VMEM((1024, 128), F32),
+            pltpu.SemaphoreType.DMA,
         ],
         "filters",
+        1,
     )
     mixed, kept = run(
         conv_kernel,
-        (pltpu.VMEM((32, 8, 128), BF16), pltpu.VMEM((1024, 2048), BF16)),
+        (pltpu.VMEM((32, 8, 128), BF16), pltpu.VMEM((1024 - EARLY, 2048), BF16)),
         (*(near(value) for value in (moved, *prepared)), *far(output_weight)),
         [pltpu.VMEM((768, 128), F32), pltpu.VMEM((256, 128), F32), pltpu.SemaphoreType.DMA],
         "convolve",
@@ -477,7 +488,7 @@
     return run(
         output_kernel,
         jax.ShapeDtypeStruct((32, 2048), BF16),
-        (near(gathered), near(kept)),
+        (near(gathered), near(kept_early), near(kept)),
         [],
         "output",
     )

time: 54.7 us -> 54.2 us (level)
  Pallas kernels: 13.1 us -> 11.8 us
  waiting for transfers between devices: 5.02 us -> 6.05 us
    pallas_call x5, Pallas kernels: 13.1 us -> 11.8 us  [run(): pl.pallas_call(kernel, out_shape=out_shape, in_specs=[VMEM] * (len(inputs...]
    all_to_all x1, waiting for transfers between devices: 5.02 us -> 6.05 us  [local(): moved = lax.all_to_all(sent, 'row', split_axis=0, concat_axis=0, tiled=True)]
    all_to_all x1, blocking collectives: 12.7 us -> 11.8 us  [local(): lax.all_to_all(mixed, 'row', split_axis=0, concat_axis=0, tiled=True)]
    all_to_all x1, blocking collectives: 11.8 us -> 12.4 us  [local(): lax.all_to_all(normed, 'col', split_axis=0, concat_axis=0, tiled=True)]
  transfers between devices with their start and end apart: 1 -> 1, of which waited for: 1 -> 1; matrix products, arithmetic and copies ran while one was open for 0% -> 0% of each run, Pallas kernels for 10% -> 9%
where the time goes in v4:
time: 54.2 us; the launch traced here: 53.9 us
  blocking collectives  24.2 us (45%)
  starting transfers between devices  11.9 us (22%)
  Pallas kernels  11.8 us (22%)
  waiting for transfers between devices  6.05 us (11%)
    all_to_all x1, blocking collectives, local(): lax.all_to_all(normed, 'col', split_axis=0, concat_axis=0, tiled=True)  12.4 us
    all_to_all x1, starting transfers between devices, local(): moved = lax.all_to_all(sent, 'row', split_axis=0, concat_axis=0, tiled=True)  11.9 us
    all_to_all x1, blocking collectives, local(): lax.all_to_all(mixed, 'row', split_axis=0, concat_axis=0, tiled=True)  11.8 us
    pallas_call x5, Pallas kernels, run(): pl.pallas_call(kernel, out_shape=out_shape, in_specs=[VMEM] * (len(inputs...  11.8 us
    all_to_all x1, waiting for transfers between devices, local(): moved = lax.all_to_all(sent, 'row', split_axis=0, concat_axis=0, tiled=True)  6.05 us
  transfers between devices with their start and end apart: 1, of which 1 were waited for; matrix products, arithmetic and copies ran while one was open for 0% of the time, Pallas kernels for 9%

profile of v4, /device:TPU:1, one launch (start us, length us, event | category | flops | bytes accessed | tf_op | source)
XLA Modules:
  0.0 53.9 jit_solution(5288405226858892923)
XLA Ops:
  0.0 3.5 %project.1 = (bf16[32,24,128]{2,1,0:T(8,128)(2,1)}, f32[33,64]{1,0:T(8,128)S(1)}, f32[1,64]{1,0:T(1,128)S(1)}, f32[64,64]{1,0:T(8,128)S(1)}, f32[1,64]{1,0:T(1,1...) custom-call(bf16[256,2048]{1,0:T(8,128)(2,1)} %refs_0_.1, ...), custom_call_target="tpu_custom_call" | custom-call | tf_op jit(solution)/shard_map/project/pallas_call | solution.py:379
  3.5 11.9 %all-to-all-start = ((bf16[32,24,128]{2,1,0:T(8,128)(2,1)}), bf16[32,24,128]{2,1,0:T(8,128)(2,1)S(1)}, u32[]{:S(2)}, u32[]{:S(2)}) async-start(bf16[32,24,128]{2,1,0:T(8,128)(2,1)} %get-tuple-element.27), calls=%async_computation | async-start | bytes 393216 | tf_op jit(solution)/shard_map/all_to_all | solution.py:446
  15.3 4.7 %filters.1 = (f32[512,128]{1,0:T(8,128)S(1)}, f32[512,128]{1,0:T(8,128)S(1)}, bf16[128,192]{1,0:T(8,128)(2,1)S(1)}, bf16[64,384]{1,0:T(8,128)(2,1)S(1)}, bf16[76...) custom-call(f32[33,64]{1,0:T(8,128)S(1)} %get-tuple-element.28.ew, ...), custom_call_target="tpu_custom_call" | custom-call | tf_op jit(solution)/shard_map/filters/pallas_call | solution.py:379
  20.0 6.0 %all-to-all-done.moved = bf16[32,24,128]{2,1,0:T(8,128)(2,1)S(1)} async-done(((bf16[32,24,128]{2,1,0:T(8,128)(2,1)}), bf16[32,24,128]{2,1,0:T(8,128)(2,1)S(1)}, u32[]{:S(2)}, u32[]{:S(2)}) %all-to-all-start) | async-done | bytes 196640 | tf_op jit(solution)/shard_map/all_to_all | solution.py:446
  26.1 2.0 %convolve.1 = (bf16[32,8,128]{2,1,0:T(8,128)(2,1)S(1)}, bf16[640,2048]{1,0:T(8,128)(2,1)S(1)}) custom-call(bf16[32,24,128]{2,1,0:T(8,128)(2,1)S(1)} %all-to-all-done.moved, f32[512,128]{1,0:T(8,128)S(1)} %get-tuple-element.37.hre, f32[512,128]{1,0:T(8,128)S(1)} %get-tuple-element.38.him, bf16[128,192]{1,0:T(8,128)(2,1)S(1)} %get-tuple-element.39.frows, ...), custom_call_target="tpu_custom_call" | custom-call | tf_op jit(solution)/shard_map/convolve/pallas_call | solution.py:379
  28.0 11.8 %all_to_all.15.moved = bf16[32,8,128]{2,1,0:T(8,128)(2,1)S(1)} all-to-all(bf16[32,8,128]{2,1,0:T(8,128)(2,1)S(1)} %get-tuple-element.45), channel_id=1, replica_groups=mesh['row'=32,'col'=8] {'row'}, dimensions={0} | all-to-all | bytes 131072 | tf_op jit(solution)/shard_map/all_to_all | solution.py:479
  39.9 0.2 groupnorm.1
  40.0 12.4 %all_to_all.16.mixed = bf16[8,32,128]{2,1,0:T(8,128)(2,1)S(1)} all-to-all(bf16[8,32,128]{2,1,0:T(8,128)(2,1)S(1)} %groupnorm.1), channel_id=1, replica_groups=mesh['row'=32,'col'=8] {'col'}, dimensions={0} | all-to-all | bytes 131072 | tf_op jit(solution)/shard_map/all_to_all | solution.py:487
  52.4 1.5 %output.1 = bf16[32,2048]{1,0:T(8,128)(2,1)} custom-call(bf16[8,32,128]{2,1,0:T(8,128)(2,1)S(1)} %all_to_all.16.mixed, bf16[384,2048]{1,0:T(8,128)(2,1)S(1)} %get-tuple-element.47.early, bf16[640,2048]{1,0:T(8,128)(2,1)S(1)} %get-tuple-element.48.late), custom_call_target="tpu_custom_call" | custom-call | tf_op jit(solution)/shard_map/output/pallas_call | solution.py:379
Async XLA Ops:
  3.5 22.6 %all-to-all-start = ((bf16[32,24,128]{2,1,0:T(8,128)(2,1)}), bf16[32,24,128]{2,1,0:T(8,128)(2,1)S(1)}, u32[]{:S(2)}, u32[]{:S(2)}) async-start(bf16[32,24,128]{2,1,0:T(8,128)(2,1)} %get-tuple-element.27), calls=%async_computation | async-start | bytes 393216 | tf_op jit(solution)/shard_map/all_to_all | solution.py:446

commit v5 on v4

--- a/solution.py
+++ b/solution.py
@@ -10,7 +10,6 @@
 
 CHANNELS = 1024
 FREQ_BANDS = 16
-EARLY = 384
 NORM_EPS = 1e-06
 DECAY_SLOW = math.log(0.01) / 1.5
 DECAY_FAST = math.log(0.01) / 0.3
@@ -100,18 +99,18 @@
 
 
 def project_kernel(*refs):
-    count = len(refs) - 15
+    extra = (len(refs) - 15) // 2
     tokens, gain, w0, w1, w2 = refs[0:5]
-    small = refs[5 : 5 + count // 2]
-    out = refs[5 + count // 2]
-    carried = refs[6 + count // 2 : 6 + count]
-    near_tokens, near_gain, n0, n1, n2, normed, scratch, arrived, carry = refs[6 + count :]
+    small = refs[5 : 5 + extra]
+    out, normed, n1 = refs[5 + extra : 8 + extra]
+    carried = refs[8 + extra : 8 + 2 * extra]
+    near_tokens, near_gain, n0, n2, scratch, arrived, carry = refs[8 + 2 * extra :]
     rows = 64
     copies = [pltpu.make_async_copy(gain, near_gain, arrived.at[0])]
     for part in range(4):
         where = pl.ds(part * rows, rows)
         copies.append(pltpu.make_async_copy(tokens.at[where], near_tokens.at[where], arrived.at[part + 1]))
-    for index, (source, target) in enumerate(((w0, n0), (w1, n1), (w2, n2))):
+    for index, (source, target) in enumerate(((w0, n0), (w2, n2), (w1, n1))):
         copies.append(pltpu.make_async_copy(source, target, arrived.at[index + 5]))
     carries = [
         pltpu.make_async_copy(source, target, carry.at[index])
@@ -125,17 +124,22 @@
         wide = near_tokens[part * rows : part * rows + rows, :].astype(F32)
         scale = lax.rsqrt(jnp.mean(wide * wide, axis=1, keepdims=True) + NORM_EPS)
         normed[part * rows : part * rows + rows, :] = (wide * scale * near_gain[...]).astype(BF16)
-    for copy in copies[5:]:
-        copy.wait()
-    weights = jnp.concatenate([n0[...], n1[...], n2[...]], axis=1)
+    copies[5].wait()
+    copies[6].wait()
+    weights = jnp.concatenate([n0[...], n2[...]], axis=1)
     for half in range(2):
         gates = dot(normed[half * 128 : half * 128 + 128, :], weights)
-        for branch in range(3):
+        for branch in range(2):
             block = gates[:, branch * 128 : branch * 128 + 128].T
             for peer in range(32):
-                start = peer * 24 + half * 12 + branch * 4
+                start = peer * 18 + half * 9 + branch * 4
                 scratch[start : start + 4, :] = block[peer * 4 : peer * 4 + 4, :]
-    out[...] = scratch[...].astype(BF16).reshape(32, 24, 128)
+    copies[7].wait()
+    edges = dot(jnp.concatenate([normed[0:16, :], normed[240:256, :]], axis=0), n1[...])
+    for peer in range(32):
+        scratch[peer * 18 + 8 : peer * 18 + 9, :] = edges[0:1, :]
+        scratch[peer * 18 + 17 : peer * 18 + 18, :] = edges[31:32, :]
+    out[...] = scratch[...].astype(BF16)
     for copy in carries:
         copy.wait()
 
@@ -147,19 +151,26 @@
         return jnp.concatenate([top, bottom], axis=0)
 
     high, low = part(cos[0], sin[0]), part(cos[1], sin[1])
-    return jnp.concatenate([high, high, low], axis=0)
+    return jnp.concatenate([high, low], axis=0)
 
 
 def filter_kernel(
-    ew, eb, iw, ib, freq, fw, sw, sb, skip, weight,
-    hre, him, frows, irows, flanes, ilanes, twiddle, scalars, kept,
-    build, lhs1, lhs2, taps, arrived,
+    normed, w1, ew, eb, iw, ib, freq, fw, sw, sb, skip,
+    hre, him, frows, irows, flanes, ilanes, twiddle, scalars, gate,
+    build, lhs1, lhs2, taps, turned,
 ):
     length = 8192
-    fetch = pltpu.make_async_copy(weight.at[0:EARLY], kept, arrived)
-    fetch.start()
     own = lax.axis_index("row") * 4
     first_channel = lax.axis_index("col") * 128 + own
+
+    source = dot(normed[...], w1[...]).astype(BF16).astype(F32)
+    zero = jnp.zeros((1, 128), F32)
+    before = jnp.concatenate([zero, source[0:255]], axis=0)
+    after = jnp.concatenate([source[1:256], zero], axis=0)
+    second = sw[1].astype(F32)
+    total = sb[1:2, :] + before * second[0:1]
+    total = total + source * second[1:2]
+    gate[...] = total + after * second[2:3]
 
     lines = []
     for branch in range(3):
@@ -233,34 +244,45 @@
     chunk = 4096
     blocks = chunk // 128
     ones16 = jnp.ones((16, chunk), BF16)
-    for step in range(length // chunk):
+    turned[0:16, :] = coarse_cos
+    turned[16:32, :] = coarse_sin
+
+    def one_chunk(step, carry):
+        first = step * blocks
+        column = pltpu.roll(turned[...], (128 - first) % 128, 1)
+        start = first.astype(F32)
         feature = []
         for block in range(blocks):
-            n1 = step * blocks + block
-            ca = jnp.broadcast_to(coarse_cos[:, n1 : n1 + 1], (16, 128))
-            sa = jnp.broadcast_to(coarse_sin[:, n1 : n1 + 1], (16, 128))
+            ca = jnp.broadcast_to(column[0:16, block : block + 1], (16, 128))
+            sa = jnp.broadcast_to(column[16:32, block : block + 1], (16, 128))
             feature.append(
                 jnp.concatenate(
                     [
                         ca * fine_cos - sa * fine_sin,
                         -(sa * fine_cos + ca * fine_sin),
-                        extra + extra_step * float(n1),
+                        extra + extra_step * (start + float(block)),
                     ],
                     axis=0,
                 )
             )
         hidden = cos_turns(dot(left1, stack3(jnp.concatenate(feature, axis=1))), SHORT_COEFFS)
-        hidden = cos_turns(dot(left2, jnp.concatenate([stack3(hidden), ones16], axis=0)), SHORT_COEFFS)
+        hidden = cos_turns(
+            dot(left2, jnp.concatenate([stack3(hidden), ones16], axis=0)), SHORT_COEFFS
+        )
         high = hidden.astype(BF16)
         value = dot(left3, jnp.concatenate([high, high], axis=0))
         for block in range(blocks):
-            n1 = step * blocks + block
-            window = jnp.exp((ramp + n1 * 128.0 / (length - 1)) * -rate)
+            here = ramp + (start + float(block)) * (128.0 / (length - 1))
+            window = jnp.exp(here * -rate)
             piece = value[:, block * 128 : block * 128 + 128] * jnp.concatenate([window, window], axis=0)
-            if n1 == 0:
-                swapped = jnp.concatenate([piece[4:8], piece[0:4], piece[12:16], piece[8:12]], axis=0)
-                piece = jnp.where(iota((16, 128), 1) == 0, 0.5 * (piece + swapped), piece)
-            taps[n1 * 16 : n1 * 16 + 16, :] = piece
+            at = pl.multiple_of((first + block) * 16, 16)
+            taps[pl.ds(at, 16), :] = piece
+        return carry
+
+    lax.fori_loop(0, length // chunk, one_chunk, 0)
+    piece = taps[0:16, :]
+    swapped = jnp.concatenate([piece[4:8], piece[0:4], piece[12:16], piece[8:12]], axis=0)
+    taps[0:16, :] = jnp.where(iota((16, 128), 1) == 0, 0.5 * (piece + swapped), piece)
 
     spread = jnp.concatenate([taps[pl.ds(r, 64, stride=16), :] for r in range(16)], axis=1)
     stage = dot(frows[...], stack3(spread))
@@ -278,7 +300,6 @@
         left = jnp.concatenate([jnp.concatenate(reals, axis=0), jnp.concatenate(imags, axis=0)], axis=1)
         left = left.astype(BF16)
         out[...] = dot(jnp.concatenate([left, left], axis=1), table)
-    fetch.wait()
 
 
 def shifted(value, amount):
@@ -292,66 +313,80 @@
     return jnp.where(lane == edge_lane, carried, rolled)
 
 
+def repeat_high(table):
+    return jnp.concatenate([table[0:256, :], table[0:256, :], table[256:512, :]], axis=0)
+
+
 def conv_kernel(
-    moved, hre, him, frows, irows, flanes, ilanes, twiddle, scalars, weight, out, kept, wide, result, arrived
+    moved, hre, him, frows, irows, flanes, ilanes, twiddle, scalars, sw, weight,
+    out, edges, kept, wide, result, state, factors, arrived,
 ):
-    fetch = pltpu.make_async_copy(weight.at[EARLY:1024], kept, arrived)
+    fetch = pltpu.make_async_copy(weight, kept, arrived)
     fetch.start()
-    wide[...] = moved[...].astype(F32).reshape(768, 128)
+    wide[...] = moved[...].astype(F32)
+    own = lax.axis_index("row")
+    before = wide[pl.ds(jnp.maximum(own - 1, 0) * 18 + 17, 1), :]
+    after = wide[pl.ds(jnp.minimum(own + 1, 31) * 18 + 8, 1), :]
+    second = sw[1].astype(F32)
+    edges[0:1, :] = jnp.where(own > 0, before, 0.0) * second[0:1]
+    edges[1:2, :] = jnp.where(own < 31, after, 0.0) * second[2:3]
     smoothed = []
-    for branch in range(3):
+    for branch in range(2):
         rows = []
         for channel in range(4):
-            value = wide[pl.ds(branch * 4 + channel, 64, stride=12), :]
-            base = channel * 16 + branch * 4
+            value = wide[pl.ds(branch * 4 + channel, 64, stride=9), :]
+            base = channel * 16 + branch * 8
             total = scalars[base : base + 1, :] + shifted(value, 1) * scalars[base + 1 : base + 2, :]
             total = total + value * scalars[base + 2 : base + 3, :]
             total = total + shifted(value, -1) * scalars[base + 3 : base + 4, :]
             rows.append(total)
         smoothed.append(rows)
-    forward_rows, inverse_rows = frows[...], irows[...]
-    forward_lanes, inverse_lanes = flanes[...], ilanes[...]
+    forward_rows, inverse_rows, forward_lanes, inverse_lanes = frows, irows, flanes, ilanes
     tw_cos, tw_sin = twiddle[0:64, :], twiddle[64:128, :]
-    signal = smoothed[2]
-    for order in range(2):
-        following = []
-        for pair in ((0, 1, 2, 3),):
-            stage = dot(forward_rows, stack3(jnp.concatenate([signal[c] for c in pair], axis=1)))
-            reals, imags = [], []
-            for place in range(4):
-                real = stage[0:64, place * 128 : place * 128 + 128]
-                imag = stage[64:128, place * 128 : place * 128 + 128]
-                reals.append(real * tw_cos + imag * tw_sin)
-                imags.append(imag * tw_cos - real * tw_sin)
-            left = jnp.concatenate([jnp.concatenate(reals, axis=0), jnp.concatenate(imags, axis=0)], axis=1)
-            spectrum = dot(lanes3(left), forward_lanes)
-            real, imag = spectrum[:, 0:128], spectrum[:, 128:256]
-            at = order * 256 + pair[0] * 64
-            tap_real, tap_imag = hre[at : at + 256, :], him[at : at + 256, :]
-            left = jnp.concatenate(
-                [real * tap_real - imag * tap_imag, real * tap_imag + imag * tap_real], axis=1
+    for channel in range(4):
+        state[channel * 64 : channel * 64 + 64, :] = smoothed[1][channel]
+        factors[channel * 64 : channel * 64 + 64, :] = smoothed[0][channel]
+    factors[256:512, :] = jnp.ones((256, 128), F32)
+
+    def one_order(order, carry):
+        signal = [state[c * 64 : c * 64 + 64, :] for c in range(4)]
+        stage = dot(forward_rows[...], stack3(jnp.concatenate(signal, axis=1)))
+        reals, imags = [], []
+        for place in range(4):
+            real = stage[0:64, place * 128 : place * 128 + 128]
+            imag = stage[64:128, place * 128 : place * 128 + 128]
+            reals.append(real * tw_cos + imag * tw_sin)
+            imags.append(imag * tw_cos - real * tw_sin)
+        left = jnp.concatenate([jnp.concatenate(reals, axis=0), jnp.concatenate(imags, axis=0)], axis=1)
+        spectrum = dot(lanes3(left), repeat_high(forward_lanes))
+        real, imag = spectrum[:, 0:128], spectrum[:, 128:256]
+        at = pl.multiple_of(order * 256, 256)
+        tap_real, tap_imag = hre[pl.ds(at, 256), :], him[pl.ds(at, 256), :]
+        left = jnp.concatenate([real * tap_real - imag * tap_imag, real * tap_imag + imag * tap_real], axis=1)
+        back = dot(lanes3(left), repeat_high(inverse_lanes))
+        columns = []
+        for place in range(4):
+            real = back[place * 64 : place * 64 + 64, 0:128]
+            imag = back[place * 64 : place * 64 + 64, 128:256]
+            columns.append(
+                jnp.concatenate([real * tw_cos - imag * tw_sin, real * tw_sin + imag * tw_cos], axis=0)
             )
-            back = dot(lanes3(left), inverse_lanes)
-            columns = []
-            for place in range(4):
-                real = back[place * 64 : place * 64 + 64, 0:128]
-                imag = back[place * 64 : place * 64 + 64, 128:256]
-                columns.append(
-                    jnp.concatenate([real * tw_cos - imag * tw_sin, real * tw_sin + imag * tw_cos], axis=0)
-                )
-            values = dot(inverse_rows, stack3(jnp.concatenate(columns, axis=1)))
-            for place, channel in enumerate(pair):
-                at = channel * 16 + 12 + order
-                conv = values[:, place * 128 : place * 128 + 128] + signal[channel] * scalars[at : at + 1, :]
-                following.append(smoothed[order][channel] * conv)
-        signal = following
+        values = dot(inverse_rows[...], stack3(jnp.concatenate(columns, axis=1)))
+        for channel in range(4):
+            skip = scalars[pl.ds(channel * 16 + 12 + order, 1), :]
+            conv = values[:, channel * 128 : channel * 128 + 128] + signal[channel] * skip
+            factor = factors[pl.ds(at + channel * 64, 64), :]
+            state[channel * 64 : channel * 64 + 64, :] = conv * factor
+        return carry
+
+    lax.fori_loop(0, 2, one_order, 0)
     for channel in range(4):
-        result[pl.ds(channel, 64, stride=4), :] = signal[channel]
+        result[pl.ds(channel, 64, stride=4), :] = state[channel * 64 : channel * 64 + 64, :]
     out[...] = result[...].astype(BF16).reshape(32, 8, 128)
     fetch.wait()
 
 
-def norm_kernel(moved, gain, out, wide, ordered):
+def norm_kernel(moved, gate, edges, gain, out, wide, ordered):
     wide[...] = moved[...].astype(F32).reshape(256, 128)
     for half in range(2):
         for channel in range(4):
@@ -359,15 +394,17 @@
                 pl.ds(half * 4 + channel, 32, stride=8), :
             ]
     for half in range(2):
-        value = ordered[half * 128 : half * 128 + 128, :]
-        scale = lax.rsqrt(jnp.mean(value * value, axis=0, keepdims=True) + NORM_EPS)
-        normed = ((value * scale).T * gain[...]).astype(BF16)
-        out[half * 4 : half * 4 + 4] = normed.reshape(4, 32, 128)
-
-
-def output_kernel(mixed, early, late, out):
+        edge_row = 0 if half == 0 else 127
+        factor = gate[half * 128 : half * 128 + 128, :]
+        factor = factor + jnp.where(iota((128, 128), 0) == edge_row, edges[half : half + 1, :], 0.0)
+        value = ordered[half * 128 : half * 128 + 128, :].T * factor
+        scale = lax.rsqrt(jnp.mean(value * value, axis=1, keepdims=True) + NORM_EPS)
+        out[half * 4 : half * 4 + 4] = (value * scale * gain[...]).astype(BF16).reshape(4, 32, 128)
+
+
+def output_kernel(mixed, weight, out):
     left = jnp.concatenate([mixed[c] for c in range(8)], axis=1)
-    out[...] = (dot(left[:, 0:EARLY], early[...]) + dot(left[:, EARLY:1024], late[...])).astype(BF16)
+    out[...] = dot(left, weight[...]).astype(BF16)
 
 
 VMEM = pl.BlockSpec(memory_space=pltpu.VMEM)
@@ -425,54 +462,64 @@
         filter_skip,
         output_gain.reshape(1, -1),
     )
-    sent, *small = run(
+    sent, rows, second, *small = run(
         project_kernel,
-        (pltpu.VMEM((32, 24, 128), BF16), *(pltpu.VMEM(value.shape, value.dtype) for value in small)),
+        (
+            pltpu.VMEM((576, 128), BF16),
+            pltpu.VMEM((256, 2048), BF16),
+            pltpu.VMEM((2048, 128), BF16),
+            *(pltpu.VMEM(value.shape, value.dtype) for value in small),
+        ),
         far(tokens, norm_gain.reshape(1, -1), first_gate, second_gate, value_weight, *small),
         [
             pltpu.VMEM((256, 2048), BF16),
             pltpu.VMEM((1, 2048), F32),
             pltpu.VMEM((2048, 128), BF16),
             pltpu.VMEM((2048, 128), BF16),
-            pltpu.VMEM((2048, 128), BF16),
-            pltpu.VMEM((256, 2048), BF16),
-            pltpu.VMEM((768, 128), F32),
+            pltpu.VMEM((576, 128), F32),
             pltpu.SemaphoreType.DMA((8,)),
             pltpu.SemaphoreType.DMA((len(small),)),
         ],
         "project",
         5 + len(small),
     )
-    moved = lax.all_to_all(sent, "row", split_axis=0, concat_axis=0, tiled=True)
-    *prepared, kept_early = run(
+    moved = lax.all_to_all(
+        sent.reshape(32, 9, 2, 128), "row", split_axis=0, concat_axis=0, tiled=True
+    ).reshape(576, 128)
+    *prepared, gate = run(
         filter_kernel,
         (
             pltpu.VMEM((512, 128), F32),
             pltpu.VMEM((512, 128), F32),
             pltpu.VMEM((128, 192), BF16),
             pltpu.VMEM((64, 384), BF16),
-            pltpu.VMEM((768, 256), BF16),
-            pltpu.VMEM((768, 256), BF16),
+            pltpu.VMEM((512, 256), BF16),
+            pltpu.VMEM((512, 256), BF16),
             pltpu.VMEM((128, 128), F32),
             pltpu.VMEM((64, 128), F32),
-            pltpu.VMEM((EARLY, 2048), BF16),
+            pltpu.VMEM((256, 128), F32),
         ),
-        (*(near(value) for value in small[:9]), *far(output_weight)),
+        tuple(near(value) for value in (rows, second, *small[:9])),
         [
             pltpu.VMEM((256, 128), F32),
             pltpu.VMEM((64, 256), BF16),
             pltpu.VMEM((64, 256), BF16),
             pltpu.VMEM((1024, 128), F32),
+            pltpu.VMEM((32, 128), F32),
+        ],
+        "filters",
+    )
+    mixed, edges, kept = run(
+        conv_kernel,
+        (pltpu.VMEM((32, 8, 128), BF16), pltpu.VMEM((2, 128), F32), pltpu.VMEM((1024, 2048), BF16)),
+        (*(near(value) for value in (moved, *prepared, small[6])), *far(output_weight)),
+        [
+            pltpu.VMEM((576, 128), F32),
+            pltpu.VMEM((256, 128), F32),
+            pltpu.VMEM((256, 128), F32),
+            pltpu.VMEM((512, 128), F32),
             pltpu.SemaphoreType.DMA,
         ],
-        "filters",
-        1,
-    )
-    mixed, kept = run(
-        conv_kernel,
-        (pltpu.VMEM((32, 8, 128), BF16), pltpu.VMEM((1024 - EARLY, 2048), BF16)),
-        (*(near(value) for value in (moved, *prepared)), *far(output_weight)),
-        [pltpu.VMEM((768, 128), F32), pltpu.VMEM((256, 128), F32), pltpu.SemaphoreType.DMA],
         "convolve",
         1,
     )
@@ -480,7 +527,7 @@
     normed = run(
         norm_kernel,
         pltpu.VMEM((8, 32, 128), BF16),
-        (near(result), near(small[9])),
+        tuple(near(value) for value in (result, gate, edges, small[9])),
         [pltpu.VMEM((256, 128), F32), pltpu.VMEM((256, 128), F32)],
         "groupnorm",
     )
@@ -488,7 +535,7 @@
     return run(
         output_kernel,
         jax.ShapeDtypeStruct((32, 2048), BF16),
-        (near(gathered), near(kept_early), near(kept)),
+        (near(gathered), near(kept)),
         [],
         "output",
     )

time: 54.2 us -> 53.3 us (0.983)
  waiting for transfers between devices: 6.05 us -> 5.3 us
    all_to_all x1, waiting for transfers between devices: 6.05 us -> 5.3 us  [local(): lax.all_to_all(sent.reshape(32, 9, 2, 128), 'row', split_axis=0, concat_a...]
    all_to_all x1, blocking collectives: 11.8 us -> 12.4 us  [local(): lax.all_to_all(mixed, 'row', split_axis=0, concat_axis=0, tiled=True)]
    all_to_all x1, blocking collectives: 12.4 us -> 11.8 us  [local(): lax.all_to_all(normed, 'col', split_axis=0, concat_axis=0, tiled=True)]
  transfers between devices with their start and end apart: 1 -> 1, of which waited for: 1 -> 1; matrix products, arithmetic and copies ran while one was open for 0% -> 0% of each run, Pallas kernels for 9% -> 8%
where the time goes in v5:
time: 53.3 us; the launch traced here: 53 us
  blocking collectives  24.2 us (45%)
  starting transfers between devices  11.9 us (22%)
  Pallas kernels  11.6 us (22%)
  waiting for transfers between devices  5.3 us (10%)
    all_to_all x1, blocking collectives, local(): lax.all_to_all(mixed, 'row', split_axis=0, concat_axis=0, tiled=True)  12.4 us
    all_to_all x1, starting transfers between devices, local(): lax.all_to_all(sent.reshape(32, 9, 2, 128), 'row', split_axis=0, concat_a...  11.9 us
    all_to_all x1, blocking collectives, local(): lax.all_to_all(normed, 'col', split_axis=0, concat_axis=0, tiled=True)  11.8 us
    pallas_call x5, Pallas kernels, run(): pl.pallas_call(kernel, out_shape=out_shape, in_specs=[VMEM] * (len(inputs...  11.6 us
    all_to_all x1, waiting for transfers between devices, local(): lax.all_to_all(sent.reshape(32, 9, 2, 128), 'row', split_axis=0, concat_a...  5.3 us
  transfers between devices with their start and end apart: 1, of which 1 were waited for; matrix products, arithmetic and copies ran while one was open for 0% of the time, Pallas kernels for 8%

profile of v5, /device:TPU:1, one launch (start us, length us, event | category | flops | bytes accessed | tf_op | source)
XLA Modules:
  0.0 53.0 jit_solution(5739285576857414033)
XLA Ops:
  0.0 3.3 %project.1 = (bf16[576,128]{1,0:T(8,128)(2,1)}, bf16[256,2048]{1,0:T(8,128)(2,1)S(1)}, bf16[2048,128]{1,0:T(8,128)(2,1)S(1)}, f32[33,64]{1,0:T(8,128)S(1)}, f32[...) custom-call(bf16[256,2048]{1,0:T(8,128)(2,1)} %refs_0_.1, ...), custom_call_target="tpu_custom_call" | custom-call | tf_op jit(solution)/shard_map/project/pallas_call | solution.py:416
  3.3 11.9 %all-to-all-start = ((bf16[32,9,2,128]{3,2,1,0:T(2,128)(2,1)}), bf16[32,9,2,128]{3,2,1,0:T(2,128)(2,1)S(1)}, u32[]{:S(2)}, u32[]{:S(2)}) async-start(bf16[32,9,2,128]{3,2,1,0:T(2,128)(2,1)} %bitcast.6), calls=%async_computation | async-start | bytes 294912 | tf_op jit(solution)/shard_map/all_to_all | solution.py:486
  15.2 4.3 %filters.1 = (f32[512,128]{1,0:T(8,128)S(1)}, f32[512,128]{1,0:T(8,128)S(1)}, bf16[128,192]{1,0:T(8,128)(2,1)S(1)}, bf16[64,384]{1,0:T(8,128)(2,1)S(1)}, bf16[51...) custom-call(bf16[256,2048]{1,0:T(8,128)(2,1)S(1)} %get-tuple-element, ...), custom_call_target="tpu_custom_call" | custom-call | tf_op jit(solution)/shard_map/filters/pallas_call | solution.py:416
  19.5 5.3 %all-to-all-done = bf16[32,9,2,128]{3,2,1,0:T(2,128)(2,1)S(1)} async-done(((bf16[32,9,2,128]{3,2,1,0:T(2,128)(2,1)}), bf16[32,9,2,128]{3,2,1,0:T(2,128)(2,1)S(1)}, u32[]{:S(2)}, u32[]{:S(2)}) %all-to-all-start) | async-done | bytes 147488 | tf_op jit(solution)/shard_map/all_to_all | solution.py:486
  24.8 2.3 %convolve.1 = (bf16[32,8,128]{2,1,0:T(8,128)(2,1)S(1)}, f32[2,128]{1,0:T(2,128)S(1)}, bf16[1024,2048]{1,0:T(8,128)(2,1)S(1)}) custom-call(bf16[576,128]{1,0:T(8,128)(2,1)S(1)} %bitcast.8, f32[512,128]{1,0:T(8,128)S(1)} %get-tuple-element.42.hre, f32[512,128]{1,0:T(8,128)S(1)} %get-tuple-element.43.him, bf16[128,192]{1,0:T(8,128)(2,1)S(1)} %get-tuple-element.44.frows, ...), custom_call_target="tpu_custom_call" | custom-call | tf_op jit(solution)/shard_map/convolve/pallas_call | solution.py:416
  27.1 12.4 %all_to_all.15.moved = bf16[32,8,128]{2,1,0:T(8,128)(2,1)S(1)} all-to-all(bf16[32,8,128]{2,1,0:T(8,128)(2,1)S(1)} %get-tuple-element.50), channel_id=1, replica_groups=mesh['row'=32,'col'=8] {'row'}, dimensions={0} | all-to-all | bytes 131072 | tf_op jit(solution)/shard_map/all_to_all | solution.py:526
  39.5 0.2 groupnorm.1
  39.7 11.8 %all_to_all.16.mixed = bf16[8,32,128]{2,1,0:T(8,128)(2,1)S(1)} all-to-all(bf16[8,32,128]{2,1,0:T(8,128)(2,1)S(1)} %groupnorm.1), channel_id=1, replica_groups=mesh['row'=32,'col'=8] {'col'}, dimensions={0} | all-to-all | bytes 131072 | tf_op jit(solution)/shard_map/all_to_all | solution.py:534
  51.5 1.5 %output.1 = bf16[32,2048]{1,0:T(8,128)(2,1)} custom-call(bf16[8,32,128]{2,1,0:T(8,128)(2,1)S(1)} %all_to_all.16.mixed, bf16[1024,2048]{1,0:T(8,128)(2,1)S(1)} %get-tuple-element.54.weight), custom_call_target="tpu_custom_call" | custom-call | tf_op jit(solution)/shard_map/output/pallas_call | solution.py:416
Async XLA Ops:
  3.3 21.5 %all-to-all-start = ((bf16[32,9,2,128]{3,2,1,0:T(2,128)(2,1)}), bf16[32,9,2,128]{3,2,1,0:T(2,128)(2,1)S(1)}, u32[]{:S(2)}, u32[]{:S(2)}) async-start(bf16[32,9,2,128]{3,2,1,0:T(2,128)(2,1)} %bitcast.6), calls=%async_computation | async-start | bytes 294912 | tf_op jit(solution)/shard_map/all_to_all | solution.py:486

commit v6 on v5

--- a/solution.py
+++ b/solution.py
@@ -10,6 +10,7 @@
 
 CHANNELS = 1024
 FREQ_BANDS = 16
+EARLY = 192
 NORM_EPS = 1e-06
 DECAY_SLOW = math.log(0.01) / 1.5
 DECAY_FAST = math.log(0.01) / 0.3
@@ -102,30 +103,32 @@
     extra = (len(refs) - 15) // 2
     tokens, gain, w0, w1, w2 = refs[0:5]
     small = refs[5 : 5 + extra]
-    out, normed, n1 = refs[5 + extra : 8 + extra]
-    carried = refs[8 + extra : 8 + 2 * extra]
-    near_tokens, near_gain, n0, n2, scratch, arrived, carry = refs[8 + 2 * extra :]
-    rows = 64
+    out, normed = refs[5 + extra : 7 + extra]
+    carried = refs[7 + extra : 7 + 2 * extra]
+    near_tokens, near_gain, n0, n1, n2, scratch, arrived, carry = refs[7 + 2 * extra :]
+    rows = 128
     copies = [pltpu.make_async_copy(gain, near_gain, arrived.at[0])]
-    for part in range(4):
+    for part in range(2):
         where = pl.ds(part * rows, rows)
         copies.append(pltpu.make_async_copy(tokens.at[where], near_tokens.at[where], arrived.at[part + 1]))
     for index, (source, target) in enumerate(((w0, n0), (w2, n2), (w1, n1))):
-        copies.append(pltpu.make_async_copy(source, target, arrived.at[index + 5]))
+        copies.append(pltpu.make_async_copy(source, target, arrived.at[index + 3]))
     carries = [
         pltpu.make_async_copy(source, target, carry.at[index])
         for index, (source, target) in enumerate(zip(small, carried))
     ]
-    for copy in copies + carries:
+    for copy in copies:
         copy.start()
     copies[0].wait()
-    for part in range(4):
+    for part in range(2):
         copies[part + 1].wait()
         wide = near_tokens[part * rows : part * rows + rows, :].astype(F32)
         scale = lax.rsqrt(jnp.mean(wide * wide, axis=1, keepdims=True) + NORM_EPS)
         normed[part * rows : part * rows + rows, :] = (wide * scale * near_gain[...]).astype(BF16)
-    copies[5].wait()
-    copies[6].wait()
+    for copy in carries:
+        copy.start()
+    copies[3].wait()
+    copies[4].wait()
     weights = jnp.concatenate([n0[...], n2[...]], axis=1)
     for half in range(2):
         gates = dot(normed[half * 128 : half * 128 + 128, :], weights)
@@ -134,7 +137,7 @@
             for peer in range(32):
                 start = peer * 18 + half * 9 + branch * 4
                 scratch[start : start + 4, :] = block[peer * 4 : peer * 4 + 4, :]
-    copies[7].wait()
+    copies[5].wait()
     edges = dot(jnp.concatenate([normed[0:16, :], normed[240:256, :]], axis=0), n1[...])
     for peer in range(32):
         scratch[peer * 18 + 8 : peer * 18 + 9, :] = edges[0:1, :]
@@ -155,22 +158,17 @@
 
 
 def filter_kernel(
-    normed, w1, ew, eb, iw, ib, freq, fw, sw, sb, skip,
-    hre, him, frows, irows, flanes, ilanes, twiddle, scalars, gate,
-    build, lhs1, lhs2, taps, turned,
+    normed, ew, eb, iw, ib, freq, fw, sw, sb, skip, second_weight, weight,
+    hre, him, frows, irows, flanes, ilanes, twiddle, scalars, gate, kept,
+    build, lhs1, lhs2, taps, turned, w1, arrived,
 ):
     length = 8192
+    fetch_second = pltpu.make_async_copy(second_weight, w1, arrived.at[1])
+    fetch_second.start()
+    fetch = pltpu.make_async_copy(weight.at[0:EARLY], kept, arrived.at[0])
+    fetch.start()
     own = lax.axis_index("row") * 4
     first_channel = lax.axis_index("col") * 128 + own
-
-    source = dot(normed[...], w1[...]).astype(BF16).astype(F32)
-    zero = jnp.zeros((1, 128), F32)
-    before = jnp.concatenate([zero, source[0:255]], axis=0)
-    after = jnp.concatenate([source[1:256], zero], axis=0)
-    second = sw[1].astype(F32)
-    total = sb[1:2, :] + before * second[0:1]
-    total = total + source * second[1:2]
-    gate[...] = total + after * second[2:3]
 
     lines = []
     for branch in range(3):
@@ -284,6 +282,16 @@
     swapped = jnp.concatenate([piece[4:8], piece[0:4], piece[12:16], piece[8:12]], axis=0)
     taps[0:16, :] = jnp.where(iota((16, 128), 1) == 0, 0.5 * (piece + swapped), piece)
 
+    fetch_second.wait()
+    source = dot(normed[...], w1[...]).astype(BF16).astype(F32)
+    zero = jnp.zeros((1, 128), F32)
+    before = jnp.concatenate([zero, source[0:255]], axis=0)
+    after = jnp.concatenate([source[1:256], zero], axis=0)
+    second = sw[1].astype(F32)
+    total = sb[1:2, :] + before * second[0:1]
+    total = total + source * second[1:2]
+    gate[...] = total + after * second[2:3]
+
     spread = jnp.concatenate([taps[pl.ds(r, 64, stride=16), :] for r in range(16)], axis=1)
     stage = dot(frows[...], stack3(spread))
     (cos_high, cos_low), (sin_high, sin_low) = cos, sin
@@ -300,6 +308,7 @@
         left = jnp.concatenate([jnp.concatenate(reals, axis=0), jnp.concatenate(imags, axis=0)], axis=1)
         left = left.astype(BF16)
         out[...] = dot(jnp.concatenate([left, left], axis=1), table)
+    fetch.wait()
 
 
 def shifted(value, amount):
@@ -321,7 +330,7 @@
     moved, hre, him, frows, irows, flanes, ilanes, twiddle, scalars, sw, weight,
     out, edges, kept, wide, result, state, factors, arrived,
 ):
-    fetch = pltpu.make_async_copy(weight, kept, arrived)
+    fetch = pltpu.make_async_copy(weight.at[EARLY:1024], kept, arrived)
     fetch.start()
     wide[...] = moved[...].astype(F32)
     own = lax.axis_index("row")
@@ -358,12 +367,14 @@
             reals.append(real * tw_cos + imag * tw_sin)
             imags.append(imag * tw_cos - real * tw_sin)
         left = jnp.concatenate([jnp.concatenate(reals, axis=0), jnp.concatenate(imags, axis=0)], axis=1)
-        spectrum = dot(lanes3(left), repeat_high(forward_lanes))
+        high = left.astype(BF16)
+        spectrum = dot(jnp.concatenate([high, high], axis=1), forward_lanes[...])
         real, imag = spectrum[:, 0:128], spectrum[:, 128:256]
         at = pl.multiple_of(order * 256, 256)
         tap_real, tap_imag = hre[pl.ds(at, 256), :], him[pl.ds(at, 256), :]
         left = jnp.concatenate([real * tap_real - imag * tap_imag, real * tap_imag + imag * tap_real], axis=1)
-        back = dot(lanes3(left), repeat_high(inverse_lanes))
+        high = left.astype(BF16)
+        back = dot(jnp.concatenate([high, high], axis=1), inverse_lanes[...])
         columns = []
         for place in range(4):
             real = back[place * 64 : place * 64 + 64, 0:128]
@@ -402,9 +413,9 @@
         out[half * 4 : half * 4 + 4] = (value * scale * gain[...]).astype(BF16).reshape(4, 32, 128)
 
 
-def output_kernel(mixed, weight, out):
+def output_kernel(mixed, early, late, out):
     left = jnp.concatenate([mixed[c] for c in range(8)], axis=1)
-    out[...] = dot(left, weight[...]).astype(BF16)
+    out[...] = (dot(left[:, 0:EARLY], early[...]) + dot(left[:, EARLY:1024], late[...])).astype(BF16)
 
 
 VMEM = pl.BlockSpec(memory_space=pltpu.VMEM)
@@ -462,12 +473,11 @@
         filter_skip,
         output_gain.reshape(1, -1),
     )
-    sent, rows, second, *small = run(
+    sent, rows, *small = run(
         project_kernel,
         (
             pltpu.VMEM((576, 128), BF16),
             pltpu.VMEM((256, 2048), BF16),
-            pltpu.VMEM((2048, 128), BF16),
             *(pltpu.VMEM(value.shape, value.dtype) for value in small),
         ),
         far(tokens, norm_gain.reshape(1, -1), first_gate, second_gate, value_weight, *small),
@@ -476,8 +486,9 @@
             pltpu.VMEM((1, 2048), F32),
             pltpu.VMEM((2048, 128), BF16),
             pltpu.VMEM((2048, 128), BF16),
+            pltpu.VMEM((2048, 128), BF16),
             pltpu.VMEM((576, 128), F32),
-            pltpu.SemaphoreType.DMA((8,)),
+            pltpu.SemaphoreType.DMA((6,)),
             pltpu.SemaphoreType.DMA((len(small),)),
         ],
         "project",
@@ -486,7 +497,7 @@
     moved = lax.all_to_all(
         sent.reshape(32, 9, 2, 128), "row", split_axis=0, concat_axis=0, tiled=True
     ).reshape(576, 128)
-    *prepared, gate = run(
+    *prepared, gate, kept_early = run(
         filter_kernel,
         (
             pltpu.VMEM((512, 128), F32),
@@ -498,20 +509,24 @@
             pltpu.VMEM((128, 128), F32),
             pltpu.VMEM((64, 128), F32),
             pltpu.VMEM((256, 128), F32),
+            pltpu.VMEM((EARLY, 2048), BF16),
         ),
-        tuple(near(value) for value in (rows, second, *small[:9])),
+        (*(near(value) for value in (rows, *small[:9])), *far(second_gate, output_weight)),
         [
             pltpu.VMEM((256, 128), F32),
             pltpu.VMEM((64, 256), BF16),
             pltpu.VMEM((64, 256), BF16),
             pltpu.VMEM((1024, 128), F32),
             pltpu.VMEM((32, 128), F32),
+            pltpu.VMEM((2048, 128), BF16),
+            pltpu.SemaphoreType.DMA((2,)),
         ],
         "filters",
+        2,
     )
     mixed, edges, kept = run(
         conv_kernel,
-        (pltpu.VMEM((32, 8, 128), BF16), pltpu.VMEM((2, 128), F32), pltpu.VMEM((1024, 2048), BF16)),
+        (pltpu.VMEM((32, 8, 128), BF16), pltpu.VMEM((2, 128), F32), pltpu.VMEM((1024 - EARLY, 2048), BF16)),
         (*(near(value) for value in (moved, *prepared, small[6])), *far(output_weight)),
         [
             pltpu.VMEM((576, 128), F32),
@@ -535,7 +550,7 @@
     return run(
         output_kernel,
         jax.ShapeDtypeStruct((32, 2048), BF16),
-        (near(gathered), near(kept)),
+        (near(gathered), near(kept_early), near(kept)),
         [],
         "output",
     )

time: 53.3 us -> 53.1 us (level)
  no operation moved by 1% of the time
where the time goes in v6:
time: 53.1 us; the launch traced here: 52.8 us
  blocking collectives  24.3 us (46%)
  starting transfers between devices  11.9 us (22%)
  Pallas kernels  11.4 us (21%)
  waiting for transfers between devices  5.16 us (10%)
    all_to_all x1, blocking collectives, local(): lax.all_to_all(mixed, 'row', split_axis=0, concat_axis=0, tiled=True)  12.5 us
    all_to_all x1, starting transfers between devices, local(): lax.all_to_all(sent.reshape(32, 9, 2, 128), 'row', split_axis=0, concat_a...  11.9 us
    all_to_all x1, blocking collectives, local(): lax.all_to_all(normed, 'col', split_axis=0, concat_axis=0, tiled=True)  11.8 us
    pallas_call x5, Pallas kernels, run(): pl.pallas_call(kernel, out_shape=out_shape, in_specs=[VMEM] * (len(inputs...  11.4 us
    all_to_all x1, waiting for transfers between devices, local(): lax.all_to_all(sent.reshape(32, 9, 2, 128), 'row', split_axis=0, concat_a...  5.16 us
  transfers between devices with their start and end apart: 1, of which 1 were waited for; matrix products, arithmetic and copies ran while one was open for 0% of the time, Pallas kernels for 8%

profile of v6, /device:TPU:1, one launch (start us, length us, event | category | flops | bytes accessed | tf_op | source)
XLA Modules:
  0.0 52.8 jit_solution(12095233893948121822)
XLA Ops:
  0.0 3.1 %project.1 = (bf16[576,128]{1,0:T(8,128)(2,1)}, bf16[256,2048]{1,0:T(8,128)(2,1)S(1)}, f32[33,64]{1,0:T(8,128)S(1)}, f32[1,64]{1,0:T(1,128)S(1)}, f32[64,64]{1,0...) custom-call(bf16[256,2048]{1,0:T(8,128)(2,1)} %refs_0_.1, ...), custom_call_target="tpu_custom_call" | custom-call | tf_op jit(solution)/shard_map/project/pallas_call | solution.py:427
  3.1 11.9 %all-to-all-start = ((bf16[32,9,2,128]{3,2,1,0:T(2,128)(2,1)}), bf16[32,9,2,128]{3,2,1,0:T(2,128)(2,1)S(1)}, u32[]{:S(2)}, u32[]{:S(2)}) async-start(bf16[32,9,2,128]{3,2,1,0:T(2,128)(2,1)} %bitcast.6), calls=%async_computation | async-start | bytes 294912 | tf_op jit(solution)/shard_map/all_to_all | solution.py:497
  15.0 4.5 %filters.1 = (f32[512,128]{1,0:T(8,128)S(1)}, f32[512,128]{1,0:T(8,128)S(1)}, bf16[128,192]{1,0:T(8,128)(2,1)S(1)}, bf16[64,384]{1,0:T(8,128)(2,1)S(1)}, bf16[51...) custom-call(bf16[256,2048]{1,0:T(8,128)(2,1)S(1)} %get-tuple-element, ...), custom_call_target="tpu_custom_call" | custom-call | tf_op jit(solution)/shard_map/filters/pallas_call | solution.py:427
  19.5 5.2 %all-to-all-done = bf16[32,9,2,128]{3,2,1,0:T(2,128)(2,1)S(1)} async-done(((bf16[32,9,2,128]{3,2,1,0:T(2,128)(2,1)}), bf16[32,9,2,128]{3,2,1,0:T(2,128)(2,1)S(1)}, u32[]{:S(2)}, u32[]{:S(2)}) %all-to-all-start) | async-done | bytes 147488 | tf_op jit(solution)/shard_map/all_to_all | solution.py:497
  24.6 2.1 %convolve.1 = (bf16[32,8,128]{2,1,0:T(8,128)(2,1)S(1)}, f32[2,128]{1,0:T(2,128)S(1)}, bf16[832,2048]{1,0:T(8,128)(2,1)S(1)}) custom-call(bf16[576,128]{1,0:T(8,128)(2,1)S(1)} %bitcast.8, f32[512,128]{1,0:T(8,128)S(1)} %get-tuple-element.41.hre, f32[512,128]{1,0:T(8,128)S(1)} %get-tuple-element.42.him, bf16[128,192]{1,0:T(8,128)(2,1)S(1)} %get-tuple-element.43.frows, ...), custom_call_target="tpu_custom_call" | custom-call | tf_op jit(solution)/shard_map/convolve/pallas_call | solution.py:427
  26.7 12.5 %all_to_all.15.moved = bf16[32,8,128]{2,1,0:T(8,128)(2,1)S(1)} all-to-all(bf16[32,8,128]{2,1,0:T(8,128)(2,1)S(1)} %get-tuple-element.49), channel_id=1, replica_groups=mesh['row'=32,'col'=8] {'row'}, dimensions={0} | all-to-all | bytes 131072 | tf_op jit(solution)/shard_map/all_to_all | solution.py:541
  39.2 0.2 groupnorm.1
  39.5 11.8 %all_to_all.16.mixed = bf16[8,32,128]{2,1,0:T(8,128)(2,1)S(1)} all-to-all(bf16[8,32,128]{2,1,0:T(8,128)(2,1)S(1)} %groupnorm.1), channel_id=1, replica_groups=mesh['row'=32,'col'=8] {'col'}, dimensions={0} | all-to-all | bytes 131072 | tf_op jit(solution)/shard_map/all_to_all | solution.py:549
  51.3 1.5 %output.1 = bf16[32,2048]{1,0:T(8,128)(2,1)} custom-call(bf16[8,32,128]{2,1,0:T(8,128)(2,1)S(1)} %all_to_all.16.mixed, bf16[192,2048]{1,0:T(8,128)(2,1)S(1)} %get-tuple-element.53.early, bf16[832,2048]{1,0:T(8,128)(2,1)S(1)} %get-tuple-element.54.late), custom_call_target="tpu_custom_call" | custom-call | tf_op jit(solution)/shard_map/output/pallas_call | solution.py:427
Async XLA Ops:
  3.1 21.5 %all-to-all-start = ((bf16[32,9,2,128]{3,2,1,0:T(2,128)(2,1)}), bf16[32,9,2,128]{3,2,1,0:T(2,128)(2,1)S(1)}, u32[]{:S(2)}, u32[]{:S(2)}) async-start(bf16[32,9,2,128]{3,2,1,0:T(2,128)(2,1)} %bitcast.6), calls=%async_computation | async-start | bytes 294912 | tf_op jit(solution)/shard_map/all_to_all | solution.py:497

commit v7 on v6

--- a/solution.py
+++ b/solution.py
@@ -367,14 +367,12 @@
             reals.append(real * tw_cos + imag * tw_sin)
             imags.append(imag * tw_cos - real * tw_sin)
         left = jnp.concatenate([jnp.concatenate(reals, axis=0), jnp.concatenate(imags, axis=0)], axis=1)
-        high = left.astype(BF16)
-        spectrum = dot(jnp.concatenate([high, high], axis=1), forward_lanes[...])
+        spectrum = dot(lanes3(left), repeat_high(forward_lanes))
         real, imag = spectrum[:, 0:128], spectrum[:, 128:256]
         at = pl.multiple_of(order * 256, 256)
         tap_real, tap_imag = hre[pl.ds(at, 256), :], him[pl.ds(at, 256), :]
         left = jnp.concatenate([real * tap_real - imag * tap_imag, real * tap_imag + imag * tap_real], axis=1)
-        high = left.astype(BF16)
-        back = dot(jnp.concatenate([high, high], axis=1), inverse_lanes[...])
+        back = dot(lanes3(left), repeat_high(inverse_lanes))
         columns = []
         for place in range(4):
             real = back[place * 64 : place * 64 + 64, 0:128]

time: 53.1 us -> 53.1 us (level)
  no operation moved by 1% of the time
where the time goes in v7:
time: 53.1 us; the launch traced here: 52.8 us
  blocking collectives  24.3 us (46%)
  starting transfers between devices  11.9 us (22%)
  Pallas kernels  11.4 us (21%)
  waiting for transfers between devices  5.16 us (10%)
    all_to_all x1, blocking collectives, local(): lax.all_to_all(mixed, 'row', split_axis=0, concat_axis=0, tiled=True)  12.5 us
    all_to_all x1, starting transfers between devices, local(): lax.all_to_all(sent.reshape(32, 9, 2, 128), 'row', split_axis=0, concat_a...  11.9 us
    all_to_all x1, blocking collectives, local(): lax.all_to_all(normed, 'col', split_axis=0, concat_axis=0, tiled=True)  11.8 us
    pallas_call x5, Pallas kernels, run(): pl.pallas_call(kernel, out_shape=out_shape, in_specs=[VMEM] * (len(inputs...  11.4 us
    all_to_all x1, waiting for transfers between devices, local(): lax.all_to_all(sent.reshape(32, 9, 2, 128), 'row', split_axis=0, concat_a...  5.16 us
  transfers between devices with their start and end apart: 1, of which 1 were waited for; matrix products, arithmetic and copies ran while one was open for 0% of the time, Pallas kernels for 8%

profile of v7, /device:TPU:1, one launch (start us, length us, event | category | flops | bytes accessed | tf_op | source)
XLA Modules:
  0.0 52.8 jit_solution(11142600490377898292)
XLA Ops:
  0.0 3.1 %project.1 = (bf16[576,128]{1,0:T(8,128)(2,1)}, bf16[256,2048]{1,0:T(8,128)(2,1)S(1)}, f32[33,64]{1,0:T(8,128)S(1)}, f32[1,64]{1,0:T(1,128)S(1)}, f32[64,64]{1,0...) custom-call(bf16[256,2048]{1,0:T(8,128)(2,1)} %refs_0_.1, ...), custom_call_target="tpu_custom_call" | custom-call | tf_op jit(solution)/shard_map/project/pallas_call | solution.py:425
  3.1 11.9 %all-to-all-start = ((bf16[32,9,2,128]{3,2,1,0:T(2,128)(2,1)}), bf16[32,9,2,128]{3,2,1,0:T(2,128)(2,1)S(1)}, u32[]{:S(2)}, u32[]{:S(2)}) async-start(bf16[32,9,2,128]{3,2,1,0:T(2,128)(2,1)} %bitcast.6), calls=%async_computation | async-start | bytes 294912 | tf_op jit(solution)/shard_map/all_to_all | solution.py:495
  15.0 4.5 %filters.1 = (f32[512,128]{1,0:T(8,128)S(1)}, f32[512,128]{1,0:T(8,128)S(1)}, bf16[128,192]{1,0:T(8,128)(2,1)S(1)}, bf16[64,384]{1,0:T(8,128)(2,1)S(1)}, bf16[51...) custom-call(bf16[256,2048]{1,0:T(8,128)(2,1)S(1)} %get-tuple-element, ...), custom_call_target="tpu_custom_call" | custom-call | tf_op jit(solution)/shard_map/filters/pallas_call | solution.py:425
  19.5 5.2 %all-to-all-done = bf16[32,9,2,128]{3,2,1,0:T(2,128)(2,1)S(1)} async-done(((bf16[32,9,2,128]{3,2,1,0:T(2,128)(2,1)}), bf16[32,9,2,128]{3,2,1,0:T(2,128)(2,1)S(1)}, u32[]{:S(2)}, u32[]{:S(2)}) %all-to-all-start) | async-done | bytes 147488 | tf_op jit(solution)/shard_map/all_to_all | solution.py:495
  24.6 2.1 %convolve.1 = (bf16[32,8,128]{2,1,0:T(8,128)(2,1)S(1)}, f32[2,128]{1,0:T(2,128)S(1)}, bf16[832,2048]{1,0:T(8,128)(2,1)S(1)}) custom-call(bf16[576,128]{1,0:T(8,128)(2,1)S(1)} %bitcast.8, f32[512,128]{1,0:T(8,128)S(1)} %get-tuple-element.41.hre, f32[512,128]{1,0:T(8,128)S(1)} %get-tuple-element.42.him, bf16[128,192]{1,0:T(8,128)(2,1)S(1)} %get-tuple-element.43.frows, ...), custom_call_target="tpu_custom_call" | custom-call | tf_op jit(solution)/shard_map/convolve/pallas_call | solution.py:425
  26.7 12.5 %all_to_all.15.moved = bf16[32,8,128]{2,1,0:T(8,128)(2,1)S(1)} all-to-all(bf16[32,8,128]{2,1,0:T(8,128)(2,1)S(1)} %get-tuple-element.49), channel_id=1, replica_groups=mesh['row'=32,'col'=8] {'row'}, dimensions={0} | all-to-all | bytes 131072 | tf_op jit(solution)/shard_map/all_to_all | solution.py:539
  39.3 0.2 groupnorm.1
  39.5 11.8 %all_to_all.16.mixed = bf16[8,32,128]{2,1,0:T(8,128)(2,1)S(1)} all-to-all(bf16[8,32,128]{2,1,0:T(8,128)(2,1)S(1)} %groupnorm.1), channel_id=1, replica_groups=mesh['row'=32,'col'=8] {'col'}, dimensions={0} | all-to-all | bytes 131072 | tf_op jit(solution)/shard_map/all_to_all | solution.py:547
  51.3 1.5 %output.1 = bf16[32,2048]{1,0:T(8,128)(2,1)} custom-call(bf16[8,32,128]{2,1,0:T(8,128)(2,1)S(1)} %all_to_all.16.mixed, bf16[192,2048]{1,0:T(8,128)(2,1)S(1)} %get-tuple-element.53.early, bf16[832,2048]{1,0:T(8,128)(2,1)S(1)} %get-tuple-element.54.late), custom_call_target="tpu_custom_call" | custom-call | tf_op jit(solution)/shard_map/output/pallas_call | solution.py:425
Async XLA Ops:
  3.1 21.5 %all-to-all-start = ((bf16[32,9,2,128]{3,2,1,0:T(2,128)(2,1)}), bf16[32,9,2,128]{3,2,1,0:T(2,128)(2,1)S(1)}, u32[]{:S(2)}, u32[]{:S(2)}) async-start(bf16[32,9,2,128]{3,2,1,0:T(2,128)(2,1)} %bitcast.6), calls=%async_computation | async-start | bytes 294912 | tf_op jit(solution)/shard_map/all_to_all | solution.py:495

commit v8 on v6

--- a/solution.py
+++ b/solution.py
@@ -117,8 +117,10 @@
         pltpu.make_async_copy(source, target, carry.at[index])
         for index, (source, target) in enumerate(zip(small, carried))
     ]
-    for copy in copies:
+    for copy in copies[:3]:
         copy.start()
+    for copy in copies[3:]:
+        copy.start(priority=1)
     copies[0].wait()
     for part in range(2):
         copies[part + 1].wait()
@@ -138,10 +140,10 @@
                 start = peer * 18 + half * 9 + branch * 4
                 scratch[start : start + 4, :] = block[peer * 4 : peer * 4 + 4, :]
     copies[5].wait()
-    edges = dot(jnp.concatenate([normed[0:16, :], normed[240:256, :]], axis=0), n1[...])
+    edges = dot(jnp.concatenate([normed[0:8, :], normed[248:256, :]], axis=0), n1[...])
     for peer in range(32):
         scratch[peer * 18 + 8 : peer * 18 + 9, :] = edges[0:1, :]
-        scratch[peer * 18 + 17 : peer * 18 + 18, :] = edges[31:32, :]
+        scratch[peer * 18 + 17 : peer * 18 + 18, :] = edges[15:16, :]
     out[...] = scratch[...].astype(BF16)
     for copy in carries:
         copy.wait()

time: 53.1 us -> 53 us (level)
  no operation moved by 1% of the time
where the time goes in v8:
time: 53 us; the launch traced here: 52.8 us
  blocking collectives  24.3 us (46%)
  starting transfers between devices  11.9 us (22%)
  Pallas kernels  11.4 us (22%)
  waiting for transfers between devices  5.16 us (10%)
    all_to_all x1, blocking collectives, local(): lax.all_to_all(mixed, 'row', split_axis=0, concat_axis=0, tiled=True)  12.5 us
    all_to_all x1, starting transfers between devices, local(): lax.all_to_all(sent.reshape(32, 9, 2, 128), 'row', split_axis=0, concat_a...  11.9 us
    all_to_all x1, blocking collectives, local(): lax.all_to_all(normed, 'col', split_axis=0, concat_axis=0, tiled=True)  11.8 us
    pallas_call x5, Pallas kernels, run(): pl.pallas_call(kernel, out_shape=out_shape, in_specs=[VMEM] * (len(inputs...  11.4 us
    all_to_all x1, waiting for transfers between devices, local(): lax.all_to_all(sent.reshape(32, 9, 2, 128), 'row', split_axis=0, concat_a...  5.16 us
  transfers between devices with their start and end apart: 1, of which 1 were waited for; matrix products, arithmetic and copies ran while one was open for 0% of the time, Pallas kernels for 8%

profile of v8, /device:TPU:1, one launch (start us, length us, event | category | flops | bytes accessed | tf_op | source)
XLA Modules:
  0.0 52.8 jit_solution(14439240300700264183)
XLA Ops:
  0.0 3.1 %project.1 = (bf16[576,128]{1,0:T(8,128)(2,1)}, bf16[256,2048]{1,0:T(8,128)(2,1)S(1)}, f32[33,64]{1,0:T(8,128)S(1)}, f32[1,64]{1,0:T(1,128)S(1)}, f32[64,64]{1,0...) custom-call(bf16[256,2048]{1,0:T(8,128)(2,1)} %refs_0_.1, ...), custom_call_target="tpu_custom_call" | custom-call | tf_op jit(solution)/shard_map/project/pallas_call | solution.py:429
  3.1 11.9 %all-to-all-start = ((bf16[32,9,2,128]{3,2,1,0:T(2,128)(2,1)}), bf16[32,9,2,128]{3,2,1,0:T(2,128)(2,1)S(1)}, u32[]{:S(2)}, u32[]{:S(2)}) async-start(bf16[32,9,2,128]{3,2,1,0:T(2,128)(2,1)} %bitcast.6), calls=%async_computation | async-start | bytes 294912 | tf_op jit(solution)/shard_map/all_to_all | solution.py:499
  15.0 4.5 %filters.1 = (f32[512,128]{1,0:T(8,128)S(1)}, f32[512,128]{1,0:T(8,128)S(1)}, bf16[128,192]{1,0:T(8,128)(2,1)S(1)}, bf16[64,384]{1,0:T(8,128)(2,1)S(1)}, bf16[51...) custom-call(bf16[256,2048]{1,0:T(8,128)(2,1)S(1)} %get-tuple-element, ...), custom_call_target="tpu_custom_call" | custom-call | tf_op jit(solution)/shard_map/filters/pallas_call | solution.py:429
  19.5 5.2 %all-to-all-done = bf16[32,9,2,128]{3,2,1,0:T(2,128)(2,1)S(1)} async-done(((bf16[32,9,2,128]{3,2,1,0:T(2,128)(2,1)}), bf16[32,9,2,128]{3,2,1,0:T(2,128)(2,1)S(1)}, u32[]{:S(2)}, u32[]{:S(2)}) %all-to-all-start) | async-done | bytes 147488 | tf_op jit(solution)/shard_map/all_to_all | solution.py:499
  24.6 2.1 %convolve.1 = (bf16[32,8,128]{2,1,0:T(8,128)(2,1)S(1)}, f32[2,128]{1,0:T(2,128)S(1)}, bf16[832,2048]{1,0:T(8,128)(2,1)S(1)}) custom-call(bf16[576,128]{1,0:T(8,128)(2,1)S(1)} %bitcast.8, f32[512,128]{1,0:T(8,128)S(1)} %get-tuple-element.41.hre, f32[512,128]{1,0:T(8,128)S(1)} %get-tuple-element.42.him, bf16[128,192]{1,0:T(8,128)(2,1)S(1)} %get-tuple-element.43.frows, ...), custom_call_target="tpu_custom_call" | custom-call | tf_op jit(solution)/shard_map/convolve/pallas_call | solution.py:429
  26.7 12.5 %all_to_all.15.moved = bf16[32,8,128]{2,1,0:T(8,128)(2,1)S(1)} all-to-all(bf16[32,8,128]{2,1,0:T(8,128)(2,1)S(1)} %get-tuple-element.49), channel_id=1, replica_groups=mesh['row'=32,'col'=8] {'row'}, dimensions={0} | all-to-all | bytes 131072 | tf_op jit(solution)/shard_map/all_to_all | solution.py:543
  39.2 0.2 groupnorm.1
  39.5 11.8 %all_to_all.16.mixed = bf16[8,32,128]{2,1,0:T(8,128)(2,1)S(1)} all-to-all(bf16[8,32,128]{2,1,0:T(8,128)(2,1)S(1)} %groupnorm.1), channel_id=1, replica_groups=mesh['row'=32,'col'=8] {'col'}, dimensions={0} | all-to-all | bytes 131072 | tf_op jit(solution)/shard_map/all_to_all | solution.py:551
  51.3 1.5 %output.1 = bf16[32,2048]{1,0:T(8,128)(2,1)} custom-call(bf16[8,32,128]{2,1,0:T(8,128)(2,1)S(1)} %all_to_all.16.mixed, bf16[192,2048]{1,0:T(8,128)(2,1)S(1)} %get-tuple-element.53.early, bf16[832,2048]{1,0:T(8,128)(2,1)S(1)} %get-tuple-element.54.late), custom_call_target="tpu_custom_call" | custom-call | tf_op jit(solution)/shard_map/output/pallas_call | solution.py:429
Async XLA Ops:
  3.1 21.5 %all-to-all-start = ((bf16[32,9,2,128]{3,2,1,0:T(2,128)(2,1)}), bf16[32,9,2,128]{3,2,1,0:T(2,128)(2,1)S(1)}, u32[]{:S(2)}, u32[]{:S(2)}) async-start(bf16[32,9,2,128]{3,2,1,0:T(2,128)(2,1)} %bitcast.6), calls=%async_computation | async-start | bytes 294912 | tf_op jit(solution)/shard_map/all_to_all | solution.py:499

commit v9 on v8

--- a/solution.py
+++ b/solution.py
@@ -166,9 +166,9 @@
 ):
     length = 8192
     fetch_second = pltpu.make_async_copy(second_weight, w1, arrived.at[1])
-    fetch_second.start()
+    fetch_second.start(priority=1)
     fetch = pltpu.make_async_copy(weight.at[0:EARLY], kept, arrived.at[0])
-    fetch.start()
+    fetch.start(priority=1)
     own = lax.axis_index("row") * 4
     first_channel = lax.axis_index("col") * 128 + own
 
@@ -333,7 +333,7 @@
     out, edges, kept, wide, result, state, factors, arrived,
 ):
     fetch = pltpu.make_async_copy(weight.at[EARLY:1024], kept, arrived)
-    fetch.start()
+    fetch.start(priority=1)
     wide[...] = moved[...].astype(F32)
     own = lax.axis_index("row")
     before = wide[pl.ds(jnp.maximum(own - 1, 0) * 18 + 17, 1), :]

time: 53 us -> 53 us (level)
  no operation moved by 1% of the time
where the time goes in v9:
time: 53 us; the launch traced here: 52.8 us
  blocking collectives  24.3 us (46%)
  starting transfers between devices  11.9 us (22%)
  Pallas kernels  11.4 us (22%)
  waiting for transfers between devices  5.16 us (10%)
    all_to_all x1, blocking collectives, local(): lax.all_to_all(mixed, 'row', split_axis=0, concat_axis=0, tiled=True)  12.5 us
    all_to_all x1, starting transfers between devices, local(): lax.all_to_all(sent.reshape(32, 9, 2, 128), 'row', split_axis=0, concat_a...  11.9 us
    all_to_all x1, blocking collectives, local(): lax.all_to_all(normed, 'col', split_axis=0, concat_axis=0, tiled=True)  11.8 us
    pallas_call x5, Pallas kernels, run(): pl.pallas_call(kernel, out_shape=out_shape, in_specs=[VMEM] * (len(inputs...  11.4 us
    all_to_all x1, waiting for transfers between devices, local(): lax.all_to_all(sent.reshape(32, 9, 2, 128), 'row', split_axis=0, concat_a...  5.16 us
  transfers between devices with their start and end apart: 1, of which 1 were waited for; matrix products, arithmetic and copies ran while one was open for 0% of the time, Pallas kernels for 8%

profile of v9, /device:TPU:1, one launch (start us, length us, event | category | flops | bytes accessed | tf_op | source)
XLA Modules:
  0.0 52.8 jit_solution(6756776248316780090)
XLA Ops:
  0.0 3.1 %project.1 = (bf16[576,128]{1,0:T(8,128)(2,1)}, bf16[256,2048]{1,0:T(8,128)(2,1)S(1)}, f32[33,64]{1,0:T(8,128)S(1)}, f32[1,64]{1,0:T(1,128)S(1)}, f32[64,64]{1,0...) custom-call(bf16[256,2048]{1,0:T(8,128)(2,1)} %refs_0_.1, ...), custom_call_target="tpu_custom_call" | custom-call | tf_op jit(solution)/shard_map/project/pallas_call | solution.py:429
  3.1 11.9 %all-to-all-start = ((bf16[32,9,2,128]{3,2,1,0:T(2,128)(2,1)}), bf16[32,9,2,128]{3,2,1,0:T(2,128)(2,1)S(1)}, u32[]{:S(2)}, u32[]{:S(2)}) async-start(bf16[32,9,2,128]{3,2,1,0:T(2,128)(2,1)} %bitcast.6), calls=%async_computation | async-start | bytes 294912 | tf_op jit(solution)/shard_map/all_to_all | solution.py:499
  15.0 4.5 %filters.1 = (f32[512,128]{1,0:T(8,128)S(1)}, f32[512,128]{1,0:T(8,128)S(1)}, bf16[128,192]{1,0:T(8,128)(2,1)S(1)}, bf16[64,384]{1,0:T(8,128)(2,1)S(1)}, bf16[51...) custom-call(bf16[256,2048]{1,0:T(8,128)(2,1)S(1)} %get-tuple-element, ...), custom_call_target="tpu_custom_call" | custom-call | tf_op jit(solution)/shard_map/filters/pallas_call | solution.py:429
  19.5 5.2 %all-to-all-done = bf16[32,9,2,128]{3,2,1,0:T(2,128)(2,1)S(1)} async-done(((bf16[32,9,2,128]{3,2,1,0:T(2,128)(2,1)}), bf16[32,9,2,128]{3,2,1,0:T(2,128)(2,1)S(1)}, u32[]{:S(2)}, u32[]{:S(2)}) %all-to-all-start) | async-done | bytes 147488 | tf_op jit(solution)/shard_map/all_to_all | solution.py:499
  24.6 2.1 %convolve.1 = (bf16[32,8,128]{2,1,0:T(8,128)(2,1)S(1)}, f32[2,128]{1,0:T(2,128)S(1)}, bf16[832,2048]{1,0:T(8,128)(2,1)S(1)}) custom-call(bf16[576,128]{1,0:T(8,128)(2,1)S(1)} %bitcast.8, f32[512,128]{1,0:T(8,128)S(1)} %get-tuple-element.41.hre, f32[512,128]{1,0:T(8,128)S(1)} %get-tuple-element.42.him, bf16[128,192]{1,0:T(8,128)(2,1)S(1)} %get-tuple-element.43.frows, ...), custom_call_target="tpu_custom_call" | custom-call | tf_op jit(solution)/shard_map/convolve/pallas_call | solution.py:429
  26.7 12.5 %all_to_all.15.moved = bf16[32,8,128]{2,1,0:T(8,128)(2,1)S(1)} all-to-all(bf16[32,8,128]{2,1,0:T(8,128)(2,1)S(1)} %get-tuple-element.49), channel_id=1, replica_groups=mesh['row'=32,'col'=8] {'row'}, dimensions={0} | all-to-all | bytes 131072 | tf_op jit(solution)/shard_map/all_to_all | solution.py:543
  39.2 0.2 groupnorm.1
  39.5 11.8 %all_to_all.16.mixed = bf16[8,32,128]{2,1,0:T(8,128)(2,1)S(1)} all-to-all(bf16[8,32,128]{2,1,0:T(8,128)(2,1)S(1)} %groupnorm.1), channel_id=1, replica_groups=mesh['row'=32,'col'=8] {'col'}, dimensions={0} | all-to-all | bytes 131072 | tf_op jit(solution)/shard_map/all_to_all | solution.py:551
  51.3 1.5 %output.1 = bf16[32,2048]{1,0:T(8,128)(2,1)} custom-call(bf16[8,32,128]{2,1,0:T(8,128)(2,1)S(1)} %all_to_all.16.mixed, bf16[192,2048]{1,0:T(8,128)(2,1)S(1)} %get-tuple-element.53.early, bf16[832,2048]{1,0:T(8,128)(2,1)S(1)} %get-tuple-element.54.late), custom_call_target="tpu_custom_call" | custom-call | tf_op jit(solution)/shard_map/output/pallas_call | solution.py:429
Async XLA Ops:
  3.1 21.5 %all-to-all-start = ((bf16[32,9,2,128]{3,2,1,0:T(2,128)(2,1)}), bf16[32,9,2,128]{3,2,1,0:T(2,128)(2,1)S(1)}, u32[]{:S(2)}, u32[]{:S(2)}) async-start(bf16[32,9,2,128]{3,2,1,0:T(2,128)(2,1)} %bitcast.6), calls=%async_computation | async-start | bytes 294912 | tf_op jit(solution)/shard_map/all_to_all | solution.py:499

commit v10 on v8

--- a/solution.py
+++ b/solution.py
@@ -10,7 +10,7 @@
 
 CHANNELS = 1024
 FREQ_BANDS = 16
-EARLY = 192
+EARLY = 224
 NORM_EPS = 1e-06
 DECAY_SLOW = math.log(0.01) / 1.5
 DECAY_FAST = math.log(0.01) / 0.3

time: 53 us -> 59.9 us (1.13)
  local copies, waits for them, and re-layouts: 0 us -> 6.77 us
  blocking collectives: 24.3 us -> 27.7 us
  waiting for transfers between devices: 5.16 us -> 1.78 us
    unnamed x0 -> x24, local copies, waits for them, and re-layouts: none -> 6.77 us
    all_to_all x1, waiting for transfers between devices: 5.16 us -> 1.78 us  [local(): lax.all_to_all(sent.reshape(32, 9, 2, 128), 'row', split_axis=0, concat_a...]
    all_to_all x1, blocking collectives: 12.5 us -> 15.9 us  [local(): lax.all_to_all(mixed, 'row', split_axis=0, concat_axis=0, tiled=True)]
  transfers between devices with their start and end apart: 1 -> 1, of which waited for: 1 -> 1; matrix products, arithmetic and copies ran while one was open for 0% -> 0% of each run, Pallas kernels for 8% -> 7%
where the time goes in v10:
time: 59.9 us; the launch traced here: 59.5 us
  blocking collectives  27.7 us (46%)
  starting transfers between devices  11.9 us (20%)
  Pallas kernels  11.4 us (19%)
  local copies, waits for them, and re-layouts  6.77 us (11%)
  waiting for transfers between devices  1.78 us (3%)
    all_to_all x1, blocking collectives, local(): lax.all_to_all(mixed, 'row', split_axis=0, concat_axis=0, tiled=True)  15.9 us
    all_to_all x1, starting transfers between devices, local(): lax.all_to_all(sent.reshape(32, 9, 2, 128), 'row', split_axis=0, concat_a...  11.9 us
    all_to_all x1, blocking collectives, local(): lax.all_to_all(normed, 'col', split_axis=0, concat_axis=0, tiled=True)  11.8 us
    pallas_call x5, Pallas kernels, run(): pl.pallas_call(kernel, out_shape=out_shape, in_specs=[VMEM] * (len(inputs...  11.4 us
    unnamed x24, local copies, waits for them, and re-layouts  6.77 us
    all_to_all x1, waiting for transfers between devices, local(): lax.all_to_all(sent.reshape(32, 9, 2, 128), 'row', split_axis=0, concat_a...  1.78 us
  transfers between devices with their start and end apart: 1, of which 1 were waited for; matrix products, arithmetic and copies ran while one was open for 0% of the time, Pallas kernels for 7%

profile of v10, /device:TPU:1, one launch (start us, length us, event | category | flops | bytes accessed | tf_op | source)
XLA Modules:
  0.0 59.5 jit_solution(18150329520945494067)
XLA Ops:
  0.0 3.1 %project.1 = (bf16[576,128]{1,0:T(8,128)(2,1)}, bf16[256,2048]{1,0:T(8,128)(2,1)S(1)}, f32[33,64]{1,0:T(8,128)S(1)}, f32[1,64]{1,0:T(1,128)S(1)}, f32[64,64]{1,0...) custom-call(bf16[256,2048]{1,0:T(8,128)(2,1)} %refs_0_.1, ...), custom_call_target="tpu_custom_call" | custom-call | tf_op jit(solution)/shard_map/project/pallas_call | solution.py:429
  3.1 0.0 copy-start
  3.1 0.6 %copy-done = f32[33,64]{1,0:T(8,128)} copy-done((f32[33,64]{1,0:T(8,128)}, f32[33,64]{1,0:T(8,128)S(1)}, u32[]{:S(2)}) %copy-start) | copy-done | bytes 8472
  3.7 0.0 copy-start.2
  3.7 0.6 copy-done.2
  4.3 0.0 copy-start.4
  4.3 0.5 copy-done.4
  4.8 0.0 copy-start.6
  4.8 0.6 copy-done.6
  5.4 0.0 copy-start.8
  5.4 0.6 copy-done.8
  6.0 0.0 copy-start.10
  6.0 0.5 copy-done.10
  6.5 11.9 %all-to-all-start = ((bf16[32,9,2,128]{3,2,1,0:T(2,128)(2,1)}), bf16[32,9,2,128]{3,2,1,0:T(2,128)(2,1)S(1)}, u32[]{:S(2)}, u32[]{:S(2)}) async-start(bf16[32,9,2,128]{3,2,1,0:T(2,128)(2,1)} %bitcast.6), calls=%async_computation | async-start | bytes 294912 | tf_op jit(solution)/shard_map/all_to_all | solution.py:499
  18.4 0.0 copy-start.1
  18.4 0.7 %copy-done.1 = f32[33,64]{1,0:T(8,128)S(1)} copy-done((f32[33,64]{1,0:T(8,128)S(1)}, f32[33,64]{1,0:T(8,128)}, u32[]{:S(2)}) %copy-start.1) | copy-done | bytes 8472
  19.1 0.0 copy-start.3
  19.1 0.7 %copy-done.3 = f32[2,4]{1,0:T(2,128)S(1)} copy-done((f32[2,4]{1,0:T(2,128)S(1)}, f32[2,4]{1,0:T(2,128)}, u32[]{:S(2)}) %copy-start.3) | copy-done | bytes 56
  19.8 0.0 copy-start.7
  19.8 0.7 %copy-done.7 = f32[1,64]{1,0:T(1,128)S(1)} copy-done((f32[1,64]{1,0:T(1,128)S(1)}, f32[1,64]{1,0:T(1,128)}, u32[]{:S(2)}) %copy-start.7) | copy-done | bytes 280
  20.5 0.0 copy-start.9
  20.5 0.7 %copy-done.9 = f32[1,64]{1,0:T(1,128)S(1)} copy-done((f32[1,64]{1,0:T(1,128)S(1)}, f32[1,64]{1,0:T(1,128)}, u32[]{:S(2)}) %copy-start.9) | copy-done | bytes 280
  21.2 0.0 copy-start.11
  21.2 0.6 %copy-done.11 = f32[1,64]{1,0:T(1,128)S(1)} copy-done((f32[1,64]{1,0:T(1,128)S(1)}, f32[1,64]{1,0:T(1,128)}, u32[]{:S(2)}) %copy-start.11) | copy-done | bytes 280
  21.8 4.4 %filters.1 = (f32[512,128]{1,0:T(8,128)S(1)}, f32[512,128]{1,0:T(8,128)S(1)}, bf16[128,192]{1,0:T(8,128)(2,1)S(1)}, bf16[64,384]{1,0:T(8,128)(2,1)S(1)}, bf16[51...) custom-call(bf16[256,2048]{1,0:T(8,128)(2,1)S(1)} %get-tuple-element, ...), custom_call_target="tpu_custom_call" | custom-call | tf_op jit(solution)/shard_map/filters/pallas_call | solution.py:429
  26.2 0.0 copy-start.5
  26.2 1.8 %all-to-all-done = bf16[32,9,2,128]{3,2,1,0:T(2,128)(2,1)S(1)} async-done(((bf16[32,9,2,128]{3,2,1,0:T(2,128)(2,1)}), bf16[32,9,2,128]{3,2,1,0:T(2,128)(2,1)S(1)}, u32[]{:S(2)}, u32[]{:S(2)}) %all-to-all-start) | async-done | bytes 147488 | tf_op jit(solution)/shard_map/all_to_all | solution.py:499
  28.0 2.0 %convolve.1 = (bf16[32,8,128]{2,1,0:T(8,128)(2,1)S(1)}, f32[2,128]{1,0:T(2,128)S(1)}, bf16[800,2048]{1,0:T(8,128)(2,1)S(1)}) custom-call(bf16[576,128]{1,0:T(8,128)(2,1)S(1)} %bitcast.8, f32[512,128]{1,0:T(8,128)S(1)} %get-tuple-element.41.hre, f32[512,128]{1,0:T(8,128)S(1)} %get-tuple-element.42.him, bf16[128,192]{1,0:T(8,128)(2,1)S(1)} %get-tuple-element.43.frows, ...), custom_call_target="tpu_custom_call" | custom-call | tf_op jit(solution)/shard_map/convolve/pallas_call | solution.py:429
  30.1 15.9 %all_to_all.15.moved = bf16[32,8,128]{2,1,0:T(8,128)(2,1)S(1)} all-to-all(bf16[32,8,128]{2,1,0:T(8,128)(2,1)S(1)} %get-tuple-element.49), channel_id=1, replica_groups=mesh['row'=32,'col'=8] {'row'}, dimensions={0} | all-to-all | bytes 131072 | tf_op jit(solution)/shard_map/all_to_all | solution.py:543
  46.0 0.0 copy-done.5
  46.0 0.2 groupnorm.1
  46.2 11.8 %all_to_all.16.mixed = bf16[8,32,128]{2,1,0:T(8,128)(2,1)S(1)} all-to-all(bf16[8,32,128]{2,1,0:T(8,128)(2,1)S(1)} %groupnorm.1), channel_id=1, replica_groups=mesh['row'=32,'col'=8] {'col'}, dimensions={0} | all-to-all | bytes 131072 | tf_op jit(solution)/shard_map/all_to_all | solution.py:551
  58.0 1.5 %output.1 = bf16[32,2048]{1,0:T(8,128)(2,1)} custom-call(bf16[8,32,128]{2,1,0:T(8,128)(2,1)S(1)} %all_to_all.16.mixed, bf16[224,2048]{1,0:T(8,128)(2,1)S(1)} %get-tuple-element.53.early, bf16[800,2048]{1,0:T(8,128)(2,1)S(1)} %get-tuple-element.54.late), custom_call_target="tpu_custom_call" | custom-call | tf_op jit(solution)/shard_map/output/pallas_call | solution.py:429
Async XLA Ops:
  3.1 0.6 %copy-start = (f32[33,64]{1,0:T(8,128)}, f32[33,64]{1,0:T(8,128)S(1)}, u32[]{:S(2)}) copy-start(f32[33,64]{1,0:T(8,128)S(1)} %get-tuple-element.32.ew) | copy-start | bytes 25348
  3.7 0.6 copy-start.2
  4.3 0.5 copy-start.4
  4.8 0.6 copy-start.6
  5.4 0.6 copy-start.8
  6.0 0.5 copy-start.10
  6.5 21.5 %all-to-all-start = ((bf16[32,9,2,128]{3,2,1,0:T(2,128)(2,1)}), bf16[32,9,2,128]{3,2,1,0:T(2,128)(2,1)S(1)}, u32[]{:S(2)}, u32[]{:S(2)}) async-start(bf16[32,9,2,128]{3,2,1,0:T(2,128)(2,1)} %bitcast.6), calls=%async_computation | async-start | bytes 294912 | tf_op jit(solution)/shard_map/all_to_all | solution.py:499
  18.4 0.7 %copy-start.1 = (f32[33,64]{1,0:T(8,128)S(1)}, f32[33,64]{1,0:T(8,128)}, u32[]{:S(2)}) copy-start(f32[33,64]{1,0:T(8,128)} %copy-done) | copy-start | bytes 25348
  19.1 0.7 %copy-start.3 = (f32[2,4]{1,0:T(2,128)S(1)}, f32[2,4]{1,0:T(2,128)}, u32[]{:S(2)}) copy-start(f32[2,4]{1,0:T(2,128)} %copy-done.2) | copy-start | bytes 100
  19.8 0.7 %copy-start.7 = (f32[1,64]{1,0:T(1,128)S(1)}, f32[1,64]{1,0:T(1,128)}, u32[]{:S(2)}) copy-start(f32[1,64]{1,0:T(1,128)} %copy-done.6) | copy-start | bytes 772
  20.5 0.7 %copy-start.9 = (f32[1,64]{1,0:T(1,128)S(1)}, f32[1,64]{1,0:T(1,128)}, u32[]{:S(2)}) copy-start(f32[1,64]{1,0:T(1,128)} %copy-done.8) | copy-start | bytes 772
  21.2 0.6 %copy-start.11 = (f32[1,64]{1,0:T(1,128)S(1)}, f32[1,64]{1,0:T(1,128)}, u32[]{:S(2)}) copy-start(f32[1,64]{1,0:T(1,128)} %copy-done.10) | copy-start | bytes 772
  26.2 19.7 %copy-start.5 = (f32[1,128]{1,0:T(1,128)S(1)}, f32[1,128]{1,0:T(1,128)}, u32[]{:S(2)}) copy-start(f32[1,128]{1,0:T(1,128)} %copy-done.4) | copy-start | bytes 1540
